TPU v7x, 256 devices: a whole 4x4x8 slice. The times are simulated.
256 devices in a mesh: ep: 64 (over z, x, core), tp: 4 (over y).
Axes of the slice: x: 4, y: 4, z: 8, core: 2. Of those that a mesh axis runs over, the one named last changes fastest.
Arguments:
- queries: bfloat16 [16384, 1024], P('ep', 'tp'), may hold values from -6 to 6
- key_rows: bfloat16 [16384, 1024], P('ep', 'tp'), may hold values from -6 to 6
- value_rows: bfloat16 [16384, 1024], P('ep', 'tp'), may hold values from -6 to 6
- out_gate: bfloat16 [16384, 1024], P('ep', 'tp'), may hold values from -6 to 6
- log_decay: float32 [16384, 8], P('ep', 'tp'), may hold values from -3 to 0, as said below
- head_gain: float32 [8, 128], P('tp'), may hold values from 0.1 to 1.9
- out_weight: bfloat16 [1024, 2048], P('tp'), may hold values from -0.1875 to 0.1875
- moe_input: bfloat16 [8192, 2048], P('ep'), may hold values from -6 to 6
- moe_gain: float32 [2048], replicated, may hold values from 0.1 to 1.9
- expert_gate: bfloat16 [64, 2048, 3584], P('ep', None, 'tp'), may hold values from -0.125 to 0.125
- expert_up: bfloat16 [64, 2048, 3584], P('ep', None, 'tp'), may hold values from -0.125 to 0.125
- expert_down: bfloat16 [64, 3584, 2048], P('ep', 'tp'), may hold values from -0.125 to 0.125
- route_ids: int32 [8192, 2], P('ep'), may hold values from 0 to 63, all different within a row; in each aligned block of 128 rows (0 to 127, 128 to 255, ...) at most 8 rows name the same one
- route_weights: float32 [8192, 2], P('ep'), may hold values from 0.2 to 1
Outputs:
- mixer_out: bfloat16 [16384, 2048], P(('ep', 'tp'))
- expert_out: bfloat16 [8192, 2048], P('ep', 'tp')
Inputs may be any that keep to these rules, and one draw needn't show every extreme that they name: `route_ids`: among the 2 entries of a row no expert repeats. In each aligned block of 128 rows (the rows of one index of ep) no expert is named more than 8 times, a bound that some block reaches. `log_decay`: every entry is negative.
All inputs are finite; a program needn't handle non-finite values.
Results may differ from a plain program's by a relative error of at most 0.017.
Values may be sent and summed in bfloat16 or wider, within the bound.
No kernel may reach another device: no remote copies, remote signals or barrier semaphores. Data moves between devices by JAX's collectives and lax.ppermute only.
A program may use at most 64 MiB of HBM per device.

v0:
```python
import jax
import jax.numpy as jnp
from jax import lax
from jax.sharding import Mesh
from jax.sharding import PartitionSpec as P

TOP = 2
EP = ("ep_0", "ep_1", "ep_2")
EP_TP = ("ep_0", "ep_1", "ep_2", "tp")


epsilon = 1e-06


def filled_with(x, identity):
    return jax.tree.map(
        lambda a, e: jnp.broadcast_to(jnp.asarray(e, a.dtype), a.shape), x, identity
    )


def prefix_by_axis(x, axes, combine, identity):
    before = start = filled_with(x, identity)
    so_far = x
    for axis in reversed(axes):
        size, index = (lax.axis_size(axis), lax.axis_index(axis))
        pieces = jax.tree.map(
            lambda part, kind: lax.all_gather(part.astype(kind), axis),
            so_far,
            (jnp.bfloat16, jnp.bfloat16),
        )
        inside, so_far = (start, start)
        for k in range(size):
            passed = k < index
            so_far = combine(
                so_far, jax.tree.map(lambda part, own: part[k].astype(own.dtype), pieces, x)
            )
            inside = jax.tree.map(lambda new, old: jnp.where(passed, new, old), so_far, inside)
        before = combine(inside, before)
    return before


def in_blocks(x, dim, size):
    before, after = (x.shape[:dim], x.shape[dim + 1 :])
    return jnp.moveaxis(x.reshape(*before, size, -1, *after), dim, 0)


def sent_and_summed(x, axis, dim):
    size = lax.axis_size(axis)
    parts = lax.all_to_all(in_blocks(x, dim, size), axis, 0, 0, tiled=True)
    return jnp.sum(parts.astype(jnp.float32), axis=0)


def joined_along(parts, dim):
    shape = list(parts.shape[1:])
    shape[dim] *= parts.shape[0]
    return jnp.moveaxis(parts, 0, dim).reshape(shape)


def exchange_in_order(parts, axes, turns):
    shape = [lax.axis_size(a) for a in axes]
    parts = parts.reshape(*shape, *parts.shape[1:])
    for k in turns:
        parts = lax.all_to_all(parts, axes[k], split_axis=k, concat_axis=k, tiled=True)
    return parts.reshape(-1, *parts.shape[len(axes) :])


def exchange_by_chip(x, groups, turns, split_dim, concat_dim):
    size = lax.axis_size(groups[0]) * lax.axis_size(groups[1])
    parts = in_blocks(x, split_dim, size)
    return joined_along(exchange_in_order(parts, groups, turns), concat_dim)


def sent_to_all(x, axis):
    size = lax.axis_size(axis)
    return lax.all_to_all(jnp.broadcast_to(x[None], (size, *x.shape)), axis, 0, 0, tiled=True)


def gather_directly(x, axis, dim):
    parts = sent_to_all(x, axis)
    return joined_along(parts, dim)


def combine_states(earlier, later):
    return (earlier[0] + later[0], jnp.exp(later[0])[:, None, None] * earlier[1] + later[1])


def retention_half(queries, key_rows, value_rows, out_gate, log_decay, head_gain, out_weight):
    length = queries.shape[0]
    local_heads = log_decay.shape[1]
    head_dim = queries.shape[1] // local_heads
    query_heads = queries.reshape(length, local_heads, head_dim)
    key_heads = key_rows.reshape(length, local_heads, head_dim)
    value_heads = value_rows.reshape(length, local_heads, head_dim)
    cumulative = jnp.cumsum(log_decay, axis=0)
    block_total = cumulative[-1]
    scores = jnp.einsum(
        "thd,shd->hts", query_heads, key_heads, preferred_element_type=jnp.float32
    ) * head_dim ** (-0.5)
    level = cumulative.T
    causal = lax.broadcasted_iota(jnp.int32, (length, length), 0) >= lax.broadcasted_iota(
        jnp.int32, (length, length), 1
    )
    spread = jnp.where(causal[None], level[:, :, None] - level[:, None, :], -jnp.inf)
    weights = (scores * jnp.exp(spread)).astype(jnp.bfloat16)
    inner = jnp.einsum("hts,shd->thd", weights, value_heads, preferred_element_type=jnp.float32)
    value_f = value_heads.astype(jnp.float32)
    scaled_keys = (
        key_heads.astype(jnp.float32) * jnp.exp(block_total[None, :] - cumulative)[:, :, None]
    )
    local_state = jnp.einsum("thd,the->hde", scaled_keys, value_f)
    identity = (jnp.zeros_like(block_total), jnp.zeros_like(local_state))
    _, entering = prefix_by_axis((block_total, local_state), EP, combine_states, identity)
    scaled_queries = query_heads.astype(jnp.float32) * jnp.exp(cumulative)[:, :, None]
    carried = jnp.einsum("thd,hde->the", scaled_queries, entering)
    retained = inner + carried
    normed = (
        retained
        * lax.rsqrt(jnp.mean(retained * retained, axis=-1, keepdims=True) + epsilon)
        * head_gain[None]
    )
    gated = normed * jax.nn.silu(
        out_gate.reshape(length, local_heads, head_dim).astype(jnp.float32)
    )
    heads_out = gated.reshape(length, local_heads * head_dim).astype(jnp.bfloat16)
    summed = sent_and_summed(
        jnp.dot(heads_out, out_weight, preferred_element_type=jnp.float32).astype(jnp.bfloat16),
        "tp",
        0,
    )
    return summed.astype(jnp.bfloat16)


def pair_slots(route_ids, experts, capacity):
    flat_ids = route_ids.reshape(-1)
    member = (flat_ids[:, None] == jnp.arange(experts, dtype=jnp.int32)[None, :]).astype(jnp.int32)
    ranks = jnp.sum(jnp.cumsum(member, axis=0) * member, axis=1) - 1
    return flat_ids * capacity + ranks


def expert_half(moe_input, moe_gain, expert_gate, expert_up, expert_down, route_ids, route_weights):
    experts = lax.axis_size(EP)
    pairs = route_ids.size
    capacity = 2 * pairs // experts
    width = moe_input.shape[1]
    rows_f = moe_input.astype(jnp.float32)
    normed = (
        rows_f
        * lax.rsqrt(jnp.mean(rows_f * rows_f, axis=-1, keepdims=True) + epsilon)
        * moe_gain[None]
    ).astype(jnp.bfloat16)
    targets = pair_slots(route_ids, experts, capacity)
    table = (
        jnp.full((experts * capacity,), pairs, jnp.int32)
        .at[targets]
        .set(jnp.arange(pairs, dtype=jnp.int32))
    )
    filled = (table < pairs)[:, None]
    picked = jnp.where(
        filled, normed[jnp.minimum(table, pairs - 1) // TOP], jnp.zeros((), jnp.bfloat16)
    )
    outgoing = picked.reshape(experts, capacity, width)
    gate_slice = expert_gate[0]
    up_slice = expert_up[0]
    down_slice = expert_down[0]
    share = capacity // lax.axis_size("tp")
    piece = lax.dynamic_slice_in_dim(outgoing, lax.axis_index("tp") * share, share, 1)
    arrived = lax.all_to_all(piece, EP, split_axis=0, concat_axis=0, tiled=True)
    rows = gather_directly(arrived, "tp", 1)
    gate_part = jnp.einsum("scd,df->scf", rows, gate_slice, preferred_element_type=jnp.float32)
    up_part = jnp.einsum("scd,df->scf", rows, up_slice, preferred_element_type=jnp.float32)
    hidden = (jax.nn.silu(gate_part) * up_part).astype(jnp.bfloat16)
    partial_sum = jnp.einsum("scf,fd->scd", hidden, down_slice, preferred_element_type=jnp.float32)
    reduced = sent_and_summed(partial_sum.astype(jnp.bfloat16), "tp", 2).astype(jnp.bfloat16)
    returned = exchange_by_chip(reduced, (("ep_0", "ep_1"), "ep_2"), (0, 1), 0, 0)
    columns = returned.shape[2]
    results = returned.reshape(experts * capacity, columns)[targets].astype(jnp.float32)
    results = results.reshape(pairs // TOP, TOP, columns)
    blended = jnp.sum(results * route_weights[:, :, None], axis=1)
    return blended.astype(jnp.bfloat16)


def per_device(
    queries,
    key_rows,
    value_rows,
    out_gate,
    log_decay,
    head_gain,
    out_weight,
    moe_input,
    moe_gain,
    expert_gate,
    expert_up,
    expert_down,
    route_ids,
    route_weights,
):
    mixer_out = retention_half(
        queries, key_rows, value_rows, out_gate, log_decay, head_gain, out_weight
    )
    expert_out = expert_half(
        moe_input, moe_gain, expert_gate, expert_up, expert_down, route_ids, route_weights
    )
    return (mixer_out, expert_out)


def solution(mesh):
    split = Mesh(mesh.devices.reshape(8, 4, 2, mesh.shape["tp"]), ("ep_0", "ep_1", "ep_2", "tp"))
    return jax.shard_map(
        per_device,
        mesh=split,
        in_specs=(
            P(EP, "tp"),
            P(EP, "tp"),
            P(EP, "tp"),
            P(EP, "tp"),
            P(EP, "tp"),
            P("tp", None),
            P("tp", None),
            P(EP, None),
            P(),
            P(EP, None, "tp"),
            P(EP, None, "tp"),
            P(EP, "tp", None),
            P(EP, None),
            P(EP, None),
        ),
        out_specs=(P(EP_TP, None), P(EP, "tp")),
        check_vma=False,
    )
```

profile of v0, /device:TPU:32, one launch (start us, length us, event | category | flops | bytes accessed | tf_op | source)
XLA Modules:
  0.0 193.5 jit_solution(2085779637158893239)
XLA Ops:
  0.6 0.9 copy.86
  1.5 0.1 eq.29
  1.7 0.1 eq.25
  1.8 0.7 broadcast_multiply_fusion
  2.5 0.6 reduce-window.16
  3.1 0.2 slice_reduce_fusion
  3.3 0.1 fusion.92
  3.5 0.1 copy.85
  3.6 0.1 mul.332
  3.7 1.4 scatter_custom_fusion
  5.2 0.1 broadcast_in_dim.31
  5.3 1.2 fusion.14
  6.5 0.1 constant_dynamic-slice_fusion
  6.6 1.2 fusion.16
  7.9 3.3 %gather_fusion = bf16[512,2048]{1,0:T(8,128)(2,1)} fusion(bf16[128,2048]{1,0:T(8,128)(2,1)S(1)} %fusion.16, s32[1024]{0:T(1024)S(1)} %pad_clamp_fusion.1), kind=kCustom, calls=%fused_computation | custom fusion | bytes 4196352 | tf_op jit(solution)/shard_map/gather | solution.py:159
  11.2 3.1 %broadcast_select_fusion = bf16[64,2,2048]{2,1,0:T(2,128)(2,1)} fusion(pred[64,2]{1,0:T(8,128)(4,1)S(1)} %constant_dynamic-slice_fusion, bf16[64,8,2048]{2,1,0:T(8,128)(2,1)} %bitcast.319, s32[]{:T(128)S(6)} %select_n.241), kind=kLoop, calls=%fused_computation.25 | loop fusion | flops 262144 | bytes 1048708 | tf_op jit(solution)/shard_map/jit(_where)/select_n | solution.py:158
  14.3 11.6 %all-to-all-start.1 = ((bf16[64,2,2048]{2,1,0:T(2,128)(2,1)}), bf16[64,2,2048]{2,1,0:T(2,128)(2,1)S(1)}, u32[]{:S(2)}, u32[]{:S(2)}) async-start(bf16[64,2,2048]{2,1,0:T(2,128)(2,1)} %broadcast_select_fusion), calls=%async_computation.1 | async-start | bytes 1048576 | tf_op jit(solution)/shard_map/all_to_all | solution.py:167
  25.9 0.6 reduce-window.14
  26.6 0.2 slice_reduce_fusion.1
  26.7 0.2 reduce-window.15
  26.9 0.1 add_bitcast_fusion.1
  27.0 0.2 fusion.135
  27.2 1.8 all-gather.1
  29.0 0.6 exponential_bitcast_fusion.1
  29.5 9.7 %all-gather.2 = bf16[4,1,2]{2,1,0:T(2,128)(2,1)S(1)} all-gather(bf16[1,1,2]{2,1,0:T(2,128)(2,1)S(1)} %get-tuple-element.22), channel_id=1, replica_groups=mesh['ep_0'=8,'ep_1'=4,'ep_2'=2,'tp'=4] {'ep_1'}, dimensions={0}, use_global_device_ids=true | all-gather | bytes 20 | tf_op jit(solution)/shard_map/all_gather | solution.py:27
  39.2 0.2 slice_reduce_fusion.2
  39.4 0.7 subtract_exponential_fusion
  40.0 2.6 %all-to-all-done.1 = bf16[64,2,2048]{2,1,0:T(2,128)(2,1)S(1)} async-done(((bf16[64,2,2048]{2,1,0:T(2,128)(2,1)}), bf16[64,2,2048]{2,1,0:T(2,128)(2,1)S(1)}, u32[]{:S(2)}, u32[]{:S(2)}) %all-to-all-start.1) | async-done | bytes 524320 | tf_op jit(solution)/shard_map/all_to_all | solution.py:167
  42.6 2.7 %broadcast_in_dim.35 = bf16[4,64,2,2048]{3,2,1,0:T(2,128)(2,1)} broadcast(bf16[64,2,2048]{2,1,0:T(2,128)(2,1)S(1)} %all-to-all-done.1), dimensions={1,2,3} | broadcast | bytes 2621440 | tf_op jit(solution)/shard_map/broadcast_in_dim | solution.py:75
  45.2 4.6 %all-to-all-start.2 = ((bf16[4,64,2,2048]{3,2,1,0:T(2,128)(2,1)}), bf16[4,64,2,2048]{3,2,1,0:T(2,128)(2,1)S(1)}, u32[]{:S(2)}, u32[]{:S(2)}) async-start(bf16[4,64,2,2048]{3,2,1,0:T(2,128)(2,1)} %broadcast_in_dim.35), calls=%async_computation.2 | async-start | bytes 4194304 | tf_op jit(solution)/shard_map/all_to_all | solution.py:75
  49.8 0.6 exponential_bitcast_fusion.3
  50.4 14.7 %all-gather.3 = bf16[8,1,2]{2,1,0:T(2,128)(2,1)S(1)} all-gather(bf16[1,1,2]{2,1,0:T(2,128)(2,1)S(1)} %get-tuple-element.12), channel_id=1, replica_groups=mesh['ep_0'=8,'ep_1'=4,'ep_2'=2,'tp'=4] {'ep_0'}, dimensions={0}, use_global_device_ids=true | all-gather | bytes 36 | tf_op jit(solution)/shard_map/all_gather | solution.py:27
  65.1 0.8 copy.95
  65.9 0.1 copy.84
  66.0 1.2 convolution_convert_fusion.1
  67.2 1.9 all-gather
  69.1 0.7 fusion.58
  69.8 12.7 %all_gather.31 = bf16[4,2,128,128]{3,2,1,0:T(8,128)(2,1)S(1)} all-gather(bf16[1,2,128,128]{3,2,1,0:T(8,128)(2,1)S(1)} %fusion.58), channel_id=1, replica_groups=mesh['ep_0'=8,'ep_1'=4,'ep_2'=2,'tp'=4] {'ep_1'}, dimensions={0}, use_global_device_ids=true | all-gather | bytes 327680 | tf_op jit(solution)/shard_map/all_gather | solution.py:27
  82.5 1.2 exponential_bitcast_fusion.4
  83.7 0.6 fusion.155
  84.4 1.4 fusion.52
  85.8 3.8 %copy.89 = bf16[64,4,2,2048]{3,2,1,0:T(2,128)(2,1)} copy(bf16[64,4,2,2048]{3,2,0,1:T(2,128)(2,1)S(1)} %bitcast.316) | data formatting | bytes 4194304 | tf_op jit(solution)/shard_map/transpose | solution.py:56
  89.6 2.7 %reshape.356 = bf16[64,8,2048]{2,1,0:T(8,128)(2,1)S(1)} reshape(bf16[64,4,2,2048]{3,2,1,0:T(2,128)(2,1)} %copy.89) | data formatting | bytes 4194304 | tf_op jit(solution)/shard_map/reshape | solution.py:56
  92.4 5.6 %fusion.4 = f32[64,8,896]{2,1,0:T(8,128)} fusion(bf16[64,8,2048]{2,1,0:T(8,128)(2,1)S(1)} %reshape.356, bf16[1,2048,896]{2,1,0:T(8,128)(2,1)} %param.23), kind=kOutput, calls=%fused_computation.7 | convolution fusion | flops 1879048192 | bytes 7602176 | tf_op jit(solution)/shard_map/scd,df->scf/dot_general | solution.py:169
  98.0 9.5 %fusion.6 = bf16[64,8,2048]{2,1,0:T(8,128)(2,1)} fusion(bf16[1,896,2048]{2,1,0:T(8,128)(2,1)} %param.25, f32[64,8,896]{2,1,0:T(8,128)} %fusion.4, bf16[64,8,2048]{2,1,0:T(8,128)(2,1)S(1)} %reshape.356, bf16[1,2048,896]{2,1,0:T(8,128)(2,1)} %param.24), kind=kOutput, calls=%fused_computation.9 | convolution fusion | flops 3761897472 | bytes 13369344 | tf_op jit(solution)/shard_map/scf,fd->scd/dot_general | solution.py:172
  107.5 3.1 %copy.128 = bf16[64,8,4,512]{3,1,0,2:T(8,128)(2,1)} copy(bf16[64,8,4,512]{3,1,2,0:T(8,128)(2,1)} %bitcast.320) | data formatting | bytes 4194304 | tf_op jit(solution)/shard_map/reshape | solution.py:44
  110.6 4.9 %all-to-all-start.3 = ((bf16[4,64,8,512]{3,2,1,0:T(8,128)(2,1)}), bf16[4,64,8,512]{3,2,1,0:T(8,128)(2,1)S(1)}, u32[]{:S(2)}, u32[]{:S(2)}) async-start(bf16[4,64,8,512]{3,2,1,0:T(8,128)(2,1)} %bitcast.317), calls=%async_computation.3 | async-start | bytes 4194304 | tf_op jit(solution)/shard_map/all_to_all | solution.py:49
  115.5 0.6 iota_compare_fusion
  116.2 26.6 %all_gather.32 = bf16[8,2,128,128]{3,2,1,0:T(8,128)(2,1)} all-gather(bf16[1,2,128,128]{3,2,1,0:T(8,128)(2,1)} %fusion.52), channel_id=1, replica_groups=mesh['ep_0'=8,'ep_1'=4,'ep_2'=2,'tp'=4] {'ep_0'}, dimensions={0}, use_global_device_ids=true | all-gather | bytes 589824 | tf_op jit(solution)/shard_map/all_gather | solution.py:27
  142.8 2.2 %convolution_bitcast_fusion.1 = f32[256,2,128]{0,2,1:T(8,128)} fusion(bf16[256,2,128]{0,2,1:T(8,128)(2,1)} %bitcast.325, f32[2,256]{1,0:T(2,128)} %bitcast.333, pred[256,256]{1,0:T(8,128)(4,1)} %iota_compare_fusion, bf16[256,256]{1,0:T(8,128)(2,1)} %param.16, bf16[256,256]{1,0:T(8,128)(2,1)} %param.14), kind=kOutput, calls=%fused_computation.20 | convolution fusion | flops 67764224 | bytes 722944 | tf_op jit(solution)/shard_map/hts,shd->thd/dot_general | solution.py:105
  144.9 2.0 %multiply_reduce_fusion.1 = (f32[256,2]{0,1:T(2,128)S(1)}, f32[256,2,128]{0,2,1:T(8,128)S(1)}) fusion(f32[256,2,128]{0,2,1:T(8,128)} %convolution_bitcast_fusion.1, f32[256,2]{0,1:T(2,128)} %get-tuple-element.15, bf16[8,2,128,128]{3,2,1,0:T(8,128)(2,1)} %all_gather.32, f32[2]{0:T(128)S(1)} %copy-done.4, f32[2]{0:T(128)S(1)} %get-tuple-element.21, ...), kind=kOutput, calls=%fused_computation.31 | convolution fusion | flops 18972160 | bytes 1577102 | tf_op jit(solution)/shard_map/thd,hde->the/dot_general | solution.py:114
  147.0 0.1 multiply_convert_fusion.1
  147.1 1.4 convolution_convert_fusion
  148.6 4.7 %all-to-all-start = ((bf16[4,64,2048]{2,1,0:T(8,128)(2,1)}), bf16[4,64,2048]{2,1,0:T(8,128)(2,1)}, u32[]{:S(2)}, u32[]{:S(2)}) async-start(bf16[4,64,2048]{2,1,0:T(8,128)(2,1)} %bitcast.318), calls=%async_computation | async-start | bytes 2097152 | tf_op jit(solution)/shard_map/all_to_all | solution.py:49
  153.3 1.3 reduce_sum.64
  154.5 9.7 %all-to-all-done = bf16[4,64,2048]{2,1,0:T(8,128)(2,1)} async-done(((bf16[4,64,2048]{2,1,0:T(8,128)(2,1)}), bf16[4,64,2048]{2,1,0:T(8,128)(2,1)}, u32[]{:S(2)}, u32[]{:S(2)}) %all-to-all-start) | async-done | bytes 1048608 | tf_op jit(solution)/shard_map/all_to_all | solution.py:49
  164.3 9.0 %all-to-all-start.4 = ((bf16[32,2,1,8,512]{4,3,1,2,0:T(8,128)(2,1)}), bf16[32,2,1,8,512]{4,3,1,2,0:T(8,128)(2,1)S(1)}, u32[]{:S(2)}, u32[]{:S(2)}) async-start(bf16[32,2,1,8,512]{4,3,1,2,0:T(8,128)(2,1)} %bitcast.321), calls=%async_computation.4 | async-start | bytes 1048576 | tf_op jit(solution)/shard_map/all_to_all | solution.py:63
  173.3 0.1 copy.93
  173.4 2.2 %reduce_sum.61 = bf16[64,2048]{1,0:T(8,128)(2,1)} reduce(bf16[4,64,2048]{2,1,0:T(8,128)(2,1)} %all-to-all-done, bf16[]{:T(256)} %constant.84.clone.1), dimensions={0}, to_apply=%region_3.4 | reduce | flops 393216 | bytes 1310722 | tf_op jit(solution)/shard_map/reduce_sum | solution.py:50
  175.6 10.8 %all-to-all-done.4 = bf16[32,2,1,8,512]{4,3,1,2,0:T(8,128)(2,1)S(1)} async-done(((bf16[32,2,1,8,512]{4,3,1,2,0:T(8,128)(2,1)}), bf16[32,2,1,8,512]{4,3,1,2,0:T(8,128)(2,1)S(1)}, u32[]{:S(2)}, u32[]{:S(2)}) %all-to-all-start.4) | async-done | bytes 524320 | tf_op jit(solution)/shard_map/all_to_all | solution.py:63
  186.4 4.2 %all_to_all.30 = bf16[32,2,1,8,512]{4,3,0,2,1:T(8,128)(2,1)S(1)} all-to-all(bf16[32,2,1,8,512]{4,3,0,2,1:T(8,128)(2,1)S(1)} %copy.91), channel_id=1, replica_groups=mesh['ep_0'=8,'ep_1'=4,'ep_2'=2,'tp'=4] {'ep_2'}, dimensions={1} | all-to-all | bytes 1048576 | tf_op jit(solution)/shard_map/all_to_all | solution.py:63
  190.6 1.2 gather_fusion.1
  191.8 0.3 reshape.375
  192.1 1.4 multiply_reduce_fusion
  (45 shorter events, 0.3 us)
Async XLA Ops:
  0.6 146.5 %copy-start = (bf16[256,2048]{1,0:T(8,128)(2,1)S(1)}, bf16[256,2048]{1,0:T(8,128)(2,1)}, u32[]{:S(2)}) copy-start(bf16[256,2048]{1,0:T(8,128)(2,1)} %param.20) | copy-start | bytes 3145732
  11.2 14.7 %copy-start.9 = (f32[256,2]{0,1:T(2,128)S(1)}, f32[256,2]{0,1:T(2,128)}, u32[]{:S(2)}) copy-start(f32[256,2]{0,1:T(2,128)} %param.18) | copy-start | bytes 6148
  14.3 28.3 %all-to-all-start.1 = ((bf16[64,2,2048]{2,1,0:T(2,128)(2,1)}), bf16[64,2,2048]{2,1,0:T(2,128)(2,1)S(1)}, u32[]{:S(2)}, u32[]{:S(2)}) async-start(bf16[64,2,2048]{2,1,0:T(2,128)(2,1)} %broadcast_select_fusion), calls=%async_computation.1 | async-start | bytes 1048576 | tf_op jit(solution)/shard_map/all_to_all | solution.py:167
  27.0 18.3 %copy-start.10 = (f32[1,2,2,128]{3,1,2,0:T(2,128)}, f32[1,2,2,128]{3,1,2,0:T(2,128)S(1)}, u32[]{:S(2)}) copy-start(f32[1,2,2,128]{3,1,2,0:T(2,128)S(1)} %copy.129) | copy-start | bytes 6148
  45.2 19.9 %copy-start.3 = (bf16[256,256]{1,0:T(8,128)(2,1)S(1)}, bf16[256,256]{1,0:T(8,128)(2,1)}, u32[]{:S(2)}) copy-start(bf16[256,256]{1,0:T(8,128)(2,1)} %param.15) | copy-start | bytes 393220
  45.2 20.6 %copy-start.2 = (bf16[256,256]{1,0:T(8,128)(2,1)S(1)}, bf16[256,256]{1,0:T(8,128)(2,1)}, u32[]{:S(2)}) copy-start(bf16[256,256]{1,0:T(8,128)(2,1)} %param.17) | copy-start | bytes 393220
  45.2 40.6 %all-to-all-start.2 = ((bf16[4,64,2,2048]{3,2,1,0:T(2,128)(2,1)}), bf16[4,64,2,2048]{3,2,1,0:T(2,128)(2,1)S(1)}, u32[]{:S(2)}, u32[]{:S(2)}) async-start(bf16[4,64,2,2048]{3,2,1,0:T(2,128)(2,1)} %broadcast_in_dim.35), calls=%async_computation.2 | async-start | bytes 4194304 | tf_op jit(solution)/shard_map/all_to_all | solution.py:75
  82.5 1.8 copy-start.1
  83.7 0.6 copy-start.6
  83.7 0.6 copy-start.7
  83.7 0.6 copy-start.8
  110.6 34.3 %copy-start.4 = (f32[2]{0:T(128)S(1)}, f32[2]{0:T(128)}, u32[]{:S(2)}) copy-start(f32[2]{0:T(128)} %get-tuple-element.23) | copy-start | bytes 28
  110.6 34.3 %copy-start.5 = (f32[2]{0:T(128)S(1)}, f32[2]{0:T(128)}, u32[]{:S(2)}) copy-start(f32[2]{0:T(128)} %get-tuple-element.13) | copy-start | bytes 28
  110.6 38.0 %all-to-all-start.3 = ((bf16[4,64,8,512]{3,2,1,0:T(8,128)(2,1)}), bf16[4,64,8,512]{3,2,1,0:T(8,128)(2,1)S(1)}, u32[]{:S(2)}, u32[]{:S(2)}) async-start(bf16[4,64,8,512]{3,2,1,0:T(8,128)(2,1)} %bitcast.317), calls=%async_computation.3 | async-start | bytes 4194304 | tf_op jit(solution)/shard_map/all_to_all | solution.py:49
  144.9 2.0 %copy-start.11 = (f32[2,128]{1,0:T(2,128)S(1)}, f32[2,128]{1,0:T(2,128)}, u32[]{:S(2)}) copy-start(f32[2,128]{1,0:T(2,128)} %param.19) | copy-start | bytes 3076
  148.6 15.7 %all-to-all-start = ((bf16[4,64,2048]{2,1,0:T(8,128)(2,1)}), bf16[4,64,2048]{2,1,0:T(8,128)(2,1)}, u32[]{:S(2)}, u32[]{:S(2)}) async-start(bf16[4,64,2048]{2,1,0:T(8,128)(2,1)} %bitcast.318), calls=%async_computation | async-start | bytes 2097152 | tf_op jit(solution)/shard_map/all_to_all | solution.py:49
  153.3 20.0 %copy-start.12 = (f32[128,2]{0,1:T(2,128)S(1)}, f32[128,2]{0,1:T(2,128)}, u32[]{:S(2)}) copy-start(f32[128,2]{0,1:T(2,128)} %param.27) | copy-start | bytes 3076
  164.3 22.1 %all-to-all-start.4 = ((bf16[32,2,1,8,512]{4,3,1,2,0:T(8,128)(2,1)}), bf16[32,2,1,8,512]{4,3,1,2,0:T(8,128)(2,1)S(1)}, u32[]{:S(2)}, u32[]{:S(2)}) async-start(bf16[32,2,1,8,512]{4,3,1,2,0:T(8,128)(2,1)} %bitcast.321), calls=%async_computation.4 | async-start | bytes 1048576 | tf_op jit(solution)/shard_map/all_to_all | solution.py:63
where the time goes:
time: 196 us; the launch traced here: 194 us
  blocking collectives  71.5 us (36%)
  starting transfers between devices  34.9 us (18%)
  local copies, waits for them, and re-layouts  23.2 us (12%)
  waiting for transfers between devices  23.1 us (12%)
  matrix products  21.9 us (11%)
  other arithmetic  18.1 us (9%)
    all_gather x6, blocking collectives, prefix_by_axis(): lax.all_gather(part.astype(kind), axis)  67.4 us
    all_to_all x1, starting transfers between devices, expert_half(): arrived = lax.all_to_all(piece, EP, split_axis=0, concat_axis=0, tiled=True)  11.6 us
    all_to_all x1, waiting for transfers between devices, exchange_in_order(): lax.all_to_all(parts, axes[k], split_axis=k, concat_axis=k, tiled=True)  10.8 us
    all_to_all x2, waiting for transfers between devices, sent_and_summed(): parts = lax.all_to_all(in_blocks(x, dim, size), axis, 0, 0, tiled=True)  9.74 us
    all_to_all x2, starting transfers between devices, sent_and_summed(): parts = lax.all_to_all(in_blocks(x, dim, size), axis, 0, 0, tiled=True)  9.65 us
    dot_general x1, matrix products, expert_half(): jnp.einsum('scf,fd->scd', hidden, down_slice, preferred_element_type=jnp....  9.47 us
    all_to_all x1, starting transfers between devices, exchange_in_order(): lax.all_to_all(parts, axes[k], split_axis=k, concat_axis=k, tiled=True)  9.03 us
    dot_general x1, matrix products, expert_half(): jnp.einsum('scd,df->scf', rows, gate_slice, preferred_element_type=jnp.fl...  5.62 us
  transfers between devices with their start and end apart: 5, of which 3 were waited for; matrix products, arithmetic and copies ran while one was open for 10% of the time, Pallas kernels for 0%

commit v1 on v0

v1 whole, which is shorter than its diff:
```python
import functools

import jax
import jax.numpy as jnp
from jax import lax
from jax.experimental import pallas as pl
from jax.experimental.pallas import tpu as pltpu
from jax.sharding import Mesh
from jax.sharding import PartitionSpec as P

EP = ("z", "x", "c")
ZX = ("z", "x")
F32 = jnp.float32
BF16 = jnp.bfloat16
epsilon = 1e-06


def iota(shape, dim):
    return lax.broadcasted_iota(jnp.int32, shape, dim)


def dot(a, b):
    return jnp.dot(a, b, preferred_element_type=F32)


def dot_t(a, b):
    return lax.dot_general(a, b, (((0,), (0,)), ((), ())), preferred_element_type=F32)


def three_parts(x):
    a = x.astype(BF16)
    rest = x - a.astype(F32)
    b = rest.astype(BF16)
    return a, b, (rest - b.astype(F32)).astype(BF16)


def call(body, outs, *args, **kw):
    return pl.pallas_call(
        body,
        out_shape=outs,
        in_specs=[pl.BlockSpec(memory_space=pltpu.VMEM)] * len(args),
        out_specs=jax.tree.map(lambda _: pl.BlockSpec(memory_space=pltpu.VMEM), outs),
        **kw,
    )(*args)


def array(shape, dtype):
    return jax.ShapeDtypeStruct(shape, dtype)


def slot_members(ids_ref, half, rows, capacity):
    tokens = ids_ref.shape[0]
    eye = (iota((tokens, tokens), 0) == iota((tokens, tokens), 1)).astype(BF16)
    ids = dot_t(ids_ref[...].astype(F32).astype(BF16), eye).astype(jnp.int32)
    core = lax.axis_index("c")
    slot = iota((rows, 1), 0)
    other = core + half - 2 * core * half
    expert = (slot // capacity) * 2 + other
    first, second = ids[0:1] == expert, ids[1:2] == expert
    member = jnp.where(first | second, 1.0, 0.0)
    earlier = (iota((tokens, tokens), 0) < iota((tokens, tokens), 1)).astype(BF16)
    rank = dot(member.astype(BF16), earlier).astype(jnp.int32)
    here = rank == (slot % capacity)
    return first & here, second & here


def dispatch_kernel(capacity, ids_ref, x_ref, gain_ref, keep_ref, send_ref):
    part = keep_ref.shape[1]
    x = x_ref[...].astype(F32)
    scale = lax.rsqrt(jnp.mean(x * x, axis=-1, keepdims=True) + epsilon)
    cols = pl.ds(pl.multiple_of(lax.axis_index("tp") * part, part), part)
    normed = (x_ref[:, cols].astype(F32) * scale * gain_ref[:, cols]).astype(BF16)
    for half, ref in enumerate((keep_ref, send_ref)):
        first, second = slot_members(ids_ref, half, ref.shape[0], capacity)
        hot = jnp.where(first | second, 1.0, 0.0).astype(BF16)
        ref[...] = dot(hot, normed).astype(BF16)


def blend_weights_kernel(capacity, ids_ref, w_ref, out_ref):
    tokens = ids_ref.shape[0]
    eye = (iota((tokens, tokens), 0) == iota((tokens, tokens), 1)).astype(BF16)
    w = sum(dot_t(t, eye) for t in three_parts(w_ref[...]))
    for half in range(2):
        first, second = slot_members(ids_ref, half, out_ref.shape[2], capacity)
        blend = jnp.where(first, w[0:1], 0.0) + jnp.where(second, w[1:2], 0.0)
        hi = blend.astype(BF16)
        out_ref[half, 0] = hi
        out_ref[half, 1] = (blend - hi.astype(F32)).astype(BF16)


def blend_kernel(w_ref, keep_ref, sent_ref, out_ref):
    total = 0.0
    for half, ref in enumerate((keep_ref, sent_ref)):
        rows = ref[...]
        total = total + dot_t(w_ref[half, 0], rows) + dot_t(w_ref[half, 1], rows)
    out_ref[...] = total.astype(BF16)


def ffn_kernel(own, left, right, far_a, far_b, gate, up, down, to2a, to2b, to1a, to1b, tom1a, tom1b, mine):
    me = lax.axis_index("tp")
    part = own.shape[1]
    half = far_a.shape[0]
    hidden = gate.shape[1]
    far = jnp.concatenate([far_a[...], far_b[...]], axis=0)

    def span(k):
        return pl.ds(pl.multiple_of(lax.rem(me + k, 4) * part, part), part)

    pieces = ((0, own[...]), (3, left[...]), (1, right[...]), (2, far))
    hid = []
    for lo in range(0, hidden, 256):
        hi = min(hidden, lo + 256)
        g = sum(dot(x, gate[span(k), lo:hi]) for k, x in pieces)
        u = sum(dot(x, up[span(k), lo:hi]) for k, x in pieces)
        hid.append((g * jax.nn.sigmoid(g) * u).astype(BF16))
    hid = jnp.concatenate(hid, axis=1)
    for k, (top, low) in ((2, (to2a, to2b)), (1, (to1a, to1b)), (3, (tom1a, tom1b)), (0, (None, None))):
        out = dot(hid, down[:, span(k)]).astype(BF16)
        if k == 0:
            mine[...] = out
        else:
            top[...] = out[:half]
            low[...] = out[half:]


def levels_of(decay):
    n = decay.shape[0]
    parts = jnp.concatenate(three_parts(decay), axis=1)
    upto = (iota((n, n), 0) >= iota((n, n), 1)).astype(BF16)
    before = (iota((n, n), 0) <= iota((n, n), 1)).astype(BF16)
    col = dot(upto, parts)
    row = dot_t(parts, before)
    return col[:, 0:2] + col[:, 2:4] + col[:, 4:6], row[0:2] + row[2:4] + row[4:6]


def inner_kernel(q_ref, k_ref, v_ref, decay_ref, inner_ref, kept_ref, kept_total_ref, send_ref):
    core = lax.axis_index("c")
    n = q_ref.shape[0]
    col, row = levels_of(decay_ref[...])
    causal = iota((n, n), 0) >= iota((n, n), 1)
    states, totals = [], []
    for h in range(2):
        cols = slice(h * 128, h * 128 + 128)
        q, k, v = q_ref[:, cols], k_ref[:, cols], v_ref[:, cols]
        scores = lax.dot_general(q, k, (((1,), (1,)), ((), ())), preferred_element_type=F32) * 128 ** (-0.5)
        spread = jnp.where(causal, col[:, h : h + 1] - row[h : h + 1], -jnp.inf)
        inner_ref[:, cols] = dot((scores * jnp.exp(spread)).astype(BF16), v)
        total = col[n - 1 : n, h : h + 1]
        scaled = (k.astype(F32) * jnp.exp(total - col[:, h : h + 1])).astype(BF16)
        states.append(dot_t(scaled, v))
        totals.append(total)
    first = core == 0
    kept_ref[...] = jnp.where(first, states[0], states[1])
    kept_total_ref[...] = jnp.broadcast_to(jnp.where(first, totals[0], totals[1]), kept_total_ref.shape)
    send_ref[0:128] = jnp.where(first, states[1], states[0]).astype(BF16)
    send_ref[128:144] = rows_of_total(jnp.where(first, totals[1], totals[0]), 16)


def rows_of_total(total, rows):
    a, b, c = (jnp.broadcast_to(t.astype(F32), (rows, 128)) for t in three_parts(total))
    r = iota((rows, 128), 0)
    return jnp.where(r == 0, a, jnp.where(r == 1, b, jnp.where(r == 2, c, 0.0))).astype(BF16)


def pair_of(kept_ref, kept_total_ref, got_ref):
    first = lax.axis_index("c") == 0
    mine, mine_total = kept_ref[...], kept_total_ref[0:1]
    theirs = got_ref[0:128].astype(F32)
    rows = got_ref[128:144].astype(F32)
    theirs_total = rows[0:1] + rows[1:2] + rows[2:3]
    return (
        (jnp.where(first, mine, theirs), jnp.where(first, mine_total, theirs_total)),
        (jnp.where(first, theirs, mine), jnp.where(first, theirs_total, mine_total)),
    )


def pair_kernel(kept_ref, kept_total_ref, got_ref, out_ref):
    (s0, t0), (s1, t1) = pair_of(kept_ref, kept_total_ref, got_ref)
    state = (jnp.exp(t1) * s0 + s1).astype(BF16)
    total = rows_of_total(t0 + t1, 4)
    for j in range(out_ref.shape[0]):
        out_ref[j, 0:4] = state[4 * j : 4 * j + 4]
        out_ref[j, 4:8] = total


def scan_kernel(in_ref, out_ref):
    state = jnp.zeros((4, 128), F32)
    for j in range(in_ref.shape[0]):
        hi = state.astype(BF16)
        out_ref[j, 0:4] = hi
        out_ref[j, 4:8] = (state - hi.astype(F32)).astype(BF16)
        block = in_ref[j].astype(F32)
        state = jnp.exp(block[4:5] + block[5:6] + block[6:7]) * state + block[0:4]


def entering_kernel(back_ref, kept_ref, kept_total_ref, got_ref, keep_ref, send_ref):
    (s0, t0), _ = pair_of(kept_ref, kept_total_ref, got_ref)
    rows = []
    for j in range(back_ref.shape[0]):
        block = back_ref[j].astype(F32)
        rows.append(block[0:4] + block[4:8])
    before = jnp.concatenate(rows, axis=0)
    after = jnp.exp(t0) * before + s0
    first = lax.axis_index("c") == 0
    keep_ref[...] = jnp.where(first, before, after).astype(BF16)
    send_ref[...] = jnp.where(first, after, before).astype(BF16)


def mixer_kernel(inner_ref, q_ref, decay_ref, keep_ref, got_ref, gain_ref, gate_ref, weight_ref, out_ref):
    first = lax.axis_index("c") == 0
    col, _ = levels_of(decay_ref[...])
    keep, got = keep_ref[...], got_ref[...]
    entering = (jnp.where(first, keep, got), jnp.where(first, got, keep))
    heads = []
    for h in range(2):
        cols = slice(h * 128, h * 128 + 128)
        carried = jnp.exp(col[:, h : h + 1]) * dot(q_ref[:, cols], entering[h])
        kept = inner_ref[:, cols] + carried
        normed = kept * lax.rsqrt(jnp.mean(kept * kept, axis=-1, keepdims=True) + epsilon) * gain_ref[h : h + 1]
        gate = gate_ref[:, cols].astype(F32)
        heads.append((normed * (gate * jax.nn.sigmoid(gate))).astype(BF16))
    heads = jnp.concatenate(heads, axis=1)
    for lo in range(0, out_ref.shape[1], 512):
        out_ref[:, lo : lo + 512] = dot(heads, weight_ref[:, lo : lo + 512]).astype(BF16)


def shifted(x, axis, by):
    n = lax.axis_size(axis)
    return lax.ppermute(x, axis, [(i, (i + by) % n) for i in range(n)])


def across_chips(x):
    n = lax.axis_size(ZX)
    out = lax.all_to_all(x.reshape(n, -1, x.shape[-1]), ZX, split_axis=0, concat_axis=0, tiled=True)
    return out.reshape(x.shape)


def gathered(x):
    half = x.shape[0] // 2
    left, right = shifted(x, "tp", 1), shifted(x, "tp", -1)
    far_a, far_b = shifted(left[:half], "tp", 1), shifted(right[half:], "tp", -1)
    return x, left, right, far_a, far_b


def reduced(to2a, to2b, to1a, to1b, tom1a, tom1b, mine):
    def add(*parts):
        return sum(p.astype(F32) for p in parts).astype(BF16)

    half = to2a.shape[0]
    a, b = shifted(to2a, "tp", 1), shifted(to2b, "tp", -1)
    l_low, r_top = shifted(to1b, "tp", 1), shifted(tom1a, "tp", -1)
    l_top, r_low = shifted(add(to1a, a), "tp", 1), shifted(add(tom1b, b), "tp", -1)
    return jnp.concatenate([add(mine[:half], l_top, r_top), add(mine[half:], l_low, r_low)], axis=0)


def per_device(
    queries,
    key_rows,
    value_rows,
    out_gate,
    log_decay,
    head_gain,
    out_weight,
    moe_input,
    moe_gain,
    expert_gate,
    expert_up,
    expert_down,
    route_ids,
    route_weights,
):
    tokens, width = moe_input.shape
    part = width // lax.axis_size("tp")
    chips = lax.axis_size(ZX)
    capacity = 2 * route_ids.size // lax.axis_size(EP)
    rows = chips * capacity
    half = rows // 2
    keep, send = call(
        functools.partial(dispatch_kernel, capacity),
        [array((rows, part), BF16)] * 2,
        route_ids,
        moe_input,
        moe_gain.reshape(1, -1),
        name="dispatch",
    )
    got = shifted(send, "c", 1)
    arrived = across_chips(keep), across_chips(got)

    inner, kept, kept_total, state_send = call(
        inner_kernel,
        [array(queries.shape, F32), array((128, 128), F32), array((8, 128), F32), array((144, 128), BF16)],
        queries,
        key_rows,
        value_rows,
        log_decay,
        name="inner",
    )
    state_got = shifted(state_send, "c", 1)
    pair = call(pair_kernel, array((chips, 8, 128), BF16), kept, kept_total, state_got, name="pair")
    scanned = call(scan_kernel, array((chips, 8, 128), BF16), across_chips(pair.reshape(-1, 128)).reshape(pair.shape), name="scan")
    back = across_chips(scanned.reshape(-1, 128)).reshape(pair.shape)
    ent_keep, ent_send = call(
        entering_kernel, [array((128, 128), BF16)] * 2, back, kept, kept_total, state_got, name="entering"
    )
    ent_got = shifted(ent_send, "c", 1)
    partial = call(
        mixer_kernel,
        array((queries.shape[0], out_weight.shape[1]), BF16),
        inner,
        queries,
        log_decay,
        ent_keep,
        ent_got,
        head_gain,
        out_gate,
        out_weight,
        name="mixer",
    )

    results = []
    for chunk in arrived:
        outs = call(
            ffn_kernel,
            [array((half, part), BF16)] * 6 + [array((rows, part), BF16)],
            *gathered(chunk),
            expert_gate[0],
            expert_up[0],
            expert_down[0],
            name="ffn",
        )
        results.append(across_chips(reduced(*outs)))
    weights = call(
        functools.partial(blend_weights_kernel, capacity),
        array((2, 2, rows, tokens), BF16),
        route_ids,
        route_weights,
        name="blend_weights",
    )
    expert_out = call(
        blend_kernel, array((tokens, part), BF16), weights, results[0], shifted(results[1], "c", 1), name="blend"
    )
    pieces = lax.all_to_all(partial.reshape(4, -1, partial.shape[1]), "tp", 0, 0, tiled=True)
    mixer_out = jnp.sum(pieces.astype(F32), axis=0).astype(BF16)
    return mixer_out, expert_out


def solution(mesh):
    split = Mesh(mesh.devices.reshape(8, 4, 2, mesh.shape["tp"]), ("z", "x", "c", "tp"))
    return jax.shard_map(
        per_device,
        mesh=split,
        in_specs=(
            P(EP, "tp"),
            P(EP, "tp"),
            P(EP, "tp"),
            P(EP, "tp"),
            P(EP, "tp"),
            P("tp", None),
            P("tp", None),
            P(EP, None),
            P(),
            P(EP, None, "tp"),
            P(EP, None, "tp"),
            P(EP, "tp", None),
            P(EP, None),
            P(EP, None),
        ),
        out_specs=(P((*EP, "tp"), None), P(EP, "tp")),
        check_vma=False,
    )
```

time: 196 us -> 177 us (0.903)
  blocking collectives: 71.5 us -> 23.4 us
  Pallas kernels: 0 us -> 34.9 us
  starting transfers between devices: 34.9 us -> 61.6 us
  matrix products: 21.9 us -> 0 us
  waiting for transfers between devices: 23.1 us -> 41.9 us
  local copies, waits for them, and re-layouts: 23.2 us -> 8.97 us
  other arithmetic: 18.1 us -> 4.57 us
    all_gather x6 -> x0, blocking collectives: 67.4 us -> none  [prefix_by_axis(): lax.all_gather(part.astype(kind), axis)]
    pallas_call x0 -> x10, Pallas kernels: none -> 34.9 us  [call(): pl.pallas_call(body, out_shape=outs, in_specs=[pl.BlockSpec(memory_space=...]
    ppermute x0 -> x24, starting transfers between devices: none -> 27.2 us  [shifted(): return lax.ppermute(x, axis, [(i, (i + by) % n) for i in range(n)])]
    dot_general x6 -> x0, matrix products: 21.9 us -> none  [the longest x1 9.47 us: expert_half(): jnp.einsum('scf,fd->scd', hidden, down_slice, preferred_element_type=jnp....]
    all_to_all x1, blocking collectives: 4.15 us -> 23.4 us  [across_chips(): lax.all_to_all(x.reshape(n, -1, x.shape[-1]), ZX, split_axis=0, concat_ax...]
    ppermute x0 -> x24, waiting for transfers between devices: none -> 18.4 us  [shifted(): return lax.ppermute(x, axis, [(i, (i + by) % n) for i in range(n)])]
    unnamed x29 -> x51, local copies, waits for them, and re-layouts: 1.05 us -> 8.93 us
    reshape x4 -> x0, local copies, waits for them, and re-layouts: 6.66 us -> none  [the longest x1 3.14 us: in_blocks(): return jnp.moveaxis(x.reshape(*before, size, -1, *after), dim, 0)]
  transfers between devices with their start and end apart: 5 -> 30, of which waited for: 3 -> 10; matrix products, arithmetic and copies ran while one was open for 10% -> 4% of each run, Pallas kernels for 0% -> 17%
where the time goes in v1:
time: 177 us; the launch traced here: 176 us
  starting transfers between devices  61.6 us (35%)
  waiting for transfers between devices  41.9 us (24%)
  Pallas kernels  34.9 us (20%)
  blocking collectives  23.4 us (13%)
  local copies, waits for them, and re-layouts  8.97 us (5%)
  other arithmetic  4.57 us (3%)
    pallas_call x10, Pallas kernels, call(): pl.pallas_call(body, out_shape=outs, in_specs=[pl.BlockSpec(memory_space=...  34.9 us
    all_to_all x5, starting transfers between devices, across_chips(): lax.all_to_all(x.reshape(n, -1, x.shape[-1]), ZX, split_axis=0, concat_ax...  30.9 us
    ppermute x24, starting transfers between devices, shifted(): return lax.ppermute(x, axis, [(i, (i + by) % n) for i in range(n)])  27.2 us
    all_to_all x5, waiting for transfers between devices, across_chips(): lax.all_to_all(x.reshape(n, -1, x.shape[-1]), ZX, split_axis=0, concat_ax...  23.5 us
    all_to_all x1, blocking collectives, across_chips(): lax.all_to_all(x.reshape(n, -1, x.shape[-1]), ZX, split_axis=0, concat_ax...  23.4 us
    ppermute x24, waiting for transfers between devices, shifted(): return lax.ppermute(x, axis, [(i, (i + by) % n) for i in range(n)])  18.4 us
    unnamed x51, local copies, waits for them, and re-layouts  8.93 us
  transfers between devices with their start and end apart: 30, of which 10 were waited for; matrix products, arithmetic and copies ran while one was open for 4% of the time, Pallas kernels for 17%

profile of v1, /device:TPU:32, one launch (start us, length us, event | category | flops | bytes accessed | tf_op | source)
XLA Modules:
  0.0 176.3 jit_solution(2415557286785119597)
XLA Ops:
  0.6 1.4 copy.18.ids_ref
  2.0 2.6 %dispatch.1 = (bf16[256,512]{1,0:T(8,128)(2,1)}, bf16[256,512]{1,0:T(8,128)(2,1)}) custom-call(s32[128,2]{1,0:T(8,128)} %copy.18.ids_ref, bf16[128,2048]{1,0:T(8,128)(2,1)} %x_ref.1, f32[1,2048]{1,0:T(1,128)} %bitcast.32), custom_call_target="tpu_custom_call" | custom-call | tf_op jit(solution)/shard_map/dispatch/pallas_call | solution.py:38
  4.6 1.7 collective-permute-done.12
  6.4 23.4 %all_to_all.35 = bf16[32,8,512]{2,1,0:T(8,128)(2,1)S(1)} all-to-all(bf16[32,8,512]{2,1,0:T(8,128)(2,1)S(1)} %bitcast.31), channel_id=1, replica_groups=mesh['z'=8,'x'=4,'c'=2,'tp'=4] {'z','x'}, dimensions={0} | all-to-all | bytes 524288 | tf_op jit(solution)/shard_map/all_to_all | solution.py:234
  29.8 4.6 %all-to-all-start.3 = ((bf16[32,8,512]{2,1,0:T(8,128)(2,1)}), bf16[32,8,512]{2,1,0:T(8,128)(2,1)S(1)}, u32[]{:S(2)}, u32[]{:S(2)}) async-start(bf16[32,8,512]{2,1,0:T(8,128)(2,1)} %bitcast.30), calls=%async_computation.3 | async-start | bytes 524288 | tf_op jit(solution)/shard_map/all_to_all | solution.py:234
  34.5 1.7 collective-permute-start.13
  36.1 1.7 collective-permute-start.14
  37.8 8.2 %all-to-all-done.3 = bf16[32,8,512]{2,1,0:T(8,128)(2,1)S(1)} async-done(((bf16[32,8,512]{2,1,0:T(8,128)(2,1)}), bf16[32,8,512]{2,1,0:T(8,128)(2,1)S(1)}, u32[]{:S(2)}, u32[]{:S(2)}) %all-to-all-start.3) | async-done | bytes 262176 | tf_op jit(solution)/shard_map/all_to_all | solution.py:234
  46.0 1.6 collective-permute-start.2
  47.5 1.7 collective-permute-start.3
  49.2 1.5 copy.16.decay_ref
  50.7 2.6 %inner.1 = (f32[256,256]{1,0:T(8,128)}, f32[128,128]{1,0:T(8,128)}, f32[8,128]{1,0:T(8,128)}, bf16[144,128]{1,0:T(8,128)(2,1)}) custom-call(bf16[256,256]{1,0:T(8,128)(2,1)} %q_ref.3, bf16[256,256]{1,0:T(8,128)(2,1)} %k_ref.1, bf16[256,256]{1,0:T(8,128)(2,1)} %v_ref.1, f32[256,2]{1,0:T(8,128)} %copy.16.decay_ref), custom_call_target="tpu_custom_call" | custom-call | tf_op jit(solution)/shard_map/inner/pallas_call | solution.py:38
  53.3 1.4 collective-permute-done.got_ref
  54.7 0.6 copy-done.12
  55.3 1.5 pair.1
  56.8 4.7 %all-to-all-start = ((bf16[32,8,128]{2,1,0:T(8,128)(2,1)}), bf16[32,8,128]{2,1,0:T(8,128)(2,1)S(1)}, u32[]{:S(2)}, u32[]{:S(2)}) async-start(bf16[32,8,128]{2,1,0:T(8,128)(2,1)} %pair.1), calls=%async_computation | async-start | bytes 131072 | tf_op jit(solution)/shard_map/all_to_all | solution.py:234
  61.5 0.4 collective-permute-start.15
  62.0 2.9 %collective-permute-start.16 = (bf16[128,512]{1,0:T(8,128)(2,1)S(1)}, bf16[128,512]{1,0:T(8,128)(2,1)S(1)}, u32[]{:S(2)}, u32[]{:S(2)}) collective-permute-start(bf16[128,512]{1,0:T(8,128)(2,1)S(1)} %slice.35), channel_id=1, source_target_pairs={{0,3},{1,0},{2,1},{3,2},{4,7},{5,4},{6,5},{7,6},{8,11},{9,8},{10,9... | collective-permute-start | bytes 393224 | tf_op jit(solution)/shard_map/ppermute | solution.py:229
  65.0 5.6 %all-to-all-done.in_ref = bf16[32,8,128]{2,1,0:T(8,128)(2,1)S(1)} async-done(((bf16[32,8,128]{2,1,0:T(8,128)(2,1)}), bf16[32,8,128]{2,1,0:T(8,128)(2,1)S(1)}, u32[]{:S(2)}, u32[]{:S(2)}) %all-to-all-start) | async-done | bytes 65568 | tf_op jit(solution)/shard_map/all_to_all | solution.py:234
  70.5 0.6 copy-done.9
  71.2 1.5 scan.1
  72.7 4.7 %all-to-all-start.1 = ((bf16[32,8,128]{2,1,0:T(8,128)(2,1)}), bf16[32,8,128]{2,1,0:T(8,128)(2,1)S(1)}, u32[]{:S(2)}, u32[]{:S(2)}) async-start(bf16[32,8,128]{2,1,0:T(8,128)(2,1)} %scan.1), calls=%async_computation.1 | async-start | bytes 131072 | tf_op jit(solution)/shard_map/all_to_all | solution.py:234
  77.4 0.4 collective-permute-start.4
  77.9 3.1 %collective-permute-start.5 = (bf16[128,512]{1,0:T(8,128)(2,1)S(1)}, bf16[128,512]{1,0:T(8,128)(2,1)S(1)}, u32[]{:S(2)}, u32[]{:S(2)}) collective-permute-start(bf16[128,512]{1,0:T(8,128)(2,1)S(1)} %slice.33), channel_id=1, source_target_pairs={{0,3},{1,0},{2,1},{3,2},{4,7},{5,4},{6,5},{7,6},{8,11},{9,8},{10,9... | collective-permute-start | bytes 393224 | tf_op jit(solution)/shard_map/ppermute | solution.py:229
  81.1 0.6 copy-done.15
  81.7 8.7 %ffn.3 = (bf16[128,512]{1,0:T(8,128)(2,1)}, bf16[128,512]{1,0:T(8,128)(2,1)}, bf16[128,512]{1,0:T(8,128)(2,1)}, bf16[128,512]{1,0:T(8,128)(2,1)}, bf16[128,512]{...) custom-call(bf16[256,512]{1,0:T(8,128)(2,1)} %bitcast.27, bf16[256,512]{1,0:T(8,128)(2,1)} %copy-done.5, ...), custom_call_target="tpu_custom_call" | custom-call | tf_op jit(solution)/shard_map/ffn/pallas_call | solution.py:38
  90.5 0.7 collective-permute-start.21
  91.1 0.6 copy-done.8
  91.8 1.5 entering.1
  93.3 1.4 collective-permute-done.1.got_ref
  94.7 0.6 copy-done.19
  95.3 3.6 %mixer.1 = bf16[256,2048]{1,0:T(8,128)(2,1)} custom-call(f32[256,256]{1,0:T(8,128)} %get-tuple-element.24.inner_ref, bf16[256,256]{1,0:T(8,128)(2,1)} %q_ref.3, f32[256,2]{1,0:T(8,128)} %copy.16.decay_ref, bf16[128,128]{1,0:T(8,128)(2,1)} %get-tuple-element.28.keep_ref, bf16[128,128]{1,0:T(8,128)(2,1)} %copy-done.19, f32[2,128]{1,0:T(2,128)} %gain_ref.1, ...), custom_call_target="tpu_custom_call" | custom-call | tf_op jit(solution)/shard_map/mixer/pallas_call | solution.py:38
  98.9 3.5 %all-to-all-start.2 = ((bf16[4,64,2048]{2,1,0:T(8,128)(2,1)}), bf16[4,64,2048]{2,1,0:T(8,128)(2,1)S(1)}, u32[]{:S(2)}, u32[]{:S(2)}) async-start(bf16[4,64,2048]{2,1,0:T(8,128)(2,1)} %bitcast.21), calls=%async_computation.2 | async-start | bytes 2097152 | tf_op jit(solution)/shard_map/all_to_all | solution.py:342
  102.5 0.6 copy-done.13
  103.2 0.7 copy-done.14
  103.8 8.7 %ffn.2 = (bf16[128,512]{1,0:T(8,128)(2,1)}, bf16[128,512]{1,0:T(8,128)(2,1)}, bf16[128,512]{1,0:T(8,128)(2,1)}, bf16[128,512]{1,0:T(8,128)(2,1)}, bf16[128,512]{...) custom-call(bf16[256,512]{1,0:T(8,128)(2,1)} %bitcast.24, bf16[256,512]{1,0:T(8,128)(2,1)} %copy-done.3, ...), custom_call_target="tpu_custom_call" | custom-call | tf_op jit(solution)/shard_map/ffn/pallas_call | solution.py:38
  112.5 3.3 %collective-permute-start.10 = (bf16[128,512]{1,0:T(8,128)(2,1)}, bf16[128,512]{1,0:T(8,128)(2,1)S(1)}, u32[]{:S(2)}, u32[]{:S(2)}) collective-permute-start(bf16[128,512]{1,0:T(8,128)(2,1)} %get-tuple-element.37), channel_id=1, source_target_pairs={{0,3},{1,0},{2,1},{3,2},{4,7},{5,4},{6,5},{7,6},{8,11},{9,8},{10,9... | collective-permute-start | bytes 393224 | tf_op jit(solution)/shard_map/ppermute | solution.py:229
  115.8 0.8 collective-permute-start.17
  116.6 2.5 %collective-permute-start.19 = (bf16[128,512]{1,0:T(8,128)(2,1)S(1)}, bf16[128,512]{1,0:T(8,128)(2,1)S(1)}, u32[]{:S(2)}, u32[]{:S(2)}) collective-permute-start(bf16[128,512]{1,0:T(8,128)(2,1)S(1)} %copy-done.22), channel_id=1, source_target_pairs={{0,3},{1,0},{2,1},{3,2},{4,7},{5,4},{6,5},{7,6},{8,11},{9,8},{10,9... | collective-permute-start | bytes 393224 | tf_op jit(solution)/shard_map/ppermute | solution.py:229
  119.2 7.2 %collective-permute-done.17 = bf16[128,512]{1,0:T(8,128)(2,1)S(1)} collective-permute-done((bf16[128,512]{1,0:T(8,128)(2,1)S(1)}, bf16[128,512]{1,0:T(8,128)(2,1)S(1)}, u32[]{:S(2)}, u32[]{:S(2)}) %collective-permute-start.17) | collective-permute-done | bytes 131104 | tf_op jit(solution)/shard_map/ppermute | solution.py:229
  126.4 2.1 %collective-permute-start.18 = (bf16[128,512]{1,0:T(8,128)(2,1)S(1)}, bf16[128,512]{1,0:T(8,128)(2,1)S(1)}, u32[]{:S(2)}, u32[]{:S(2)}) collective-permute-start(bf16[128,512]{1,0:T(8,128)(2,1)S(1)} %add_convert_fusion.3), channel_id=1, source_target_pairs={{0,1},{1,2},{2,3},{3,0},{4,5},{5,6},{6,7},{7,4},{8,9},{9,10},{10,1... | collective-permute-start | bytes 393224 | tf_op jit(solution)/shard_map/ppermute | solution.py:229
  128.5 0.9 add_convert_fusion.5
  129.5 1.3 collective-permute-start.8
  130.8 0.8 collective-permute-start.9
  131.6 1.2 collective-permute-done.22
  132.8 1.3 collective-permute-start.11
  134.0 0.1 add_convert_fusion.2
  134.1 0.8 maximum_bitcast_fusion.1
  134.9 9.9 %all-to-all-start.6 = ((bf16[32,8,512]{2,1,0:T(8,128)(2,1)}), bf16[32,8,512]{2,1,0:T(8,128)(2,1)S(1)}, u32[]{:S(2)}, u32[]{:S(2)}) async-start(bf16[32,8,512]{2,1,0:T(8,128)(2,1)} %maximum_bitcast_fusion.1), calls=%async_computation.6 | async-start | bytes 524288 | tf_op jit(solution)/shard_map/all_to_all | solution.py:234
  144.8 0.9 add_convert_fusion.7
  145.7 0.8 collective-permute-start.7
  146.6 5.4 %collective-permute-done.7 = bf16[128,512]{1,0:T(8,128)(2,1)S(1)} collective-permute-done((bf16[128,512]{1,0:T(8,128)(2,1)S(1)}, bf16[128,512]{1,0:T(8,128)(2,1)S(1)}, u32[]{:S(2)}, u32[]{:S(2)}) %collective-permute-start.7) | collective-permute-done | bytes 131104 | tf_op jit(solution)/shard_map/ppermute | solution.py:229
  152.0 0.1 add_convert_fusion.6
  152.1 0.7 maximum_bitcast_fusion
  152.8 2.7 %all-to-all-done.6 = bf16[32,8,512]{2,1,0:T(8,128)(2,1)S(1)} async-done(((bf16[32,8,512]{2,1,0:T(8,128)(2,1)}), bf16[32,8,512]{2,1,0:T(8,128)(2,1)S(1)}, u32[]{:S(2)}, u32[]{:S(2)}) %all-to-all-start.6) | async-done | bytes 262176 | tf_op jit(solution)/shard_map/all_to_all | solution.py:234
  155.6 7.0 %all-to-all-start.4 = ((bf16[32,8,512]{2,1,0:T(8,128)(2,1)}), bf16[32,8,512]{2,1,0:T(8,128)(2,1)S(1)}, u32[]{:S(2)}, u32[]{:S(2)}) async-start(bf16[32,8,512]{2,1,0:T(8,128)(2,1)} %maximum_bitcast_fusion), calls=%async_computation.4 | async-start | bytes 524288 | tf_op jit(solution)/shard_map/all_to_all | solution.py:234
  162.6 0.1 collective-permute-start.23
  162.7 0.7 copy.19.w_ref
  163.5 2.0 %blend_weights.1.w_ref = bf16[2,2,256,128]{3,2,1,0:T(8,128)(2,1)} custom-call(s32[128,2]{1,0:T(8,128)} %copy.18.ids_ref, f32[128,2]{1,0:T(8,128)} %copy.19.w_ref), custom_call_target="tpu_custom_call" | custom-call | tf_op jit(solution)/shard_map/blend_weights/pallas_call | solution.py:38
  165.5 0.9 reduce_sum.12
  166.4 7.0 %all-to-all-done.4 = bf16[32,8,512]{2,1,0:T(8,128)(2,1)S(1)} async-done(((bf16[32,8,512]{2,1,0:T(8,128)(2,1)}), bf16[32,8,512]{2,1,0:T(8,128)(2,1)S(1)}, u32[]{:S(2)}, u32[]{:S(2)}) %all-to-all-start.4) | async-done | bytes 262176 | tf_op jit(solution)/shard_map/all_to_all | solution.py:234
  173.4 0.7 copy-done.2
  174.1 0.1 copy-done.7
  174.2 2.1 %blend.1 = bf16[128,512]{1,0:T(8,128)(2,1)} custom-call(bf16[2,2,256,128]{3,2,1,0:T(8,128)(2,1)} %blend_weights.1.w_ref, bf16[256,512]{1,0:T(8,128)(2,1)} %bitcast.28, bf16[256,512]{1,0:T(8,128)(2,1)} %copy-done.7), custom_call_target="tpu_custom_call" | custom-call | tf_op jit(solution)/shard_map/blend/pallas_call | solution.py:38
  (71 shorter events, 0.3 us)
Async XLA Ops:
  4.6 1.7 collective-permute-start.12
  29.8 51.2 %copy-start.1 = (bf16[32,8,512]{2,1,0:T(8,128)(2,1)}, bf16[32,8,512]{2,1,0:T(8,128)(2,1)S(1)}, u32[]{:S(2)}) copy-start(bf16[32,8,512]{2,1,0:T(8,128)(2,1)S(1)} %all_to_all.35) | copy-start | bytes 786436
  29.8 16.1 %all-to-all-start.3 = ((bf16[32,8,512]{2,1,0:T(8,128)(2,1)}), bf16[32,8,512]{2,1,0:T(8,128)(2,1)S(1)}, u32[]{:S(2)}, u32[]{:S(2)}) async-start(bf16[32,8,512]{2,1,0:T(8,128)(2,1)} %bitcast.30), calls=%async_computation.3 | async-start | bytes 524288 | tf_op jit(solution)/shard_map/all_to_all | solution.py:234
  34.5 27.0 %collective-permute-start.13 = (bf16[256,512]{1,0:T(8,128)(2,1)S(1)}, bf16[256,512]{1,0:T(8,128)(2,1)S(1)}, u32[]{:S(2)}, u32[]{:S(2)}) collective-permute-start(bf16[256,512]{1,0:T(8,128)(2,1)S(1)} %bitcast.25), channel_id=1, source_target_pairs={{0,1},{1,2},{2,3},{3,0},{4,5},{5,6},{6,7},{7,4},{8,9},{9,10},{10,1... | collective-permute-start | bytes 786440 | tf_op jit(solution)/shard_map/ppermute | solution.py:229
  36.1 25.9 %collective-permute-start.14 = (bf16[256,512]{1,0:T(8,128)(2,1)S(1)}, bf16[256,512]{1,0:T(8,128)(2,1)S(1)}, u32[]{:S(2)}, u32[]{:S(2)}) collective-permute-start(bf16[256,512]{1,0:T(8,128)(2,1)S(1)} %bitcast.26), channel_id=1, source_target_pairs={{0,3},{1,0},{2,1},{3,2},{4,7},{5,4},{6,5},{7,6},{8,11},{9,8},{10,9... | collective-permute-start | bytes 786440 | tf_op jit(solution)/shard_map/ppermute | solution.py:229
  46.0 44.5 %copy-start = (bf16[32,8,512]{2,1,0:T(8,128)(2,1)}, bf16[32,8,512]{2,1,0:T(8,128)(2,1)S(1)}, u32[]{:S(2)}) copy-start(bf16[32,8,512]{2,1,0:T(8,128)(2,1)S(1)} %all-to-all-done.3) | copy-start | bytes 786436
  46.0 31.4 %collective-permute-start.2 = (bf16[256,512]{1,0:T(8,128)(2,1)S(1)}, bf16[256,512]{1,0:T(8,128)(2,1)S(1)}, u32[]{:S(2)}, u32[]{:S(2)}) collective-permute-start(bf16[256,512]{1,0:T(8,128)(2,1)S(1)} %bitcast.22), channel_id=1, source_target_pairs={{0,1},{1,2},{2,3},{3,0},{4,5},{5,6},{6,7},{7,4},{8,9},{9,10},{10,1... | collective-permute-start | bytes 786440 | tf_op jit(solution)/shard_map/ppermute | solution.py:229
  47.5 30.3 %collective-permute-start.3 = (bf16[256,512]{1,0:T(8,128)(2,1)S(1)}, bf16[256,512]{1,0:T(8,128)(2,1)S(1)}, u32[]{:S(2)}, u32[]{:S(2)}) collective-permute-start(bf16[256,512]{1,0:T(8,128)(2,1)S(1)} %bitcast.23), channel_id=1, source_target_pairs={{0,3},{1,0},{2,1},{3,2},{4,7},{5,4},{6,5},{7,6},{8,11},{9,8},{10,9... | collective-permute-start | bytes 786440 | tf_op jit(solution)/shard_map/ppermute | solution.py:229
  53.3 1.4 collective-permute-start
  54.7 0.6 copy-start.12
  56.8 13.7 %all-to-all-start = ((bf16[32,8,128]{2,1,0:T(8,128)(2,1)}), bf16[32,8,128]{2,1,0:T(8,128)(2,1)S(1)}, u32[]{:S(2)}, u32[]{:S(2)}) async-start(bf16[32,8,128]{2,1,0:T(8,128)(2,1)} %pair.1), calls=%async_computation | async-start | bytes 131072 | tf_op jit(solution)/shard_map/all_to_all | solution.py:234
  61.5 19.6 %copy-start.5 = (bf16[256,512]{1,0:T(8,128)(2,1)}, bf16[256,512]{1,0:T(8,128)(2,1)S(1)}, u32[]{:S(2)}) copy-start(bf16[256,512]{1,0:T(8,128)(2,1)S(1)} %collective-permute-done.13.left) | copy-start | bytes 786436
  61.5 19.5 %collective-permute-start.15 = (bf16[128,512]{1,0:T(8,128)(2,1)S(1)}, bf16[128,512]{1,0:T(8,128)(2,1)S(1)}, u32[]{:S(2)}, u32[]{:S(2)}) collective-permute-start(bf16[128,512]{1,0:T(8,128)(2,1)S(1)} %slice.34), channel_id=1, source_target_pairs={{0,1},{1,2},{2,3},{3,0},{4,5},{5,6},{6,7},{7,4},{8,9},{9,10},{10,1... | collective-permute-start | bytes 393224 | tf_op jit(solution)/shard_map/ppermute | solution.py:229
  62.0 19.1 %copy-start.6 = (bf16[256,512]{1,0:T(8,128)(2,1)}, bf16[256,512]{1,0:T(8,128)(2,1)S(1)}, u32[]{:S(2)}) copy-start(bf16[256,512]{1,0:T(8,128)(2,1)S(1)} %collective-permute-done.14.right) | copy-start | bytes 786436
  62.0 19.0 %collective-permute-start.16 = (bf16[128,512]{1,0:T(8,128)(2,1)S(1)}, bf16[128,512]{1,0:T(8,128)(2,1)S(1)}, u32[]{:S(2)}, u32[]{:S(2)}) collective-permute-start(bf16[128,512]{1,0:T(8,128)(2,1)S(1)} %slice.35), channel_id=1, source_target_pairs={{0,3},{1,0},{2,1},{3,2},{4,7},{5,4},{6,5},{7,6},{8,11},{9,8},{10,9... | collective-permute-start | bytes 393224 | tf_op jit(solution)/shard_map/ppermute | solution.py:229
  70.5 0.6 copy-start.9
  72.7 18.4 %all-to-all-start.1 = ((bf16[32,8,128]{2,1,0:T(8,128)(2,1)}), bf16[32,8,128]{2,1,0:T(8,128)(2,1)S(1)}, u32[]{:S(2)}, u32[]{:S(2)}) async-start(bf16[32,8,128]{2,1,0:T(8,128)(2,1)} %scan.1), calls=%async_computation.1 | async-start | bytes 131072 | tf_op jit(solution)/shard_map/all_to_all | solution.py:234
  77.4 13.0 %copy-start.3 = (bf16[256,512]{1,0:T(8,128)(2,1)}, bf16[256,512]{1,0:T(8,128)(2,1)S(1)}, u32[]{:S(2)}) copy-start(bf16[256,512]{1,0:T(8,128)(2,1)S(1)} %collective-permute-done.2.left) | copy-start | bytes 786436
  77.4 25.0 %collective-permute-start.4 = (bf16[128,512]{1,0:T(8,128)(2,1)S(1)}, bf16[128,512]{1,0:T(8,128)(2,1)S(1)}, u32[]{:S(2)}, u32[]{:S(2)}) collective-permute-start(bf16[128,512]{1,0:T(8,128)(2,1)S(1)} %slice.32), channel_id=1, source_target_pairs={{0,1},{1,2},{2,3},{3,0},{4,5},{5,6},{6,7},{7,4},{8,9},{9,10},{10,1... | collective-permute-start | bytes 393224 | tf_op jit(solution)/shard_map/ppermute | solution.py:229
  77.9 12.6 %copy-start.4 = (bf16[256,512]{1,0:T(8,128)(2,1)}, bf16[256,512]{1,0:T(8,128)(2,1)S(1)}, u32[]{:S(2)}) copy-start(bf16[256,512]{1,0:T(8,128)(2,1)S(1)} %collective-permute-done.3.right) | copy-start | bytes 786436
  77.9 24.6 %collective-permute-start.5 = (bf16[128,512]{1,0:T(8,128)(2,1)S(1)}, bf16[128,512]{1,0:T(8,128)(2,1)S(1)}, u32[]{:S(2)}, u32[]{:S(2)}) collective-permute-start(bf16[128,512]{1,0:T(8,128)(2,1)S(1)} %slice.33), channel_id=1, source_target_pairs={{0,3},{1,0},{2,1},{3,2},{4,7},{5,4},{6,5},{7,6},{8,11},{9,8},{10,9... | collective-permute-start | bytes 393224 | tf_op jit(solution)/shard_map/ppermute | solution.py:229
  81.0 0.6 copy-start.15
  81.0 0.7 copy-start.16
  90.5 28.6 %collective-permute-start.21 = (bf16[128,512]{1,0:T(8,128)(2,1)}, bf16[128,512]{1,0:T(8,128)(2,1)S(1)}, u32[]{:S(2)}, u32[]{:S(2)}) collective-permute-start(bf16[128,512]{1,0:T(8,128)(2,1)} %get-tuple-element.45), channel_id=1, source_target_pairs={{0,3},{1,0},{2,1},{3,2},{4,7},{5,4},{6,5},{7,6},{8,11},{9,8},{10,9... | collective-permute-start | bytes 393224 | tf_op jit(solution)/shard_map/ppermute | solution.py:229
  91.1 0.6 copy-start.8
  93.3 1.4 collective-permute-start.1
  94.7 0.6 copy-start.19
  98.9 36.0 %all-to-all-start.2 = ((bf16[4,64,2048]{2,1,0:T(8,128)(2,1)}), bf16[4,64,2048]{2,1,0:T(8,128)(2,1)S(1)}, u32[]{:S(2)}, u32[]{:S(2)}) async-start(bf16[4,64,2048]{2,1,0:T(8,128)(2,1)} %bitcast.21), calls=%async_computation.2 | async-start | bytes 2097152 | tf_op jit(solution)/shard_map/all_to_all | solution.py:342
  102.4 13.4 %copy-start.23 = (bf16[128,512]{1,0:T(8,128)(2,1)S(1)}, bf16[128,512]{1,0:T(8,128)(2,1)}, u32[]{:S(2)}) copy-start(bf16[128,512]{1,0:T(8,128)(2,1)} %get-tuple-element.41) | copy-start | bytes 393220
  102.4 14.2 %copy-start.22 = (bf16[128,512]{1,0:T(8,128)(2,1)S(1)}, bf16[128,512]{1,0:T(8,128)(2,1)}, u32[]{:S(2)}) copy-start(bf16[128,512]{1,0:T(8,128)(2,1)} %get-tuple-element.42) | copy-start | bytes 393220
  102.4 16.7 %copy-start.21 = (bf16[128,512]{1,0:T(8,128)(2,1)S(1)}, bf16[128,512]{1,0:T(8,128)(2,1)}, u32[]{:S(2)}) copy-start(bf16[128,512]{1,0:T(8,128)(2,1)} %get-tuple-element.43) | copy-start | bytes 393220
  102.5 16.7 %copy-start.18 = (bf16[128,512]{1,0:T(8,128)(2,1)S(1)}, bf16[128,512]{1,0:T(8,128)(2,1)}, u32[]{:S(2)}) copy-start(bf16[128,512]{1,0:T(8,128)(2,1)} %get-tuple-element.44) | copy-start | bytes 393220
  102.5 23.9 %copy-start.17 = (bf16[128,512]{1,0:T(8,128)(2,1)S(1)}, bf16[128,512]{1,0:T(8,128)(2,1)}, u32[]{:S(2)}) copy-start(bf16[128,512]{1,0:T(8,128)(2,1)} %get-tuple-element.40) | copy-start | bytes 393220
  102.5 31.6 %copy-start.10 = (bf16[256,512]{1,0:T(8,128)(2,1)S(1)}, bf16[256,512]{1,0:T(8,128)(2,1)}, u32[]{:S(2)}) copy-start(bf16[256,512]{1,0:T(8,128)(2,1)} %get-tuple-element.39) | copy-start | bytes 786436
  102.5 0.7 copy-start.13
  103.2 0.7 copy-start.14
  112.5 39.5 %copy-start.11 = (bf16[256,512]{1,0:T(8,128)(2,1)S(1)}, bf16[256,512]{1,0:T(8,128)(2,1)}, u32[]{:S(2)}) copy-start(bf16[256,512]{1,0:T(8,128)(2,1)} %get-tuple-element.31) | copy-start | bytes 786436
  112.5 50.2 %copy-start.20 = (f32[128,2]{0,1:T(2,128)S(1)}, f32[128,2]{0,1:T(2,128)}, u32[]{:S(2)}) copy-start(f32[128,2]{0,1:T(2,128)} %param.27) | copy-start | bytes 3076
  112.5 13.9 %collective-permute-start.10 = (bf16[128,512]{1,0:T(8,128)(2,1)}, bf16[128,512]{1,0:T(8,128)(2,1)S(1)}, u32[]{:S(2)}, u32[]{:S(2)}) collective-permute-start(bf16[128,512]{1,0:T(8,128)(2,1)} %get-tuple-element.37), channel_id=1, source_target_pairs={{0,3},{1,0},{2,1},{3,2},{4,7},{5,4},{6,5},{7,6},{8,11},{9,8},{10,9... | collective-permute-start | bytes 393224 | tf_op jit(solution)/shard_map/ppermute | solution.py:229
  115.8 29.0 %collective-permute-start.6 = (bf16[128,512]{1,0:T(8,128)(2,1)}, bf16[128,512]{1,0:T(8,128)(2,1)S(1)}, u32[]{:S(2)}, u32[]{:S(2)}) collective-permute-start(bf16[128,512]{1,0:T(8,128)(2,1)} %get-tuple-element.33), channel_id=1, source_target_pairs={{0,1},{1,2},{2,3},{3,0},{4,5},{5,6},{6,7},{7,4},{8,9},{9,10},{10,1... | collective-permute-start | bytes 393224 | tf_op jit(solution)/shard_map/ppermute | solution.py:229
  115.8 10.6 %collective-permute-start.17 = (bf16[128,512]{1,0:T(8,128)(2,1)S(1)}, bf16[128,512]{1,0:T(8,128)(2,1)S(1)}, u32[]{:S(2)}, u32[]{:S(2)}) collective-permute-start(bf16[128,512]{1,0:T(8,128)(2,1)S(1)} %copy-done.23), channel_id=1, source_target_pairs={{0,1},{1,2},{2,3},{3,0},{4,5},{5,6},{6,7},{7,4},{8,9},{9,10},{10,1... | collective-permute-start | bytes 393224 | tf_op jit(solution)/shard_map/ppermute | solution.py:229
  116.6 12.9 %collective-permute-start.19 = (bf16[128,512]{1,0:T(8,128)(2,1)S(1)}, bf16[128,512]{1,0:T(8,128)(2,1)S(1)}, u32[]{:S(2)}, u32[]{:S(2)}) collective-permute-start(bf16[128,512]{1,0:T(8,128)(2,1)S(1)} %copy-done.22), channel_id=1, source_target_pairs={{0,3},{1,0},{2,1},{3,2},{4,7},{5,4},{6,5},{7,6},{8,11},{9,8},{10,9... | collective-permute-start | bytes 393224 | tf_op jit(solution)/shard_map/ppermute | solution.py:229
  119.1 11.7 %collective-permute-start.20 = (bf16[128,512]{1,0:T(8,128)(2,1)S(1)}, bf16[128,512]{1,0:T(8,128)(2,1)S(1)}, u32[]{:S(2)}, u32[]{:S(2)}) collective-permute-start(bf16[128,512]{1,0:T(8,128)(2,1)S(1)} %copy-done.21), channel_id=1, source_target_pairs={{0,1},{1,2},{2,3},{3,0},{4,5},{5,6},{6,7},{7,4},{8,9},{9,10},{10,1... | collective-permute-start | bytes 393224 | tf_op jit(solution)/shard_map/ppermute | solution.py:229
  126.4 6.4 %collective-permute-start.22 = (bf16[128,512]{1,0:T(8,128)(2,1)S(1)}, bf16[128,512]{1,0:T(8,128)(2,1)S(1)}, u32[]{:S(2)}, u32[]{:S(2)}) collective-permute-start(bf16[128,512]{1,0:T(8,128)(2,1)S(1)} %add_convert_fusion.1), channel_id=1, source_target_pairs={{0,3},{1,0},{2,1},{3,2},{4,7},{5,4},{6,5},{7,6},{8,11},{9,8},{10,9... | collective-permute-start | bytes 393224 | tf_op jit(solution)/shard_map/ppermute | solution.py:229
  126.4 7.6 %collective-permute-start.18 = (bf16[128,512]{1,0:T(8,128)(2,1)S(1)}, bf16[128,512]{1,0:T(8,128)(2,1)S(1)}, u32[]{:S(2)}, u32[]{:S(2)}) collective-permute-start(bf16[128,512]{1,0:T(8,128)(2,1)S(1)} %add_convert_fusion.3), channel_id=1, source_target_pairs={{0,1},{1,2},{2,3},{3,0},{4,5},{5,6},{6,7},{7,4},{8,9},{9,10},{10,1... | collective-permute-start | bytes 393224 | tf_op jit(solution)/shard_map/ppermute | solution.py:229
  129.5 17.1 %collective-permute-start.8 = (bf16[128,512]{1,0:T(8,128)(2,1)}, bf16[128,512]{1,0:T(8,128)(2,1)S(1)}, u32[]{:S(2)}, u32[]{:S(2)}) collective-permute-start(bf16[128,512]{1,0:T(8,128)(2,1)} %get-tuple-element.34), channel_id=1, source_target_pairs={{0,3},{1,0},{2,1},{3,2},{4,7},{5,4},{6,5},{7,6},{8,11},{9,8},{10,9... | collective-permute-start | bytes 393224 | tf_op jit(solution)/shard_map/ppermute | solution.py:229
  130.8 15.8 %collective-permute-start.9 = (bf16[128,512]{1,0:T(8,128)(2,1)}, bf16[128,512]{1,0:T(8,128)(2,1)S(1)}, u32[]{:S(2)}, u32[]{:S(2)}) collective-permute-start(bf16[128,512]{1,0:T(8,128)(2,1)} %get-tuple-element.35), channel_id=1, source_target_pairs={{0,1},{1,2},{2,3},{3,0},{4,5},{5,6},{6,7},{7,4},{8,9},{9,10},{10,1... | collective-permute-start | bytes 393224 | tf_op jit(solution)/shard_map/ppermute | solution.py:229
  132.8 13.8 %collective-permute-start.11 = (bf16[128,512]{1,0:T(8,128)(2,1)S(1)}, bf16[128,512]{1,0:T(8,128)(2,1)S(1)}, u32[]{:S(2)}, u32[]{:S(2)}) collective-permute-start(bf16[128,512]{1,0:T(8,128)(2,1)S(1)} %add_convert_fusion.5), channel_id=1, source_target_pairs={{0,3},{1,0},{2,1},{3,2},{4,7},{5,4},{6,5},{7,6},{8,11},{9,8},{10,9... | collective-permute-start | bytes 393224 | tf_op jit(solution)/shard_map/ppermute | solution.py:229
  134.9 20.7 %all-to-all-start.6 = ((bf16[32,8,512]{2,1,0:T(8,128)(2,1)}), bf16[32,8,512]{2,1,0:T(8,128)(2,1)S(1)}, u32[]{:S(2)}, u32[]{:S(2)}) async-start(bf16[32,8,512]{2,1,0:T(8,128)(2,1)} %maximum_bitcast_fusion.1), calls=%async_computation.6 | async-start | bytes 524288 | tf_op jit(solution)/shard_map/all_to_all | solution.py:234
  145.7 6.3 %collective-permute-start.7 = (bf16[128,512]{1,0:T(8,128)(2,1)S(1)}, bf16[128,512]{1,0:T(8,128)(2,1)S(1)}, u32[]{:S(2)}, u32[]{:S(2)}) collective-permute-start(bf16[128,512]{1,0:T(8,128)(2,1)S(1)} %add_convert_fusion.7), channel_id=1, source_target_pairs={{0,1},{1,2},{2,3},{3,0},{4,5},{5,6},{6,7},{7,4},{8,9},{9,10},{10,1... | collective-permute-start | bytes 393224 | tf_op jit(solution)/shard_map/ppermute | solution.py:229
  155.6 17.8 %all-to-all-start.4 = ((bf16[32,8,512]{2,1,0:T(8,128)(2,1)}), bf16[32,8,512]{2,1,0:T(8,128)(2,1)S(1)}, u32[]{:S(2)}, u32[]{:S(2)}) async-start(bf16[32,8,512]{2,1,0:T(8,128)(2,1)} %maximum_bitcast_fusion), calls=%async_computation.4 | async-start | bytes 524288 | tf_op jit(solution)/shard_map/all_to_all | solution.py:234
  162.6 10.8 %collective-permute-start.23 = (bf16[256,512]{1,0:T(8,128)(2,1)S(1)}, bf16[256,512]{1,0:T(8,128)(2,1)S(1)}, u32[]{:S(2)}, u32[]{:S(2)}) collective-permute-start(bf16[256,512]{1,0:T(8,128)(2,1)S(1)} %bitcast.29), channel_id=1, source_target_pairs={{0,4},{4,0},{1,5},{5,1},{2,6},{6,2},{3,7},{7,3},{8,12},{12,8},{9,1... | collective-permute-start | bytes 786440 | tf_op jit(solution)/shard_map/ppermute | solution.py:229
  173.4 0.7 copy-start.2
  173.4 0.8 copy-start.7

commit v2 on v1

v2 whole, which is shorter than its diff:
```python
import functools

import jax
import jax.numpy as jnp
from jax import lax
from jax.experimental import pallas as pl
from jax.experimental.pallas import tpu as pltpu
from jax.sharding import Mesh
from jax.sharding import PartitionSpec as P


EP = ("z", "x", "c")
ZX = ("z", "x")
F32 = jnp.float32
BF16 = jnp.bfloat16
epsilon = 1e-06
VMEM_LIMIT = 16 << 20


def iota(shape, dim):
    return lax.broadcasted_iota(jnp.int32, shape, dim)


def dot(a, b):
    return jnp.dot(a, b, preferred_element_type=F32)


def dot_t(a, b):
    return lax.dot_general(a, b, (((0,), (0,)), ((), ())), preferred_element_type=F32)


def three_parts(x):
    a = x.astype(BF16)
    rest = x - a.astype(F32)
    b = rest.astype(BF16)
    return a, b, (rest - b.astype(F32)).astype(BF16)


def call(body, outs, *args, plain=0, held=(), scratch_shapes=(), limit=VMEM_LIMIT):
    space = pl.BlockSpec(memory_space=pltpu.VMEM)
    kernel = pl.pallas_call(
        body,
        out_shape=outs,
        in_specs=[pl.BlockSpec(memory_space=pl.ANY)] * len(held) + [space] * len(args),
        out_specs=[space] * len(outs) if isinstance(outs, list) else space,
        scratch_shapes=scratch_shapes,
        compiler_params=pltpu.CompilerParams(vmem_limit_bytes=limit),
    )
    hbm = [pltpu.with_memory_space_constraint(a, pltpu.HBM) for a in (*held, *args[:plain])]
    return kernel(*hbm, *(pltpu.with_memory_space_constraint(a, pltpu.VMEM) for a in args[plain:]))


def array(shape, dtype):
    return pltpu.VMEM(shape, dtype)


def slot_members(ids_ref, half, rows, capacity):
    tokens = ids_ref.shape[1]
    core = lax.axis_index("c")
    slot = iota((rows, 1), 0)
    expert = (slot // capacity) * 2 + (core + half - 2 * core * half)
    first, second = ids_ref[0:1] == expert, ids_ref[1:2] == expert
    member = jnp.where(first | second, 1.0, 0.0)
    earlier = (iota((tokens, tokens), 0) < iota((tokens, tokens), 1)).astype(BF16)
    here = dot(member.astype(BF16), earlier).astype(jnp.int32) == slot % capacity
    return first & here, second & here


def dispatch_kernel(capacity, ids_ref, x_ref, gain_ref, keep_ref, send_ref):
    part = keep_ref.shape[1]
    x = x_ref[...].astype(F32)
    scale = lax.rsqrt(jnp.mean(x * x, axis=-1, keepdims=True) + epsilon)
    cols = pl.ds(pl.multiple_of(lax.axis_index("tp") * part, part), part)
    normed = (x_ref[:, cols].astype(F32) * scale * gain_ref[:, cols]).astype(BF16)
    for half, ref in enumerate((keep_ref, send_ref)):
        first, second = slot_members(ids_ref, half, ref.shape[0], capacity)
        hot = jnp.where(first | second, 1.0, 0.0).astype(BF16)
        ref[...] = dot(hot, normed).astype(BF16)


def blend_weights_kernel(capacity, ids_ref, w_ref, out_ref):
    for half in range(2):
        first, second = slot_members(ids_ref, half, out_ref.shape[2], capacity)
        blend = jnp.where(first, w_ref[0:1], 0.0) + jnp.where(second, w_ref[1:2], 0.0)
        hi = blend.astype(BF16)
        out_ref[half, 0] = hi
        out_ref[half, 1] = (blend - hi.astype(F32)).astype(BF16)


def blend_kernel(w_ref, back_ref, sent_ref, out_ref):
    keep = jnp.concatenate([back_ref[j, 0:8] for j in range(back_ref.shape[0])], axis=0)
    total = 0.0
    for half, rows in enumerate((keep, sent_ref[...])):
        total = total + dot_t(w_ref[half, 0], rows) + dot_t(w_ref[half, 1], rows)
    out_ref[...] = total.astype(BF16)


def parted_kernel(back_ref, out_ref):
    for j in range(back_ref.shape[0]):
        out_ref[8 * j : 8 * j + 8] = back_ref[j, 8:16]


def span(k, size):
    n = lax.axis_size("tp")
    return pl.ds(pl.multiple_of(lax.rem(lax.axis_index("tp") + k, n) * size, size), size)


def tiles(size):
    return [slice(lo, min(size, lo + 256)) for lo in range(0, size, 256)]


def started(sems, *pairs):
    copies = [pltpu.make_async_copy(src, dst, sems.at[i]) for i, (src, dst) in enumerate(pairs)]
    for copy in copies:
        copy.start()
    return copies


def near_kernel(gate, up, down, own, left_a, left_b, right_a, right_b, g_ref, u_ref, far_gate, far_up, far_down, gates, ups, sems):
    part = own.shape[1]
    left = (left_a, left_b)
    right = (right_a, right_b)
    order = ((0, (own,)), (3, left), (1, right))
    copies = started(
        sems,
        *(
            pair
            for i, (k, _) in enumerate(order)
            for pair in ((gate.at[span(k, part)], gates.at[i]), (up.at[span(k, part)], ups.at[i]))
        ),
        (gate.at[span(2, part)], far_gate),
        (up.at[span(2, part)], far_up),
        (down.at[:, span(2, part)], far_down),
    )
    for i, (_, refs) in enumerate(order):
        x = jnp.concatenate([r[...] for r in refs], axis=0)
        for weights, total, copy in ((gates, g_ref, copies[2 * i]), (ups, u_ref, copies[2 * i + 1])):
            copy.wait()
            for cols in tiles(total.shape[1]):
                new = dot(x, weights[i, :, cols])
                total[:, cols] = new if i == 0 else total[:, cols] + new
    for copy in copies[6:]:
        copy.wait()


def far_kernel(far_a, far_b, g_in, u_in, gate, up, down, hid_ref, to2a, to2b):
    half = far_a.shape[0]
    far = jnp.concatenate([far_a[...], far_b[...]], axis=0)
    for cols in tiles(gate.shape[1]):
        g = g_in[:, cols] + dot(far, gate[:, cols])
        u = u_in[:, cols] + dot(far, up[:, cols])
        hid_ref[:, cols] = (g * jax.nn.sigmoid(g) * u).astype(BF16)
    out = dot(hid_ref[...], down[...]).astype(BF16)
    to2a[...] = out[:half]
    to2b[...] = out[half:]


def rest_kernel(down, hid, to1a, to1b, tom1a, tom1b, mine, downs, sems):
    part, half = to1a.shape[1], to1a.shape[0]
    order = (1, 3, 0)
    copies = started(sems, *((down.at[:, span(k, part)], downs.at[i]) for i, k in enumerate(order)))
    for i, pair in enumerate(((to1a, to1b), (tom1a, tom1b), (mine.at[:half], mine.at[half:]))):
        copies[i].wait()
        out = dot(hid[...], downs[i]).astype(BF16)
        for ref, rows in zip(pair, (out[:half], out[half:])):
            ref[...] = rows


def onward_kernel(to1a, tom1b, got_a, got_b, out1, outm1):
    out1[...] = (to1a[...].astype(F32) + got_a[...].astype(F32)).astype(BF16)
    outm1[...] = (tom1b[...].astype(F32) + got_b[...].astype(F32)).astype(BF16)


def settle_kernel(mine, top_l, low_l, top_r, low_r, out):
    half = top_l.shape[0]
    for rows, a, b in ((slice(0, half), top_l, top_r), (slice(half, 2 * half), low_l, low_r)):
        out[rows] = (mine[rows].astype(F32) + a[...].astype(F32) + b[...].astype(F32)).astype(BF16)


def join_kernel(keep_ref, got_ref, out_ref):
    for j in range(out_ref.shape[0]):
        out_ref[j, 0:8] = keep_ref[8 * j : 8 * j + 8]
        out_ref[j, 8:16] = got_ref[8 * j : 8 * j + 8]


def levels_of(decay):
    n = decay.shape[1]
    parts = jnp.concatenate([t.astype(F32) for t in three_parts(decay)], axis=0).astype(BF16)
    upto = (iota((n, n), 0) >= iota((n, n), 1)).astype(BF16)
    before = (iota((n, n), 0) <= iota((n, n), 1)).astype(BF16)
    col = lax.dot_general(upto, parts, (((1,), (1,)), ((), ())), preferred_element_type=F32)
    row = dot(parts, before)
    return col[:, 0:2] + col[:, 2:4] + col[:, 4:6], row[0:2] + row[2:4] + row[4:6]


def inner_kernel(q_ref, k_ref, v_ref, decay_ref, inner_ref, kept_ref, kept_total_ref, send_ref):
    core = lax.axis_index("c")
    n = q_ref.shape[0]
    col, row = levels_of(decay_ref[...])
    causal = iota((n, n), 0) >= iota((n, n), 1)
    states, totals = [], []
    for h in range(2):
        cols = slice(h * 128, h * 128 + 128)
        q, k, v = q_ref[:, cols], k_ref[:, cols], v_ref[:, cols]
        scores = lax.dot_general(q, k, (((1,), (1,)), ((), ())), preferred_element_type=F32) * 128 ** (-0.5)
        spread = jnp.where(causal, col[:, h : h + 1] - row[h : h + 1], -jnp.inf)
        inner_ref[:, cols] = dot((scores * jnp.exp(spread)).astype(BF16), v)
        total = col[n - 1 : n, h : h + 1]
        scaled = (k.astype(F32) * jnp.exp(total - col[:, h : h + 1])).astype(BF16)
        states.append(dot_t(scaled, v))
        totals.append(total)
    first = core == 0
    kept_ref[...] = jnp.where(first, states[0], states[1])
    kept_total_ref[...] = jnp.broadcast_to(jnp.where(first, totals[0], totals[1]), kept_total_ref.shape)
    send_ref[0:128] = jnp.where(first, states[1], states[0]).astype(BF16)
    send_ref[128:144] = rows_of_total(jnp.where(first, totals[1], totals[0]), 16)


def rows_of_total(total, rows):
    a, b, c = (jnp.broadcast_to(t.astype(F32), (rows, 128)) for t in three_parts(total))
    r = iota((rows, 128), 0)
    return jnp.where(r == 0, a, jnp.where(r == 1, b, jnp.where(r == 2, c, 0.0))).astype(BF16)


def pair_of(kept_ref, kept_total_ref, got_ref):
    first = lax.axis_index("c") == 0
    mine, mine_total = kept_ref[...], kept_total_ref[0:1]
    theirs = got_ref[0:128].astype(F32)
    rows = got_ref[128:144].astype(F32)
    theirs_total = rows[0:1] + rows[1:2] + rows[2:3]
    return (
        (jnp.where(first, mine, theirs), jnp.where(first, mine_total, theirs_total)),
        (jnp.where(first, theirs, mine), jnp.where(first, theirs_total, mine_total)),
    )


def packed(state, total, out_ref):
    out_ref[0:128] = state.astype(BF16)
    out_ref[128:144] = rows_of_total(total, 16)


def unpacked(ref):
    rows = ref[128:144].astype(F32)
    return ref[0:128].astype(F32), rows[0:1] + rows[1:2] + rows[2:3]


def after(earlier, later):
    return jnp.exp(later[1]) * earlier[0] + later[0], earlier[1] + later[1]


def pair_kernel(kept_ref, kept_total_ref, got_ref, out_ref):
    packed(*after(*pair_of(kept_ref, kept_total_ref, got_ref)), out_ref)


def row_kernel(own_ref, one_ref, two_ref, three_ref, before_ref, before_total_ref, out_ref):
    me = lax.axis_index("x")
    pieces = [unpacked(r) for r in (own_ref, one_ref, two_ref, three_ref)]
    so_far = before = (jnp.zeros((128, 128), F32), jnp.zeros((1, 128), F32))
    for k in range(len(pieces)):
        before = tuple(jnp.where(me == k, new, old) for new, old in zip(so_far, before))
        back = lax.rem(me - k + len(pieces), len(pieces))
        here = pieces[0]
        for by in range(1, len(pieces)):
            here = tuple(jnp.where(back == by, new, old) for new, old in zip(pieces[by], here))
        so_far = after(so_far, here)
    before_ref[...] = before[0]
    before_total_ref[...] = jnp.broadcast_to(before[1], before_total_ref.shape)
    packed(*so_far, out_ref)


def two_kernel(own_ref, one_ref, out_ref):
    packed(*after(unpacked(one_ref), unpacked(own_ref)), out_ref)


def four_kernel(own_ref, one_ref, two_ref, before_ref, before_total_ref, out_ref):
    before = after(unpacked(two_ref), unpacked(one_ref))
    before_ref[...] = before[0]
    before_total_ref[...] = jnp.broadcast_to(before[1], before_total_ref.shape)
    packed(*after(before, unpacked(own_ref)), out_ref)


def entering_kernel(
    four_ref, rows_ref, rows_total_ref, row_ref, row_total_ref, kept_ref, kept_total_ref, got_ref, keep_ref, send_ref
):
    rows, row = (rows_ref[...], rows_total_ref[0:1]), (row_ref[...], row_total_ref[0:1])
    before = after(after(unpacked(four_ref), rows), row)
    later, _ = after(before, pair_of(kept_ref, kept_total_ref, got_ref)[0])
    first = lax.axis_index("c") == 0
    keep_ref[...] = jnp.where(first, before[0], later).astype(BF16)
    send_ref[...] = jnp.where(first, later, before[0]).astype(BF16)


def mixer_kernel(q_ref, decay_ref, gain_ref, gate_ref, weight_ref, inner_ref, keep_ref, got_ref, *refs):
    *outs, rows_ref = refs
    first = lax.axis_index("c") == 0
    col, _ = levels_of(decay_ref[...])
    keep, got = keep_ref[...], got_ref[...]
    entering = (jnp.where(first, keep, got), jnp.where(first, got, keep))
    heads = []
    for h in range(2):
        cols = slice(h * 128, h * 128 + 128)
        carried = jnp.exp(col[:, h : h + 1]) * dot(q_ref[:, cols], entering[h])
        kept = inner_ref[:, cols] + carried
        normed = kept * lax.rsqrt(jnp.mean(kept * kept, axis=-1, keepdims=True) + epsilon) * gain_ref[h : h + 1]
        gate = gate_ref[:, cols].astype(F32)
        heads.append((normed * (gate * jax.nn.sigmoid(gate))).astype(BF16).astype(F32))
    rows_ref[...] = jnp.concatenate(heads, axis=1)
    part = outs[0].shape[0]
    rows = jnp.concatenate([rows_ref[span(k, part)] for k in range(len(outs))], axis=0)
    for lo in range(0, weight_ref.shape[1], 512):
        out = dot(rows.astype(BF16), weight_ref[:, lo : lo + 512]).astype(BF16)
        for k, ref in enumerate(outs):
            ref[:, lo : lo + 512] = out[k * part : (k + 1) * part]


def mix_sum_kernel(mine, right, far, left, out):
    out[...] = sum(r[...].astype(F32) for r in (mine, right, far, left)).astype(BF16)


def shifted(x, axis, by):
    n = lax.axis_size(axis)
    return lax.ppermute(x, axis, [(i, (i + by) % n) for i in range(n)])


def brought(x, axis, by):
    return lax.ppermute(x, axis, [(i, i + by) for i in range(lax.axis_size(axis) - by)])


def across_chips(x):
    n = lax.axis_size(ZX)
    out = lax.all_to_all(x.reshape(n, -1, x.shape[-1]), ZX, split_axis=0, concat_axis=0, tiled=True)
    return out.reshape(x.shape)


def experts(rows, gate, up, down):
    half, part = rows.shape[0] // 2, rows.shape[1]
    hidden = gate.shape[1]
    piece, sums = array((half, part), BF16), [array((2 * half, hidden), F32)] * 2
    top, low = rows[:half], rows[half:]
    left_a, right_b = shifted(top, "tp", 1), shifted(low, "tp", -1)
    left_b, right_a = shifted(low, "tp", 1), shifted(top, "tp", -1)
    far_a, far_b = shifted(left_a, "tp", 1), shifted(right_b, "tp", -1)
    rows_of, cols_of = (part, hidden), (hidden, part)
    g, u, far_gate, far_up, far_down = call(
        near_kernel,
        sums + [array(rows_of, BF16)] * 2 + [array(cols_of, BF16)],
        rows,
        left_a,
        left_b,
        right_a,
        right_b,
        held=(gate, up, down),
        scratch_shapes=[pltpu.VMEM((3, *rows_of), BF16)] * 2 + [pltpu.SemaphoreType.DMA((9,))],
    )
    hid, to2a, to2b = call(
        far_kernel, [array((2 * half, hidden), BF16), piece, piece], far_a, far_b, g, u, far_gate, far_up, far_down
    )
    got_a, got_b = shifted(to2a, "tp", 1), shifted(to2b, "tp", -1)
    to1a, to1b, tom1a, tom1b, mine = call(
        rest_kernel,
        [piece] * 4 + [array((2 * half, part), BF16)],
        hid,
        held=(down,),
        scratch_shapes=[pltpu.VMEM((3, *cols_of), BF16), pltpu.SemaphoreType.DMA((3,))],
    )
    low_l, top_r = shifted(to1b, "tp", 1), shifted(tom1a, "tp", -1)
    to1a, tom1b = call(onward_kernel, [piece] * 2, to1a, tom1b, got_a, got_b)
    top_l, low_r = shifted(to1a, "tp", 1), shifted(tom1b, "tp", -1)
    return call(settle_kernel, array(rows.shape, BF16), mine, top_l, low_l, top_r, low_r)


def per_device(
    queries,
    key_rows,
    value_rows,
    out_gate,
    log_decay,
    head_gain,
    out_weight,
    moe_input,
    moe_gain,
    expert_gate,
    expert_up,
    expert_down,
    route_ids,
    route_weights,
):
    return layer(
        queries,
        key_rows,
        value_rows,
        out_gate,
        log_decay.T,
        head_gain,
        out_weight,
        moe_input,
        moe_gain.reshape(1, -1),
        expert_gate[0],
        expert_up[0],
        expert_down[0],
        route_ids.T,
        route_weights.T,
    )


def layer(q, k, v, out_gate, decay, head_gain, out_weight, x, gain, gate, up, down, ids, blend):
    tokens, width = x.shape
    part = width // lax.axis_size("tp")
    chips = lax.axis_size(ZX)
    capacity = 2 * ids.size // lax.axis_size(EP)
    rows = chips * capacity
    keep, send = call(
        functools.partial(dispatch_kernel, capacity), [array((rows, part), BF16)] * 2, ids, x, gain, plain=3
    )
    got = shifted(send, "c", 1)
    joined = call(join_kernel, array((chips, 2 * capacity, part), BF16), keep, got)
    arrived = across_chips(joined.reshape(-1, part))
    inner, kept, kept_total, state_send = call(
        inner_kernel,
        [array(q.shape, F32), array((128, 128), F32), array((8, 128), F32), array((144, 128), BF16)],
        q,
        k,
        v,
        decay,
        plain=4,
    )
    state_got = shifted(state_send, "c", 1)
    whole, state, total = array((144, 128), BF16), array((128, 128), F32), array((8, 128), F32)
    pair = call(pair_kernel, whole, kept, kept_total, state_got)
    around = [shifted(pair, "x", by) for by in (1, 2, 3)]
    row_before, row_total, row = call(row_kernel, [state, total, whole], pair, *around)
    one = brought(row, "z", 1)
    two = brought(call(two_kernel, whole, row, one), "z", 2)
    rows_before, rows_total, upto = call(four_kernel, [state, total, whole], row, one, two)
    ent_keep, ent_send = call(
        entering_kernel,
        [array((128, 128), BF16)] * 2,
        brought(upto, "z", 4),
        rows_before,
        rows_total,
        row_before,
        row_total,
        kept,
        kept_total,
        state_got,
    )
    ent_got = shifted(ent_send, "c", 1)
    mine, right, far, left = call(
        mixer_kernel,
        [array((q.shape[0] // 4, out_weight.shape[1]), BF16)] * 4,
        q,
        decay,
        head_gain,
        out_gate,
        out_weight,
        inner,
        ent_keep,
        ent_got,
        plain=5,
        scratch_shapes=[pltpu.VMEM(q.shape, F32)],
    )
    mixer_out = call(
        mix_sum_kernel,
        jax.ShapeDtypeStruct(mine.shape, BF16),
        mine,
        shifted(right, "tp", 1),
        shifted(far, "tp", 2),
        shifted(left, "tp", 3),
    )
    weights = call(
        functools.partial(blend_weights_kernel, capacity), array((2, 2, rows, tokens), BF16), ids, blend, plain=2
    )
    results = experts(arrived, gate, up, down)
    back = across_chips(results).reshape(chips, 2 * capacity, part)
    sent = call(parted_kernel, array((rows, part), BF16), back)
    expert_out = call(blend_kernel, jax.ShapeDtypeStruct((tokens, part), BF16), weights, back, shifted(sent, "c", 1))
    return mixer_out, expert_out


def solution(mesh):
    split = Mesh(mesh.devices.reshape(8, 4, 2, mesh.shape["tp"]), ("z", "x", "c", "tp"))
    return jax.shard_map(
        per_device,
        mesh=split,
        in_specs=(
            P(EP, "tp"),
            P(EP, "tp"),
            P(EP, "tp"),
            P(EP, "tp"),
            P(EP, "tp"),
            P("tp", None),
            P("tp", None),
            P(EP, None),
            P(),
            P(EP, None, "tp"),
            P(EP, None, "tp"),
            P(EP, "tp", None),
            P(EP, None),
            P(EP, None),
        ),
        out_specs=(P((*EP, "tp"), None), P(EP, "tp")),
        check_vma=False,
    )
```

time: 177 us -> 141 us (0.80)
  the two profiles are of different devices: /device:TPU:32 before, /device:TPU:1 now
where the time goes in v2:
time: 141 us
  starting transfers between devices  62 us (44%)
  waiting for transfers between devices  31.8 us (23%)
  blocking collectives  25.7 us (18%)
  Pallas kernels  20.5 us (15%)
    ppermute x22, starting transfers between devices, shifted(): return lax.ppermute(x, axis, [(i, (i + by) % n) for i in range(n)])  39.1 us
    ppermute x22, waiting for transfers between devices, shifted(): return lax.ppermute(x, axis, [(i, (i + by) % n) for i in range(n)])  28.7 us
    all_to_all x1, blocking collectives, across_chips(): lax.all_to_all(x.reshape(n, -1, x.shape[-1]), ZX, split_axis=0, concat_ax...  25.7 us
    pallas_call x18, Pallas kernels, call(): kernel(*hbm, *(pltpu.with_memory_space_constraint(a, pltpu.VMEM) for a in...  20.5 us
    ppermute x3, starting transfers between devices, brought(): lax.ppermute(x, axis, [(i, i + by) for i in range(lax.axis_size(axis) - b...  17.6 us
    all_to_all x1, starting transfers between devices, across_chips(): lax.all_to_all(x.reshape(n, -1, x.shape[-1]), ZX, split_axis=0, concat_ax...  5.35 us
    ppermute x3, waiting for transfers between devices, brought(): lax.ppermute(x, axis, [(i, i + by) for i in range(lax.axis_size(axis) - b...  3.13 us
  transfers between devices with their start and end apart: 26, of which 15 were waited for; matrix products, arithmetic and copies ran while one was open for 0% of the time, Pallas kernels for 11%

profile of v2, /device:TPU:1, one launch (start us, length us, event | category | flops | bytes accessed | tf_op | source)
XLA Modules:
  0.0 140.9 jit_solution(1088816878375576487)
XLA Ops:
  0.6 1.7 %shard_map.158 = (bf16[256,512]{1,0:T(8,128)(2,1)S(1)}, bf16[256,512]{1,0:T(8,128)(2,1)S(1)}) custom-call(s32[2,128]{1,0:T(2,128)} %bitcast.23, bf16[128,2048]{1,0:T(8,128)(2,1)} %x_ref.1, f32[1,2048]{1,0:T(1,128)} %bitcast.20), custom_call_target="tpu_custom_call" | custom-call | tf_op jit(solution)/shard_map/pallas_call | solution.py:50
  2.3 3.3 %collective-permute-start.11 = (bf16[256,512]{1,0:T(8,128)(2,1)S(1)}, bf16[256,512]{1,0:T(8,128)(2,1)S(1)}, u32[]{:S(2)}, u32[]{:S(2)}) collective-permute-start(bf16[256,512]{1,0:T(8,128)(2,1)S(1)} %get-tuple-element.52), channel_id=1, source_target_pairs={{0,4},{4,0},{1,5},{5,1},{2,6},{6,2},{3,7},{7,3},{8,12},{12,8},{9,1... | collective-permute-start | bytes 786440 | tf_op jit(solution)/shard_map/ppermute | solution.py:322
  5.6 1.2 collective-permute-done.11.got_ref
  6.8 25.7 %all_to_all.10 = bf16[32,16,512]{2,1,0:T(8,128)(2,1)S(1)} all-to-all(bf16[32,16,512]{2,1,0:T(8,128)(2,1)S(1)} %shard_map.159), channel_id=1, replica_groups=mesh['z'=8,'x'=4,'c'=2,'tp'=4] {'z','x'}, dimensions={0} | all-to-all | bytes 1048576 | tf_op jit(solution)/shard_map/all_to_all | solution.py:331
  32.6 1.4 collective-permute-start.12
  34.0 1.5 %collective-permute-start.14 = (bf16[256,512]{1,0:T(8,128)(2,1)S(1)}, bf16[256,512]{1,0:T(8,128)(2,1)S(1)}, u32[]{:S(2)}, u32[]{:S(2)}) collective-permute-start(bf16[256,512]{1,0:T(8,128)(2,1)S(1)} %bitcast.18), channel_id=1, source_target_pairs={{0,3},{1,0},{2,1},{3,2},{4,7},{5,4},{6,5},{7,6},{8,11},{9,8},{10,9... | collective-permute-start | bytes 786440 | tf_op jit(solution)/shard_map/ppermute | solution.py:322
  35.5 0.0 collective-permute-start.16
  35.5 2.7 %collective-permute-start.17 = (bf16[256,512]{1,0:T(8,128)(2,1)S(1)}, bf16[256,512]{1,0:T(8,128)(2,1)S(1)}, u32[]{:S(2)}, u32[]{:S(2)}) collective-permute-start(bf16[256,512]{1,0:T(8,128)(2,1)S(1)} %bitcast.17), channel_id=1, source_target_pairs={{0,3},{1,0},{2,1},{3,2},{4,7},{5,4},{6,5},{7,6},{8,11},{9,8},{10,9... | collective-permute-start | bytes 786440 | tf_op jit(solution)/shard_map/ppermute | solution.py:322
  38.2 1.6 %collective-permute-done.12.left_a = bf16[256,512]{1,0:T(8,128)(2,1)S(1)} collective-permute-done((bf16[256,512]{1,0:T(8,128)(2,1)S(1)}, bf16[256,512]{1,0:T(8,128)(2,1)S(1)}, u32[]{:S(2)}, u32[]{:S(2)}) %collective-permute-start.12) | collective-permute-done | bytes 262176 | tf_op jit(solution)/shard_map/ppermute | solution.py:322
  39.7 0.0 collective-permute-start.13
  39.7 0.0 collective-permute-done.14.right_b
  39.7 2.7 %collective-permute-start.15 = (bf16[256,512]{1,0:T(8,128)(2,1)S(1)}, bf16[256,512]{1,0:T(8,128)(2,1)S(1)}, u32[]{:S(2)}, u32[]{:S(2)}) collective-permute-start(bf16[256,512]{1,0:T(8,128)(2,1)S(1)} %collective-permute-done.14.right_b), channel_id=1, source_target_pairs={{0,3},{1,0},{2,1},{3,2},{4,7},{5,4},{6,5},{7,6},{8,11},{9,8},{10,9... | collective-permute-start | bytes 786440 | tf_op jit(solution)/shard_map/ppermute | solution.py:322
  42.4 2.9 %collective-permute-done.16.left_b = bf16[256,512]{1,0:T(8,128)(2,1)S(1)} collective-permute-done((bf16[256,512]{1,0:T(8,128)(2,1)S(1)}, bf16[256,512]{1,0:T(8,128)(2,1)S(1)}, u32[]{:S(2)}, u32[]{:S(2)}) %collective-permute-start.16) | collective-permute-done | bytes 262176 | tf_op jit(solution)/shard_map/ppermute | solution.py:322
  45.3 0.0 collective-permute-done.17.right_a
  45.3 5.5 %shard_map.160 = (f32[512,896]{1,0:T(8,128)S(1)}, f32[512,896]{1,0:T(8,128)S(1)}, bf16[512,896]{1,0:T(8,128)(2,1)S(1)}, bf16[512,896]{1,0:T(8,128)(2,1)S(1)}, bf16[896,512]{1,0:T(8,128)(2,1)S(1)}) custom-call(bf16[2048,896]{1,0:T(8,128)(2,1)} %bitcast.14, bf16[2048,896]{1,0:T(8,128)(2,1)} %bitcast.15, bf16[896,2048]{1,0:T(8,128)(2,1)} %bitcast.12, ...), custom_call_target="tpu_custom_call" | custom-call | tf_op jit(solution)/shard_map/pallas_call | solution.py:50
  50.8 0.1 collective-permute-done.13.far_a
  51.0 0.0 collective-permute-done.15.far_b
  51.0 1.8 %shard_map.161 = (bf16[512,896]{1,0:T(8,128)(2,1)S(1)}, bf16[256,512]{1,0:T(8,128)(2,1)S(1)}, bf16[256,512]{1,0:T(8,128)(2,1)S(1)}) custom-call(bf16[256,512]{1,0:T(8,128)(2,1)S(1)} %collective-permute-done.13.far_a, bf16[256,512]{1,0:T(8,128)(2,1)S(1)} %collective-permute-done.15.far_b, f32[512,896]{1,0:T(8,128)S(1)} %get-tuple-element.53.g_in, ...), custom_call_target="tpu_custom_call" | custom-call | tf_op jit(solution)/shard_map/pallas_call | solution.py:50
  52.8 1.0 collective-permute-start.18
  53.8 1.9 %collective-permute-start.19 = (bf16[256,512]{1,0:T(8,128)(2,1)S(1)}, bf16[256,512]{1,0:T(8,128)(2,1)S(1)}, u32[]{:S(2)}, u32[]{:S(2)}) collective-permute-start(bf16[256,512]{1,0:T(8,128)(2,1)S(1)} %get-tuple-element.63), channel_id=1, source_target_pairs={{0,3},{1,0},{2,1},{3,2},{4,7},{5,4},{6,5},{7,6},{8,11},{9,8},{10,9... | collective-permute-start | bytes 786440 | tf_op jit(solution)/shard_map/ppermute | solution.py:322
  55.7 3.3 %shard_map.162 = (bf16[256,512]{1,0:T(8,128)(2,1)S(1)}, bf16[256,512]{1,0:T(8,128)(2,1)S(1)}, bf16[256,512]{1,0:T(8,128)(2,1)S(1)}, bf16[256,512]{1,0:T(8,128)(2,1)S(1)}, bf16[512,512]{1,0:T(8,128)(2,1)S(1)}) custom-call(bf16[896,2048]{1,0:T(8,128)(2,1)} %bitcast.13, bf16[512,896]{1,0:T(8,128)(2,1)S(1)} %get-tuple-element.58.hid), custom_call_target="tpu_custom_call" | custom-call | tf_op jit(solution)/shard_map/pallas_call | solution.py:50
  59.0 0.1 collective-permute-start.21
  59.1 2.7 %collective-permute-start.22 = (bf16[256,512]{1,0:T(8,128)(2,1)S(1)}, bf16[256,512]{1,0:T(8,128)(2,1)S(1)}, u32[]{:S(2)}, u32[]{:S(2)}) collective-permute-start(bf16[256,512]{1,0:T(8,128)(2,1)S(1)} %get-tuple-element.66), channel_id=1, source_target_pairs={{0,3},{1,0},{2,1},{3,2},{4,7},{5,4},{6,5},{7,6},{8,11},{9,8},{10,9... | collective-permute-start | bytes 786440 | tf_op jit(solution)/shard_map/ppermute | solution.py:322
  61.8 0.0 collective-permute-done.18.got_a
  61.8 0.0 collective-permute-done.19.got_b
  61.8 0.1 shard_map.163
  61.9 0.1 collective-permute-start.20
  62.0 2.7 %collective-permute-start.23 = (bf16[256,512]{1,0:T(8,128)(2,1)S(1)}, bf16[256,512]{1,0:T(8,128)(2,1)S(1)}, u32[]{:S(2)}, u32[]{:S(2)}) collective-permute-start(bf16[256,512]{1,0:T(8,128)(2,1)S(1)} %get-tuple-element.67), channel_id=1, source_target_pairs={{0,3},{1,0},{2,1},{3,2},{4,7},{5,4},{6,5},{7,6},{8,11},{9,8},{10,9... | collective-permute-start | bytes 786440 | tf_op jit(solution)/shard_map/ppermute | solution.py:322
  64.6 3.7 %collective-permute-done.21.low_l = bf16[256,512]{1,0:T(8,128)(2,1)S(1)} collective-permute-done((bf16[256,512]{1,0:T(8,128)(2,1)S(1)}, bf16[256,512]{1,0:T(8,128)(2,1)S(1)}, u32[]{:S(2)}, u32[]{:S(2)}) %collective-permute-start.21) | collective-permute-done | bytes 262176 | tf_op jit(solution)/shard_map/ppermute | solution.py:322
  68.4 0.0 collective-permute-done.22.top_r
  68.4 4.7 %collective-permute-done.20.top_l = bf16[256,512]{1,0:T(8,128)(2,1)S(1)} collective-permute-done((bf16[256,512]{1,0:T(8,128)(2,1)S(1)}, bf16[256,512]{1,0:T(8,128)(2,1)S(1)}, u32[]{:S(2)}, u32[]{:S(2)}) %collective-permute-start.20) | collective-permute-done | bytes 262176 | tf_op jit(solution)/shard_map/ppermute | solution.py:322
  73.1 0.0 collective-permute-done.23.low_r
  73.1 1.0 shard_map.164
  74.1 5.3 %all-to-all-start.1 = ((bf16[32,16,512]{2,1,0:T(8,128)(2,1)}), bf16[32,16,512]{2,1,0:T(8,128)(2,1)S(1)}, u32[]{:S(2)}, u32[]{:S(2)}) async-start(bf16[32,16,512]{2,1,0:T(8,128)(2,1)} %bitcast.10), calls=%async_computation.1 | async-start | bytes 1048576 | tf_op jit(solution)/shard_map/all_to_all | solution.py:331
  79.4 1.8 %shard_map.149 = (f32[256,256]{1,0:T(8,128)S(1)}, f32[128,128]{1,0:T(8,128)S(1)}, f32[8,128]{1,0:T(8,128)S(1)}, bf16[144,128]{1,0:T(8,128)(2,1)S(1)}) custom-call(bf16[256,256]{1,0:T(8,128)(2,1)} %q_ref.3, bf16[256,256]{1,0:T(8,128)(2,1)} %k_ref.1, bf16[256,256]{1,0:T(8,128)(2,1)} %v_ref.1, f32[2,256]{1,0:T(2,128)} %bitcast.21), custom_call_target="tpu_custom_call" | custom-call | tf_op jit(solution)/shard_map/pallas_call | solution.py:50
  81.2 3.6 %collective-permute-start = (bf16[144,128]{1,0:T(8,128)(2,1)S(1)}, bf16[144,128]{1,0:T(8,128)(2,1)S(1)}, u32[]{:S(2)}, u32[]{:S(2)}) collective-permute-start(bf16[144,128]{1,0:T(8,128)(2,1)S(1)} %get-tuple-element.38), channel_id=1, source_target_pairs={{0,4},{4,0},{1,5},{5,1},{2,6},{6,2},{3,7},{7,3},{8,12},{12,8},{9,1... | collective-permute-start | bytes 110600 | tf_op jit(solution)/shard_map/ppermute | solution.py:322
  84.8 0.9 collective-permute-done.got_ref
  85.7 1.6 %collective-permute-start.1 = (bf16[144,128]{1,0:T(8,128)(2,1)S(1)}, bf16[144,128]{1,0:T(8,128)(2,1)S(1)}, u32[]{:S(2)}, u32[]{:S(2)}) collective-permute-start(bf16[144,128]{1,0:T(8,128)(2,1)S(1)} %shard_map.150.own_ref), channel_id=1, source_target_pairs={{0,8},{8,16},{16,24},{24,0},{1,9},{9,17},{17,25},{25,1},{2,10},{10... | collective-permute-start | bytes 110600 | tf_op jit(solution)/shard_map/ppermute | solution.py:322
  87.3 2.4 %collective-permute-start.2 = (bf16[144,128]{1,0:T(8,128)(2,1)S(1)}, bf16[144,128]{1,0:T(8,128)(2,1)S(1)}, u32[]{:S(2)}, u32[]{:S(2)}) collective-permute-start(bf16[144,128]{1,0:T(8,128)(2,1)S(1)} %shard_map.150.own_ref), channel_id=1, source_target_pairs={{0,16},{8,24},{16,0},{24,8},{1,17},{9,25},{17,1},{25,9},{2,18},{10... | collective-permute-start | bytes 110600 | tf_op jit(solution)/shard_map/ppermute | solution.py:322
  89.7 1.2 collective-permute-start.3
  90.9 0.0 collective-permute-done.1.one_ref
  90.9 1.6 %collective-permute-done.2.two_ref = bf16[144,128]{1,0:T(8,128)(2,1)S(1)} collective-permute-done((bf16[144,128]{1,0:T(8,128)(2,1)S(1)}, bf16[144,128]{1,0:T(8,128)(2,1)S(1)}, u32[]{:S(2)}, u32[]{:S(2)}) %collective-permute-start.2) | collective-permute-done | bytes 36896 | tf_op jit(solution)/shard_map/ppermute | solution.py:322
  92.6 0.3 collective-permute-done.3.three_ref
  92.9 0.1 shard_map.151
  93.0 4.0 %collective-permute-start.4 = (bf16[144,128]{1,0:T(8,128)(2,1)S(1)}, bf16[144,128]{1,0:T(8,128)(2,1)S(1)}, u32[]{:S(2)}, u32[]{:S(2)}) collective-permute-start(bf16[144,128]{1,0:T(8,128)(2,1)S(1)} %get-tuple-element.39.own_ref), channel_id=1, source_target_pairs={{0,32},{32,64},{64,96},{96,128},{128,160},{160,192},{192,224},{1,3... | collective-permute-start | bytes 110600 | tf_op jit(solution)/shard_map/ppermute | solution.py:326
  97.0 1.0 collective-permute-done.4.one_ref
  98.0 3.7 %collective-permute-start.5 = (bf16[144,128]{1,0:T(8,128)(2,1)S(1)}, bf16[144,128]{1,0:T(8,128)(2,1)S(1)}, u32[]{:S(2)}, u32[]{:S(2)}) collective-permute-start(bf16[144,128]{1,0:T(8,128)(2,1)S(1)} %shard_map.152), channel_id=1, source_target_pairs={{0,64},{32,96},{64,128},{96,160},{128,192},{160,224},{1,65},{33,97... | collective-permute-start | bytes 110600 | tf_op jit(solution)/shard_map/ppermute | solution.py:326
  101.7 1.0 collective-permute-done.5.two_ref
  102.8 9.9 %collective-permute-start.6 = (bf16[144,128]{1,0:T(8,128)(2,1)S(1)}, bf16[144,128]{1,0:T(8,128)(2,1)S(1)}, u32[]{:S(2)}, u32[]{:S(2)}) collective-permute-start(bf16[144,128]{1,0:T(8,128)(2,1)S(1)} %get-tuple-element.40), channel_id=1, source_target_pairs={{0,128},{32,160},{64,192},{96,224},{1,129},{33,161},{65,193},{97,2... | collective-permute-start | bytes 110600 | tf_op jit(solution)/shard_map/ppermute | solution.py:326
  112.7 1.0 collective-permute-done.6.four_ref
  113.8 5.0 %collective-permute-start.7 = (bf16[128,128]{1,0:T(8,128)(2,1)S(1)}, bf16[128,128]{1,0:T(8,128)(2,1)S(1)}, u32[]{:S(2)}, u32[]{:S(2)}) collective-permute-start(bf16[128,128]{1,0:T(8,128)(2,1)S(1)} %get-tuple-element.46), channel_id=1, source_target_pairs={{0,4},{4,0},{1,5},{5,1},{2,6},{6,2},{3,7},{7,3},{8,12},{12,8},{9,1... | collective-permute-start | bytes 98312 | tf_op jit(solution)/shard_map/ppermute | solution.py:322
  118.8 0.9 collective-permute-done.7.got_ref
  119.7 2.3 %shard_map.155 = (bf16[64,2048]{1,0:T(8,128)(2,1)S(1)}, bf16[64,2048]{1,0:T(8,128)(2,1)S(1)}, bf16[64,2048]{1,0:T(8,128)(2,1)S(1)}, bf16[64,2048]{1,0:T(8,128)(2,1)S(1)}) custom-call(bf16[256,256]{1,0:T(8,128)(2,1)} %q_ref.3, f32[2,256]{1,0:T(2,128)} %bitcast.22, f32[2,128]{1,0:T(2,128)} %gain_ref.1, bf16[256,256]{1,0:T(8,128)(2,1)} %gate_ref.1, ...), custom_call_target="tpu_custom_call" | custom-call | tf_op jit(solution)/shard_map/pallas_call | solution.py:50
  122.0 3.0 %collective-permute-start.10 = (bf16[64,2048]{1,0:T(8,128)(2,1)S(1)}, bf16[64,2048]{1,0:T(8,128)(2,1)S(1)}, u32[]{:S(2)}, u32[]{:S(2)}) collective-permute-start(bf16[64,2048]{1,0:T(8,128)(2,1)S(1)} %get-tuple-element.50), channel_id=1, source_target_pairs={{0,3},{1,0},{2,1},{3,2},{4,7},{5,4},{6,5},{7,6},{8,11},{9,8},{10,9... | collective-permute-start | bytes 786440 | tf_op jit(solution)/shard_map/ppermute | solution.py:322
  125.0 0.0 collective-permute-start.8
  125.0 1.3 collective-permute-start.9
  126.3 0.0 all-to-all-done.1.back_ref
  126.3 1.0 collective-permute-start.24
  127.3 1.0 shard_map.157.w_ref
  128.2 7.5 %collective-permute-done.10.left = bf16[64,2048]{1,0:T(8,128)(2,1)S(1)} collective-permute-done((bf16[64,2048]{1,0:T(8,128)(2,1)S(1)}, bf16[64,2048]{1,0:T(8,128)(2,1)S(1)}, u32[]{:S(2)}, u32[]{:S(2)}) %collective-permute-start.10) | collective-permute-done | bytes 262176 | tf_op jit(solution)/shard_map/ppermute | solution.py:322
  135.8 3.3 %collective-permute-done.8.right = bf16[64,2048]{1,0:T(8,128)(2,1)S(1)} collective-permute-done((bf16[64,2048]{1,0:T(8,128)(2,1)S(1)}, bf16[64,2048]{1,0:T(8,128)(2,1)S(1)}, u32[]{:S(2)}, u32[]{:S(2)}) %collective-permute-start.8) | collective-permute-done | bytes 262176 | tf_op jit(solution)/shard_map/ppermute | solution.py:322
  139.1 0.0 collective-permute-done.9.far
  139.1 0.8 shard_map.156
  139.9 1.0 shard_map.166
  (8 shorter events, 0.2 us)
Async XLA Ops:
  2.3 4.5 %collective-permute-start.11 = (bf16[256,512]{1,0:T(8,128)(2,1)S(1)}, bf16[256,512]{1,0:T(8,128)(2,1)S(1)}, u32[]{:S(2)}, u32[]{:S(2)}) collective-permute-start(bf16[256,512]{1,0:T(8,128)(2,1)S(1)} %get-tuple-element.52), channel_id=1, source_target_pairs={{0,4},{4,0},{1,5},{5,1},{2,6},{6,2},{3,7},{7,3},{8,12},{12,8},{9,1... | collective-permute-start | bytes 786440 | tf_op jit(solution)/shard_map/ppermute | solution.py:322
  32.6 7.1 %collective-permute-start.12 = (bf16[256,512]{1,0:T(8,128)(2,1)S(1)}, bf16[256,512]{1,0:T(8,128)(2,1)S(1)}, u32[]{:S(2)}, u32[]{:S(2)}) collective-permute-start(bf16[256,512]{1,0:T(8,128)(2,1)S(1)} %bitcast.16), channel_id=1, source_target_pairs={{0,1},{1,2},{2,3},{3,0},{4,5},{5,6},{6,7},{7,4},{8,9},{9,10},{10,1... | collective-permute-start | bytes 786440 | tf_op jit(solution)/shard_map/ppermute | solution.py:322
  34.0 5.8 %collective-permute-start.14 = (bf16[256,512]{1,0:T(8,128)(2,1)S(1)}, bf16[256,512]{1,0:T(8,128)(2,1)S(1)}, u32[]{:S(2)}, u32[]{:S(2)}) collective-permute-start(bf16[256,512]{1,0:T(8,128)(2,1)S(1)} %bitcast.18), channel_id=1, source_target_pairs={{0,3},{1,0},{2,1},{3,2},{4,7},{5,4},{6,5},{7,6},{8,11},{9,8},{10,9... | collective-permute-start | bytes 786440 | tf_op jit(solution)/shard_map/ppermute | solution.py:322
  35.5 9.9 %collective-permute-start.16 = (bf16[256,512]{1,0:T(8,128)(2,1)S(1)}, bf16[256,512]{1,0:T(8,128)(2,1)S(1)}, u32[]{:S(2)}, u32[]{:S(2)}) collective-permute-start(bf16[256,512]{1,0:T(8,128)(2,1)S(1)} %bitcast.19), channel_id=1, source_target_pairs={{0,1},{1,2},{2,3},{3,0},{4,5},{5,6},{6,7},{7,4},{8,9},{9,10},{10,1... | collective-permute-start | bytes 786440 | tf_op jit(solution)/shard_map/ppermute | solution.py:322
  35.5 9.9 %collective-permute-start.17 = (bf16[256,512]{1,0:T(8,128)(2,1)S(1)}, bf16[256,512]{1,0:T(8,128)(2,1)S(1)}, u32[]{:S(2)}, u32[]{:S(2)}) collective-permute-start(bf16[256,512]{1,0:T(8,128)(2,1)S(1)} %bitcast.17), channel_id=1, source_target_pairs={{0,3},{1,0},{2,1},{3,2},{4,7},{5,4},{6,5},{7,6},{8,11},{9,8},{10,9... | collective-permute-start | bytes 786440 | tf_op jit(solution)/shard_map/ppermute | solution.py:322
  39.7 11.2 %collective-permute-start.13 = (bf16[256,512]{1,0:T(8,128)(2,1)S(1)}, bf16[256,512]{1,0:T(8,128)(2,1)S(1)}, u32[]{:S(2)}, u32[]{:S(2)}) collective-permute-start(bf16[256,512]{1,0:T(8,128)(2,1)S(1)} %collective-permute-done.12.left_a), channel_id=1, source_target_pairs={{0,1},{1,2},{2,3},{3,0},{4,5},{5,6},{6,7},{7,4},{8,9},{9,10},{10,1... | collective-permute-start | bytes 786440 | tf_op jit(solution)/shard_map/ppermute | solution.py:322
  39.7 11.2 %collective-permute-start.15 = (bf16[256,512]{1,0:T(8,128)(2,1)S(1)}, bf16[256,512]{1,0:T(8,128)(2,1)S(1)}, u32[]{:S(2)}, u32[]{:S(2)}) collective-permute-start(bf16[256,512]{1,0:T(8,128)(2,1)S(1)} %collective-permute-done.14.right_b), channel_id=1, source_target_pairs={{0,3},{1,0},{2,1},{3,2},{4,7},{5,4},{6,5},{7,6},{8,11},{9,8},{10,9... | collective-permute-start | bytes 786440 | tf_op jit(solution)/shard_map/ppermute | solution.py:322
  52.8 9.0 %collective-permute-start.18 = (bf16[256,512]{1,0:T(8,128)(2,1)S(1)}, bf16[256,512]{1,0:T(8,128)(2,1)S(1)}, u32[]{:S(2)}, u32[]{:S(2)}) collective-permute-start(bf16[256,512]{1,0:T(8,128)(2,1)S(1)} %get-tuple-element.62), channel_id=1, source_target_pairs={{0,1},{1,2},{2,3},{3,0},{4,5},{5,6},{6,7},{7,4},{8,9},{9,10},{10,1... | collective-permute-start | bytes 786440 | tf_op jit(solution)/shard_map/ppermute | solution.py:322
  53.8 8.0 %collective-permute-start.19 = (bf16[256,512]{1,0:T(8,128)(2,1)S(1)}, bf16[256,512]{1,0:T(8,128)(2,1)S(1)}, u32[]{:S(2)}, u32[]{:S(2)}) collective-permute-start(bf16[256,512]{1,0:T(8,128)(2,1)S(1)} %get-tuple-element.63), channel_id=1, source_target_pairs={{0,3},{1,0},{2,1},{3,2},{4,7},{5,4},{6,5},{7,6},{8,11},{9,8},{10,9... | collective-permute-start | bytes 786440 | tf_op jit(solution)/shard_map/ppermute | solution.py:322
  59.0 9.4 %collective-permute-start.21 = (bf16[256,512]{1,0:T(8,128)(2,1)S(1)}, bf16[256,512]{1,0:T(8,128)(2,1)S(1)}, u32[]{:S(2)}, u32[]{:S(2)}) collective-permute-start(bf16[256,512]{1,0:T(8,128)(2,1)S(1)} %get-tuple-element.65), channel_id=1, source_target_pairs={{0,1},{1,2},{2,3},{3,0},{4,5},{5,6},{6,7},{7,4},{8,9},{9,10},{10,1... | collective-permute-start | bytes 786440 | tf_op jit(solution)/shard_map/ppermute | solution.py:322
  59.1 9.3 %collective-permute-start.22 = (bf16[256,512]{1,0:T(8,128)(2,1)S(1)}, bf16[256,512]{1,0:T(8,128)(2,1)S(1)}, u32[]{:S(2)}, u32[]{:S(2)}) collective-permute-start(bf16[256,512]{1,0:T(8,128)(2,1)S(1)} %get-tuple-element.66), channel_id=1, source_target_pairs={{0,3},{1,0},{2,1},{3,2},{4,7},{5,4},{6,5},{7,6},{8,11},{9,8},{10,9... | collective-permute-start | bytes 786440 | tf_op jit(solution)/shard_map/ppermute | solution.py:322
  61.9 11.2 %collective-permute-start.20 = (bf16[256,512]{1,0:T(8,128)(2,1)S(1)}, bf16[256,512]{1,0:T(8,128)(2,1)S(1)}, u32[]{:S(2)}, u32[]{:S(2)}) collective-permute-start(bf16[256,512]{1,0:T(8,128)(2,1)S(1)} %get-tuple-element.64), channel_id=1, source_target_pairs={{0,1},{1,2},{2,3},{3,0},{4,5},{5,6},{6,7},{7,4},{8,9},{9,10},{10,1... | collective-permute-start | bytes 786440 | tf_op jit(solution)/shard_map/ppermute | solution.py:322
  62.0 11.1 %collective-permute-start.23 = (bf16[256,512]{1,0:T(8,128)(2,1)S(1)}, bf16[256,512]{1,0:T(8,128)(2,1)S(1)}, u32[]{:S(2)}, u32[]{:S(2)}) collective-permute-start(bf16[256,512]{1,0:T(8,128)(2,1)S(1)} %get-tuple-element.67), channel_id=1, source_target_pairs={{0,3},{1,0},{2,1},{3,2},{4,7},{5,4},{6,5},{7,6},{8,11},{9,8},{10,9... | collective-permute-start | bytes 786440 | tf_op jit(solution)/shard_map/ppermute | solution.py:322
  74.1 52.2 %all-to-all-start.1 = ((bf16[32,16,512]{2,1,0:T(8,128)(2,1)}), bf16[32,16,512]{2,1,0:T(8,128)(2,1)S(1)}, u32[]{:S(2)}, u32[]{:S(2)}) async-start(bf16[32,16,512]{2,1,0:T(8,128)(2,1)} %bitcast.10), calls=%async_computation.1 | async-start | bytes 1048576 | tf_op jit(solution)/shard_map/all_to_all | solution.py:331
  81.2 4.5 %collective-permute-start = (bf16[144,128]{1,0:T(8,128)(2,1)S(1)}, bf16[144,128]{1,0:T(8,128)(2,1)S(1)}, u32[]{:S(2)}, u32[]{:S(2)}) collective-permute-start(bf16[144,128]{1,0:T(8,128)(2,1)S(1)} %get-tuple-element.38), channel_id=1, source_target_pairs={{0,4},{4,0},{1,5},{5,1},{2,6},{6,2},{3,7},{7,3},{8,12},{12,8},{9,1... | collective-permute-start | bytes 110600 | tf_op jit(solution)/shard_map/ppermute | solution.py:322
  85.7 5.2 %collective-permute-start.1 = (bf16[144,128]{1,0:T(8,128)(2,1)S(1)}, bf16[144,128]{1,0:T(8,128)(2,1)S(1)}, u32[]{:S(2)}, u32[]{:S(2)}) collective-permute-start(bf16[144,128]{1,0:T(8,128)(2,1)S(1)} %shard_map.150.own_ref), channel_id=1, source_target_pairs={{0,8},{8,16},{16,24},{24,0},{1,9},{9,17},{17,25},{25,1},{2,10},{10... | collective-permute-start | bytes 110600 | tf_op jit(solution)/shard_map/ppermute | solution.py:322
  87.3 5.2 %collective-permute-start.2 = (bf16[144,128]{1,0:T(8,128)(2,1)S(1)}, bf16[144,128]{1,0:T(8,128)(2,1)S(1)}, u32[]{:S(2)}, u32[]{:S(2)}) collective-permute-start(bf16[144,128]{1,0:T(8,128)(2,1)S(1)} %shard_map.150.own_ref), channel_id=1, source_target_pairs={{0,16},{8,24},{16,0},{24,8},{1,17},{9,25},{17,1},{25,9},{2,18},{10... | collective-permute-start | bytes 110600 | tf_op jit(solution)/shard_map/ppermute | solution.py:322
  89.7 3.1 %collective-permute-start.3 = (bf16[144,128]{1,0:T(8,128)(2,1)S(1)}, bf16[144,128]{1,0:T(8,128)(2,1)S(1)}, u32[]{:S(2)}, u32[]{:S(2)}) collective-permute-start(bf16[144,128]{1,0:T(8,128)(2,1)S(1)} %shard_map.150.own_ref), channel_id=1, source_target_pairs={{0,24},{8,0},{16,8},{24,16},{1,25},{9,1},{17,9},{25,17},{2,26},{10... | collective-permute-start | bytes 110600 | tf_op jit(solution)/shard_map/ppermute | solution.py:322
  93.0 5.0 %collective-permute-start.4 = (bf16[144,128]{1,0:T(8,128)(2,1)S(1)}, bf16[144,128]{1,0:T(8,128)(2,1)S(1)}, u32[]{:S(2)}, u32[]{:S(2)}) collective-permute-start(bf16[144,128]{1,0:T(8,128)(2,1)S(1)} %get-tuple-element.39.own_ref), channel_id=1, source_target_pairs={{0,32},{32,64},{64,96},{96,128},{128,160},{160,192},{192,224},{1,3... | collective-permute-start | bytes 110600 | tf_op jit(solution)/shard_map/ppermute | solution.py:326
  98.0 4.8 %collective-permute-start.5 = (bf16[144,128]{1,0:T(8,128)(2,1)S(1)}, bf16[144,128]{1,0:T(8,128)(2,1)S(1)}, u32[]{:S(2)}, u32[]{:S(2)}) collective-permute-start(bf16[144,128]{1,0:T(8,128)(2,1)S(1)} %shard_map.152), channel_id=1, source_target_pairs={{0,64},{32,96},{64,128},{96,160},{128,192},{160,224},{1,65},{33,97... | collective-permute-start | bytes 110600 | tf_op jit(solution)/shard_map/ppermute | solution.py:326
  102.8 10.9 %collective-permute-start.6 = (bf16[144,128]{1,0:T(8,128)(2,1)S(1)}, bf16[144,128]{1,0:T(8,128)(2,1)S(1)}, u32[]{:S(2)}, u32[]{:S(2)}) collective-permute-start(bf16[144,128]{1,0:T(8,128)(2,1)S(1)} %get-tuple-element.40), channel_id=1, source_target_pairs={{0,128},{32,160},{64,192},{96,224},{1,129},{33,161},{65,193},{97,2... | collective-permute-start | bytes 110600 | tf_op jit(solution)/shard_map/ppermute | solution.py:326
  113.8 5.9 %collective-permute-start.7 = (bf16[128,128]{1,0:T(8,128)(2,1)S(1)}, bf16[128,128]{1,0:T(8,128)(2,1)S(1)}, u32[]{:S(2)}, u32[]{:S(2)}) collective-permute-start(bf16[128,128]{1,0:T(8,128)(2,1)S(1)} %get-tuple-element.46), channel_id=1, source_target_pairs={{0,4},{4,0},{1,5},{5,1},{2,6},{6,2},{3,7},{7,3},{8,12},{12,8},{9,1... | collective-permute-start | bytes 98312 | tf_op jit(solution)/shard_map/ppermute | solution.py:322
  122.0 13.8 %collective-permute-start.10 = (bf16[64,2048]{1,0:T(8,128)(2,1)S(1)}, bf16[64,2048]{1,0:T(8,128)(2,1)S(1)}, u32[]{:S(2)}, u32[]{:S(2)}) collective-permute-start(bf16[64,2048]{1,0:T(8,128)(2,1)S(1)} %get-tuple-element.50), channel_id=1, source_target_pairs={{0,3},{1,0},{2,1},{3,2},{4,7},{5,4},{6,5},{7,6},{8,11},{9,8},{10,9... | collective-permute-start | bytes 786440 | tf_op jit(solution)/shard_map/ppermute | solution.py:322
  125.0 14.1 %collective-permute-start.8 = (bf16[64,2048]{1,0:T(8,128)(2,1)S(1)}, bf16[64,2048]{1,0:T(8,128)(2,1)S(1)}, u32[]{:S(2)}, u32[]{:S(2)}) collective-permute-start(bf16[64,2048]{1,0:T(8,128)(2,1)S(1)} %get-tuple-element.48), channel_id=1, source_target_pairs={{0,1},{1,2},{2,3},{3,0},{4,5},{5,6},{6,7},{7,4},{8,9},{9,10},{10,1... | collective-permute-start | bytes 786440 | tf_op jit(solution)/shard_map/ppermute | solution.py:322
  125.0 14.1 %collective-permute-start.9 = (bf16[64,2048]{1,0:T(8,128)(2,1)S(1)}, bf16[64,2048]{1,0:T(8,128)(2,1)S(1)}, u32[]{:S(2)}, u32[]{:S(2)}) collective-permute-start(bf16[64,2048]{1,0:T(8,128)(2,1)S(1)} %get-tuple-element.49), channel_id=1, source_target_pairs={{0,2},{1,3},{2,0},{3,1},{4,6},{5,7},{6,4},{7,5},{8,10},{9,11},{10,... | collective-permute-start | bytes 786440 | tf_op jit(solution)/shard_map/ppermute | solution.py:322
  126.3 13.6 %collective-permute-start.24 = (bf16[256,512]{1,0:T(8,128)(2,1)S(1)}, bf16[256,512]{1,0:T(8,128)(2,1)S(1)}, u32[]{:S(2)}, u32[]{:S(2)}) collective-permute-start(bf16[256,512]{1,0:T(8,128)(2,1)S(1)} %shard_map.165), channel_id=1, source_target_pairs={{0,4},{4,0},{1,5},{5,1},{2,6},{6,2},{3,7},{7,3},{8,12},{12,8},{9,1... | collective-permute-start | bytes 786440 | tf_op jit(solution)/shard_map/ppermute | solution.py:322

commit v3 on v2

--- a/solution.py
+++ b/solution.py
@@ -116,7 +116,7 @@
     return copies
 
 
-def near_kernel(gate, up, down, own, left_a, left_b, right_a, right_b, g_ref, u_ref, far_gate, far_up, far_down, gates, ups, sems):
+def near_kernel(gate, up, down, own, left_a, left_b, right_a, right_b, g_ref, u_ref, far_gate, far_up, far_down, rest_down, gates, ups, sems):
     part = own.shape[1]
     left = (left_a, left_b)
     right = (right_a, right_b)
@@ -131,6 +131,7 @@
         (gate.at[span(2, part)], far_gate),
         (up.at[span(2, part)], far_up),
         (down.at[:, span(2, part)], far_down),
+        *((down.at[:, span(k, part)], rest_down.at[i]) for i, k in enumerate((1, 3, 0))),
     )
     for i, (_, refs) in enumerate(order):
         x = jnp.concatenate([r[...] for r in refs], axis=0)
@@ -155,13 +156,10 @@
     to2b[...] = out[half:]
 
 
-def rest_kernel(down, hid, to1a, to1b, tom1a, tom1b, mine, downs, sems):
-    part, half = to1a.shape[1], to1a.shape[0]
-    order = (1, 3, 0)
-    copies = started(sems, *((down.at[:, span(k, part)], downs.at[i]) for i, k in enumerate(order)))
+def rest_kernel(hid, down, to1a, to1b, tom1a, tom1b, mine):
+    half = to1a.shape[0]
     for i, pair in enumerate(((to1a, to1b), (tom1a, tom1b), (mine.at[:half], mine.at[half:]))):
-        copies[i].wait()
-        out = dot(hid[...], downs[i]).astype(BF16)
+        out = dot(hid[...], down[i]).astype(BF16)
         for ref, rows in zip(pair, (out[:half], out[half:])):
             ref[...] = rows
 
@@ -193,12 +191,10 @@
     return col[:, 0:2] + col[:, 2:4] + col[:, 4:6], row[0:2] + row[2:4] + row[4:6]
 
 
-def inner_kernel(q_ref, k_ref, v_ref, decay_ref, inner_ref, kept_ref, kept_total_ref, send_ref):
-    core = lax.axis_index("c")
+def inner_kernel(q_ref, k_ref, v_ref, decay_ref, inner_ref, state_ref, total_ref, send_ref):
     n = q_ref.shape[0]
     col, row = levels_of(decay_ref[...])
     causal = iota((n, n), 0) >= iota((n, n), 1)
-    states, totals = [], []
     for h in range(2):
         cols = slice(h * 128, h * 128 + 128)
         q, k, v = q_ref[:, cols], k_ref[:, cols], v_ref[:, cols]
@@ -207,13 +203,9 @@
         inner_ref[:, cols] = dot((scores * jnp.exp(spread)).astype(BF16), v)
         total = col[n - 1 : n, h : h + 1]
         scaled = (k.astype(F32) * jnp.exp(total - col[:, h : h + 1])).astype(BF16)
-        states.append(dot_t(scaled, v))
-        totals.append(total)
-    first = core == 0
-    kept_ref[...] = jnp.where(first, states[0], states[1])
-    kept_total_ref[...] = jnp.broadcast_to(jnp.where(first, totals[0], totals[1]), kept_total_ref.shape)
-    send_ref[0:128] = jnp.where(first, states[1], states[0]).astype(BF16)
-    send_ref[128:144] = rows_of_total(jnp.where(first, totals[1], totals[0]), 16)
+        state = dot_t(scaled, v)
+        kept(h, (state, total), state_ref, total_ref)
+        packed(h, (state, total), send_ref)
 
 
 def rows_of_total(total, rows):
@@ -222,86 +214,84 @@
     return jnp.where(r == 0, a, jnp.where(r == 1, b, jnp.where(r == 2, c, 0.0))).astype(BF16)
 
 
-def pair_of(kept_ref, kept_total_ref, got_ref):
-    first = lax.axis_index("c") == 0
-    mine, mine_total = kept_ref[...], kept_total_ref[0:1]
-    theirs = got_ref[0:128].astype(F32)
-    rows = got_ref[128:144].astype(F32)
-    theirs_total = rows[0:1] + rows[1:2] + rows[2:3]
-    return (
-        (jnp.where(first, mine, theirs), jnp.where(first, mine_total, theirs_total)),
-        (jnp.where(first, theirs, mine), jnp.where(first, theirs_total, mine_total)),
-    )
-
-
-def packed(state, total, out_ref):
-    out_ref[0:128] = state.astype(BF16)
-    out_ref[128:144] = rows_of_total(total, 16)
-
-
-def unpacked(ref):
-    rows = ref[128:144].astype(F32)
-    return ref[0:128].astype(F32), rows[0:1] + rows[1:2] + rows[2:3]
+def kept(h, run, state_ref, total_ref):
+    state_ref[128 * h : 128 * h + 128] = run[0]
+    total_ref[8 * h : 8 * h + 8] = jnp.broadcast_to(run[1], (8, 128))
+
+
+def had(h, state_ref, total_ref):
+    return state_ref[128 * h : 128 * h + 128], total_ref[8 * h : 8 * h + 1]
+
+
+def packed(h, run, ref):
+    ref[144 * h : 144 * h + 128] = run[0].astype(BF16)
+    ref[144 * h + 128 : 144 * h + 144] = rows_of_total(run[1], 16)
+
+
+def unpacked(h, ref):
+    rows = ref[144 * h + 128 : 144 * h + 144].astype(F32)
+    return ref[144 * h : 144 * h + 128].astype(F32), rows[0:1] + rows[1:2] + rows[2:3]
 
 
 def after(earlier, later):
     return jnp.exp(later[1]) * earlier[0] + later[0], earlier[1] + later[1]
 
 
-def pair_kernel(kept_ref, kept_total_ref, got_ref, out_ref):
-    packed(*after(*pair_of(kept_ref, kept_total_ref, got_ref)), out_ref)
+def chosen(which, a, b):
+    return tuple(jnp.where(which, x, y) for x, y in zip(a, b))
+
+
+def pair_kernel(state_ref, total_ref, got_ref, out_ref):
+    first = lax.axis_index("c") == 0
+    for h in range(2):
+        mine, theirs = had(h, state_ref, total_ref), unpacked(h, got_ref)
+        packed(h, after(chosen(first, mine, theirs), chosen(first, theirs, mine)), out_ref)
 
 
 def row_kernel(own_ref, one_ref, two_ref, three_ref, before_ref, before_total_ref, out_ref):
     me = lax.axis_index("x")
-    pieces = [unpacked(r) for r in (own_ref, one_ref, two_ref, three_ref)]
-    so_far = before = (jnp.zeros((128, 128), F32), jnp.zeros((1, 128), F32))
-    for k in range(len(pieces)):
-        before = tuple(jnp.where(me == k, new, old) for new, old in zip(so_far, before))
-        back = lax.rem(me - k + len(pieces), len(pieces))
-        here = pieces[0]
-        for by in range(1, len(pieces)):
-            here = tuple(jnp.where(back == by, new, old) for new, old in zip(pieces[by], here))
-        so_far = after(so_far, here)
-    before_ref[...] = before[0]
-    before_total_ref[...] = jnp.broadcast_to(before[1], before_total_ref.shape)
-    packed(*so_far, out_ref)
+    for h in range(2):
+        pieces = [unpacked(h, r) for r in (own_ref, one_ref, two_ref, three_ref)]
+        so_far = before = (jnp.zeros((128, 128), F32), jnp.zeros((1, 128), F32))
+        for k in range(len(pieces)):
+            before = chosen(me == k, so_far, before)
+            back = lax.rem(me - k + len(pieces), len(pieces))
+            here = pieces[0]
+            for by in range(1, len(pieces)):
+                here = chosen(back == by, pieces[by], here)
+            so_far = after(so_far, here)
+        kept(h, before, before_ref, before_total_ref)
+        packed(h, so_far, out_ref)
 
 
 def two_kernel(own_ref, one_ref, out_ref):
-    packed(*after(unpacked(one_ref), unpacked(own_ref)), out_ref)
+    for h in range(2):
+        packed(h, after(unpacked(h, one_ref), unpacked(h, own_ref)), out_ref)
 
 
 def four_kernel(own_ref, one_ref, two_ref, before_ref, before_total_ref, out_ref):
-    before = after(unpacked(two_ref), unpacked(one_ref))
-    before_ref[...] = before[0]
-    before_total_ref[...] = jnp.broadcast_to(before[1], before_total_ref.shape)
-    packed(*after(before, unpacked(own_ref)), out_ref)
-
-
-def entering_kernel(
-    four_ref, rows_ref, rows_total_ref, row_ref, row_total_ref, kept_ref, kept_total_ref, got_ref, keep_ref, send_ref
-):
-    rows, row = (rows_ref[...], rows_total_ref[0:1]), (row_ref[...], row_total_ref[0:1])
-    before = after(after(unpacked(four_ref), rows), row)
-    later, _ = after(before, pair_of(kept_ref, kept_total_ref, got_ref)[0])
-    first = lax.axis_index("c") == 0
-    keep_ref[...] = jnp.where(first, before[0], later).astype(BF16)
-    send_ref[...] = jnp.where(first, later, before[0]).astype(BF16)
-
-
-def mixer_kernel(q_ref, decay_ref, gain_ref, gate_ref, weight_ref, inner_ref, keep_ref, got_ref, *refs):
-    *outs, rows_ref = refs
-    first = lax.axis_index("c") == 0
+    for h in range(2):
+        before = after(unpacked(h, two_ref), unpacked(h, one_ref))
+        kept(h, before, before_ref, before_total_ref)
+        packed(h, after(before, unpacked(h, own_ref)), out_ref)
+
+
+def entering(h, four_ref, rows_ref, rows_total_ref, row_ref, row_total_ref, got_ref):
+    before = after(after(unpacked(h, four_ref), had(h, rows_ref, rows_total_ref)), had(h, row_ref, row_total_ref))
+    later = after(before, unpacked(h, got_ref))
+    return jnp.where(lax.axis_index("c") == 0, before[0], later[0]).astype(BF16)
+
+
+def mixer_kernel(q_ref, decay_ref, gain_ref, gate_ref, weight_ref, inner_ref, *refs):
+    *refs, out_0, out_1, out_2, out_3, rows_ref = refs
+    outs = (out_0, out_1, out_2, out_3)
     col, _ = levels_of(decay_ref[...])
-    keep, got = keep_ref[...], got_ref[...]
-    entering = (jnp.where(first, keep, got), jnp.where(first, got, keep))
     heads = []
     for h in range(2):
         cols = slice(h * 128, h * 128 + 128)
-        carried = jnp.exp(col[:, h : h + 1]) * dot(q_ref[:, cols], entering[h])
-        kept = inner_ref[:, cols] + carried
-        normed = kept * lax.rsqrt(jnp.mean(kept * kept, axis=-1, keepdims=True) + epsilon) * gain_ref[h : h + 1]
+        carried = jnp.exp(col[:, h : h + 1]) * dot(q_ref[:, cols], entering(h, *refs))
+        whole = inner_ref[:, cols] + carried
+        normed = whole * lax.rsqrt(jnp.mean(whole * whole, axis=-1, keepdims=True) + epsilon) * gain_ref[h : h + 1]
         gate = gate_ref[:, cols].astype(F32)
         heads.append((normed * (gate * jax.nn.sigmoid(gate))).astype(BF16).astype(F32))
     rows_ref[...] = jnp.concatenate(heads, axis=1)
@@ -341,28 +331,22 @@
     left_b, right_a = shifted(low, "tp", 1), shifted(top, "tp", -1)
     far_a, far_b = shifted(left_a, "tp", 1), shifted(right_b, "tp", -1)
     rows_of, cols_of = (part, hidden), (hidden, part)
-    g, u, far_gate, far_up, far_down = call(
+    g, u, far_gate, far_up, far_down, rest_down = call(
         near_kernel,
-        sums + [array(rows_of, BF16)] * 2 + [array(cols_of, BF16)],
+        sums + [array(rows_of, BF16)] * 2 + [array(cols_of, BF16), array((3, *cols_of), BF16)],
         rows,
         left_a,
         left_b,
         right_a,
         right_b,
         held=(gate, up, down),
-        scratch_shapes=[pltpu.VMEM((3, *rows_of), BF16)] * 2 + [pltpu.SemaphoreType.DMA((9,))],
+        scratch_shapes=[pltpu.VMEM((3, *rows_of), BF16)] * 2 + [pltpu.SemaphoreType.DMA((12,))],
     )
     hid, to2a, to2b = call(
         far_kernel, [array((2 * half, hidden), BF16), piece, piece], far_a, far_b, g, u, far_gate, far_up, far_down
     )
     got_a, got_b = shifted(to2a, "tp", 1), shifted(to2b, "tp", -1)
-    to1a, to1b, tom1a, tom1b, mine = call(
-        rest_kernel,
-        [piece] * 4 + [array((2 * half, part), BF16)],
-        hid,
-        held=(down,),
-        scratch_shapes=[pltpu.VMEM((3, *cols_of), BF16), pltpu.SemaphoreType.DMA((3,))],
-    )
+    to1a, to1b, tom1a, tom1b, mine = call(rest_kernel, [piece] * 4 + [array((2 * half, part), BF16)], hid, rest_down)
     low_l, top_r = shifted(to1b, "tp", 1), shifted(tom1a, "tp", -1)
     to1a, tom1b = call(onward_kernel, [piece] * 2, to1a, tom1b, got_a, got_b)
     top_l, low_r = shifted(to1a, "tp", 1), shifted(tom1b, "tp", -1)
@@ -415,36 +399,17 @@
     got = shifted(send, "c", 1)
     joined = call(join_kernel, array((chips, 2 * capacity, part), BF16), keep, got)
     arrived = across_chips(joined.reshape(-1, part))
-    inner, kept, kept_total, state_send = call(
-        inner_kernel,
-        [array(q.shape, F32), array((128, 128), F32), array((8, 128), F32), array((144, 128), BF16)],
-        q,
-        k,
-        v,
-        decay,
-        plain=4,
+    whole, state, total = array((288, 128), BF16), array((256, 128), F32), array((16, 128), F32)
+    inner, own_state, own_total, state_send = call(
+        inner_kernel, [array(q.shape, F32), state, total, whole], q, k, v, decay, plain=4
     )
     state_got = shifted(state_send, "c", 1)
-    whole, state, total = array((144, 128), BF16), array((128, 128), F32), array((8, 128), F32)
-    pair = call(pair_kernel, whole, kept, kept_total, state_got)
+    pair = call(pair_kernel, whole, own_state, own_total, state_got)
     around = [shifted(pair, "x", by) for by in (1, 2, 3)]
     row_before, row_total, row = call(row_kernel, [state, total, whole], pair, *around)
     one = brought(row, "z", 1)
     two = brought(call(two_kernel, whole, row, one), "z", 2)
     rows_before, rows_total, upto = call(four_kernel, [state, total, whole], row, one, two)
-    ent_keep, ent_send = call(
-        entering_kernel,
-        [array((128, 128), BF16)] * 2,
-        brought(upto, "z", 4),
-        rows_before,
-        rows_total,
-        row_before,
-        row_total,
-        kept,
-        kept_total,
-        state_got,
-    )
-    ent_got = shifted(ent_send, "c", 1)
     mine, right, far, left = call(
         mixer_kernel,
         [array((q.shape[0] // 4, out_weight.shape[1]), BF16)] * 4,
@@ -454,8 +419,12 @@
         out_gate,
         out_weight,
         inner,
-        ent_keep,
-        ent_got,
+        brought(upto, "z", 4),
+        rows_before,
+        rows_total,
+        row_before,
+        row_total,
+        state_got,
         plain=5,
         scratch_shapes=[pltpu.VMEM(q.shape, F32)],
     )

time: 141 us -> 137 us (0.972)
  the two profiles are of different devices: /device:TPU:1 before, /device:TPU:32 now
where the time goes in v3:
time: 137 us; the launch traced here: 135 us
  starting transfers between devices  51.3 us (37%)
  waiting for transfers between devices  35.5 us (26%)
  blocking collectives  28.5 us (21%)
  Pallas kernels  19.1 us (14%)
    ppermute x21, starting transfers between devices, shifted(): return lax.ppermute(x, axis, [(i, (i + by) % n) for i in range(n)])  30.7 us
    all_to_all x1, blocking collectives, across_chips(): lax.all_to_all(x.reshape(n, -1, x.shape[-1]), ZX, split_axis=0, concat_ax...  28.5 us
    ppermute x21, waiting for transfers between devices, shifted(): return lax.ppermute(x, axis, [(i, (i + by) % n) for i in range(n)])  28 us
    pallas_call x17, Pallas kernels, call(): kernel(*hbm, *(pltpu.with_memory_space_constraint(a, pltpu.VMEM) for a in...  19.1 us
    ppermute x3, starting transfers between devices, brought(): lax.ppermute(x, axis, [(i, i + by) for i in range(lax.axis_size(axis) - b...  15.2 us
    ppermute x3, waiting for transfers between devices, brought(): lax.ppermute(x, axis, [(i, i + by) for i in range(lax.axis_size(axis) - b...  7.54 us
    all_to_all x1, starting transfers between devices, across_chips(): lax.all_to_all(x.reshape(n, -1, x.shape[-1]), ZX, split_axis=0, concat_ax...  5.39 us
  transfers between devices with their start and end apart: 25, of which 17 were waited for; matrix products, arithmetic and copies ran while one was open for 0% of the time, Pallas kernels for 10%

profile of v3, /device:TPU:32, one launch (start us, length us, event | category | flops | bytes accessed | tf_op | source)
XLA Modules:
  0.0 135.3 jit_solution(13551814754201193356)
XLA Ops:
  0.6 1.7 %shard_map.157 = (bf16[256,512]{1,0:T(8,128)(2,1)S(1)}, bf16[256,512]{1,0:T(8,128)(2,1)S(1)}) custom-call(s32[2,128]{1,0:T(2,128)} %bitcast.22, bf16[128,2048]{1,0:T(8,128)(2,1)} %x_ref.1, f32[1,2048]{1,0:T(1,128)} %bitcast.19), custom_call_target="tpu_custom_call" | custom-call | tf_op jit(solution)/shard_map/pallas_call | solution.py:50
  2.3 0.1 collective-permute-start.10
  2.4 1.5 %collective-permute-done.10.got_ref = bf16[256,512]{1,0:T(8,128)(2,1)S(1)} collective-permute-done((bf16[256,512]{1,0:T(8,128)(2,1)S(1)}, bf16[256,512]{1,0:T(8,128)(2,1)S(1)}, u32[]{:S(2)}, u32[]{:S(2)}) %collective-permute-start.10) | collective-permute-done | bytes 262176 | tf_op jit(solution)/shard_map/ppermute | solution.py:312
  4.0 28.5 %all_to_all.10 = bf16[32,16,512]{2,1,0:T(8,128)(2,1)S(1)} all-to-all(bf16[32,16,512]{2,1,0:T(8,128)(2,1)S(1)} %shard_map.158), channel_id=1, replica_groups=mesh['z'=8,'x'=4,'c'=2,'tp'=4] {'z','x'}, dimensions={0} | all-to-all | bytes 1048576 | tf_op jit(solution)/shard_map/all_to_all | solution.py:321
  32.5 1.7 %collective-permute-start.11 = (bf16[256,512]{1,0:T(8,128)(2,1)S(1)}, bf16[256,512]{1,0:T(8,128)(2,1)S(1)}, u32[]{:S(2)}, u32[]{:S(2)}) collective-permute-start(bf16[256,512]{1,0:T(8,128)(2,1)S(1)} %bitcast.15), channel_id=1, source_target_pairs={{0,1},{1,2},{2,3},{3,0},{4,5},{5,6},{6,7},{7,4},{8,9},{9,10},{10,1... | collective-permute-start | bytes 786440 | tf_op jit(solution)/shard_map/ppermute | solution.py:312
  34.1 1.7 %collective-permute-start.13 = (bf16[256,512]{1,0:T(8,128)(2,1)S(1)}, bf16[256,512]{1,0:T(8,128)(2,1)S(1)}, u32[]{:S(2)}, u32[]{:S(2)}) collective-permute-start(bf16[256,512]{1,0:T(8,128)(2,1)S(1)} %bitcast.17), channel_id=1, source_target_pairs={{0,3},{1,0},{2,1},{3,2},{4,7},{5,4},{6,5},{7,6},{8,11},{9,8},{10,9... | collective-permute-start | bytes 786440 | tf_op jit(solution)/shard_map/ppermute | solution.py:312
  35.8 0.4 collective-permute-start.15
  36.2 2.9 %collective-permute-start.16 = (bf16[256,512]{1,0:T(8,128)(2,1)S(1)}, bf16[256,512]{1,0:T(8,128)(2,1)S(1)}, u32[]{:S(2)}, u32[]{:S(2)}) collective-permute-start(bf16[256,512]{1,0:T(8,128)(2,1)S(1)} %bitcast.16), channel_id=1, source_target_pairs={{0,3},{1,0},{2,1},{3,2},{4,7},{5,4},{6,5},{7,6},{8,11},{9,8},{10,9... | collective-permute-start | bytes 786440 | tf_op jit(solution)/shard_map/ppermute | solution.py:312
  39.0 3.9 %collective-permute-done.11.left_a = bf16[256,512]{1,0:T(8,128)(2,1)S(1)} collective-permute-done((bf16[256,512]{1,0:T(8,128)(2,1)S(1)}, bf16[256,512]{1,0:T(8,128)(2,1)S(1)}, u32[]{:S(2)}, u32[]{:S(2)}) %collective-permute-start.11) | collective-permute-done | bytes 262176 | tf_op jit(solution)/shard_map/ppermute | solution.py:312
  43.0 0.4 collective-permute-start.12
  43.3 0.0 collective-permute-done.13.right_b
  43.3 2.9 %collective-permute-start.14 = (bf16[256,512]{1,0:T(8,128)(2,1)S(1)}, bf16[256,512]{1,0:T(8,128)(2,1)S(1)}, u32[]{:S(2)}, u32[]{:S(2)}) collective-permute-start(bf16[256,512]{1,0:T(8,128)(2,1)S(1)} %collective-permute-done.13.right_b), channel_id=1, source_target_pairs={{0,3},{1,0},{2,1},{3,2},{4,7},{5,4},{6,5},{7,6},{8,11},{9,8},{10,9... | collective-permute-start | bytes 786440 | tf_op jit(solution)/shard_map/ppermute | solution.py:312
  46.2 2.4 %collective-permute-done.15.left_b = bf16[256,512]{1,0:T(8,128)(2,1)S(1)} collective-permute-done((bf16[256,512]{1,0:T(8,128)(2,1)S(1)}, bf16[256,512]{1,0:T(8,128)(2,1)S(1)}, u32[]{:S(2)}, u32[]{:S(2)}) %collective-permute-start.15) | collective-permute-done | bytes 262176 | tf_op jit(solution)/shard_map/ppermute | solution.py:312
  48.6 0.1 collective-permute-done.16.right_a
  48.7 5.5 %shard_map.159 = (f32[512,896]{1,0:T(8,128)S(1)}, f32[512,896]{1,0:T(8,128)S(1)}, bf16[512,896]{1,0:T(8,128)(2,1)S(1)}, bf16[512,896]{1,0:T(8,128)(2,1)S(1)}, bf...) custom-call(bf16[2048,896]{1,0:T(8,128)(2,1)} %bitcast.12, bf16[2048,896]{1,0:T(8,128)(2,1)} %bitcast.13, ...), custom_call_target="tpu_custom_call" | custom-call | tf_op jit(solution)/shard_map/pallas_call | solution.py:50
  54.3 0.0 collective-permute-done.12.far_a
  54.3 0.0 collective-permute-done.14.far_b
  54.3 1.8 %shard_map.160 = (bf16[512,896]{1,0:T(8,128)(2,1)S(1)}, bf16[256,512]{1,0:T(8,128)(2,1)S(1)}, bf16[256,512]{1,0:T(8,128)(2,1)S(1)}) custom-call(bf16[256,512]{1,0:T(8,128)(2,1)S(1)} %collective-permute-done.12.far_a, bf16[256,512]{1,0:T(8,128)(2,1)S(1)} %collective-permute-done.14.far_b, f32[512,896]{1,0:T(8,128)S(1)} %get-tuple-element.50.g_in, ...), custom_call_target="tpu_custom_call" | custom-call | tf_op jit(solution)/shard_map/pallas_call | solution.py:50
  56.1 1.6 %collective-permute-start.17 = (bf16[256,512]{1,0:T(8,128)(2,1)S(1)}, bf16[256,512]{1,0:T(8,128)(2,1)S(1)}, u32[]{:S(2)}, u32[]{:S(2)}) collective-permute-start(bf16[256,512]{1,0:T(8,128)(2,1)S(1)} %get-tuple-element.60), channel_id=1, source_target_pairs={{0,1},{1,2},{2,3},{3,0},{4,5},{5,6},{6,7},{7,4},{8,9},{9,10},{10,1... | collective-permute-start | bytes 786440 | tf_op jit(solution)/shard_map/ppermute | solution.py:312
  57.7 1.7 %collective-permute-start.18 = (bf16[256,512]{1,0:T(8,128)(2,1)S(1)}, bf16[256,512]{1,0:T(8,128)(2,1)S(1)}, u32[]{:S(2)}, u32[]{:S(2)}) collective-permute-start(bf16[256,512]{1,0:T(8,128)(2,1)S(1)} %get-tuple-element.61), channel_id=1, source_target_pairs={{0,3},{1,0},{2,1},{3,2},{4,7},{5,4},{6,5},{7,6},{8,11},{9,8},{10,9... | collective-permute-start | bytes 786440 | tf_op jit(solution)/shard_map/ppermute | solution.py:312
  59.5 1.8 %shard_map.161 = (bf16[256,512]{1,0:T(8,128)(2,1)S(1)}, bf16[256,512]{1,0:T(8,128)(2,1)S(1)}, bf16[256,512]{1,0:T(8,128)(2,1)S(1)}, bf16[256,512]{1,0:T(8,128)(2,1)S(1)}, bf16[512,512]{1,0:T(8,128)(2,1)S(1)}) custom-call(bf16[512,896]{1,0:T(8,128)(2,1)S(1)} %get-tuple-element.55.hid, bf16[3,896,512]{2,1,0:T(8,128)(2,1)S(1)} %get-tuple-element.56.down), custom_call_target="tpu_custom_call" | custom-call | tf_op jit(solution)/shard_map/pallas_call | solution.py:50
  61.2 0.4 collective-permute-start.20
  61.6 2.9 %collective-permute-start.21 = (bf16[256,512]{1,0:T(8,128)(2,1)S(1)}, bf16[256,512]{1,0:T(8,128)(2,1)S(1)}, u32[]{:S(2)}, u32[]{:S(2)}) collective-permute-start(bf16[256,512]{1,0:T(8,128)(2,1)S(1)} %get-tuple-element.64), channel_id=1, source_target_pairs={{0,3},{1,0},{2,1},{3,2},{4,7},{5,4},{6,5},{7,6},{8,11},{9,8},{10,9... | collective-permute-start | bytes 786440 | tf_op jit(solution)/shard_map/ppermute | solution.py:312
  64.6 2.0 %collective-permute-done.17.got_a = bf16[256,512]{1,0:T(8,128)(2,1)S(1)} collective-permute-done((bf16[256,512]{1,0:T(8,128)(2,1)S(1)}, bf16[256,512]{1,0:T(8,128)(2,1)S(1)}, u32[]{:S(2)}, u32[]{:S(2)}) %collective-permute-start.17) | collective-permute-done | bytes 262176 | tf_op jit(solution)/shard_map/ppermute | solution.py:312
  66.6 0.1 collective-permute-done.18.got_b
  66.7 0.1 shard_map.162
  66.8 1.5 %collective-permute-start.19 = (bf16[256,512]{1,0:T(8,128)(2,1)S(1)}, bf16[256,512]{1,0:T(8,128)(2,1)S(1)}, u32[]{:S(2)}, u32[]{:S(2)}) collective-permute-start(bf16[256,512]{1,0:T(8,128)(2,1)S(1)} %get-tuple-element.62), channel_id=1, source_target_pairs={{0,1},{1,2},{2,3},{3,0},{4,5},{5,6},{6,7},{7,4},{8,9},{9,10},{10,1... | collective-permute-start | bytes 786440 | tf_op jit(solution)/shard_map/ppermute | solution.py:312
  68.4 1.8 %collective-permute-start.22 = (bf16[256,512]{1,0:T(8,128)(2,1)S(1)}, bf16[256,512]{1,0:T(8,128)(2,1)S(1)}, u32[]{:S(2)}, u32[]{:S(2)}) collective-permute-start(bf16[256,512]{1,0:T(8,128)(2,1)S(1)} %get-tuple-element.65), channel_id=1, source_target_pairs={{0,3},{1,0},{2,1},{3,2},{4,7},{5,4},{6,5},{7,6},{8,11},{9,8},{10,9... | collective-permute-start | bytes 786440 | tf_op jit(solution)/shard_map/ppermute | solution.py:312
  70.1 0.4 collective-permute-done.20.low_l
  70.6 0.0 collective-permute-done.21.top_r
  70.6 3.9 %collective-permute-done.19.top_l = bf16[256,512]{1,0:T(8,128)(2,1)S(1)} collective-permute-done((bf16[256,512]{1,0:T(8,128)(2,1)S(1)}, bf16[256,512]{1,0:T(8,128)(2,1)S(1)}, u32[]{:S(2)}, u32[]{:S(2)}) %collective-permute-start.19) | collective-permute-done | bytes 262176 | tf_op jit(solution)/shard_map/ppermute | solution.py:312
  74.5 0.3 collective-permute-done.22.low_r
  74.7 1.0 shard_map.163
  75.7 5.4 %all-to-all-start.1 = ((bf16[32,16,512]{2,1,0:T(8,128)(2,1)}), bf16[32,16,512]{2,1,0:T(8,128)(2,1)S(1)}, u32[]{:S(2)}, u32[]{:S(2)}) async-start(bf16[32,16,512]{2,1,0:T(8,128)(2,1)} %bitcast.10), calls=%async_computation.1 | async-start | bytes 1048576 | tf_op jit(solution)/shard_map/all_to_all | solution.py:321
  81.1 1.8 %shard_map.149 = (f32[256,256]{1,0:T(8,128)S(1)}, f32[256,128]{1,0:T(8,128)S(1)}, f32[16,128]{1,0:T(8,128)S(1)}, bf16[288,128]{1,0:T(8,128)(2,1)S(1)}) custom-call(bf16[256,256]{1,0:T(8,128)(2,1)} %q_ref.3, bf16[256,256]{1,0:T(8,128)(2,1)} %k_ref.1, bf16[256,256]{1,0:T(8,128)(2,1)} %v_ref.1, f32[2,256]{1,0:T(2,128)} %bitcast.20), custom_call_target="tpu_custom_call" | custom-call | tf_op jit(solution)/shard_map/pallas_call | solution.py:50
  82.9 0.1 collective-permute-start
  83.0 1.3 collective-permute-done.got_ref.refs_5_
  84.3 1.5 %collective-permute-start.1 = (bf16[288,128]{1,0:T(8,128)(2,1)S(1)}, bf16[288,128]{1,0:T(8,128)(2,1)S(1)}, u32[]{:S(2)}, u32[]{:S(2)}) collective-permute-start(bf16[288,128]{1,0:T(8,128)(2,1)S(1)} %shard_map.150.own_ref), channel_id=1, source_target_pairs={{0,8},{8,16},{16,24},{24,0},{1,9},{9,17},{17,25},{25,1},{2,10},{10... | collective-permute-start | bytes 221192 | tf_op jit(solution)/shard_map/ppermute | solution.py:312
  85.8 2.7 %collective-permute-start.2 = (bf16[288,128]{1,0:T(8,128)(2,1)S(1)}, bf16[288,128]{1,0:T(8,128)(2,1)S(1)}, u32[]{:S(2)}, u32[]{:S(2)}) collective-permute-start(bf16[288,128]{1,0:T(8,128)(2,1)S(1)} %shard_map.150.own_ref), channel_id=1, source_target_pairs={{0,16},{8,24},{16,0},{24,8},{1,17},{9,25},{17,1},{25,9},{2,18},{10... | collective-permute-start | bytes 221192 | tf_op jit(solution)/shard_map/ppermute | solution.py:312
  88.5 1.5 %collective-permute-start.3 = (bf16[288,128]{1,0:T(8,128)(2,1)S(1)}, bf16[288,128]{1,0:T(8,128)(2,1)S(1)}, u32[]{:S(2)}, u32[]{:S(2)}) collective-permute-start(bf16[288,128]{1,0:T(8,128)(2,1)S(1)} %shard_map.150.own_ref), channel_id=1, source_target_pairs={{0,24},{8,0},{16,8},{24,16},{1,25},{9,1},{17,9},{25,17},{2,26},{10... | collective-permute-start | bytes 221192 | tf_op jit(solution)/shard_map/ppermute | solution.py:312
  90.0 1.0 collective-permute-done.1.one_ref
  91.0 3.7 %collective-permute-done.2.two_ref = bf16[288,128]{1,0:T(8,128)(2,1)S(1)} collective-permute-done((bf16[288,128]{1,0:T(8,128)(2,1)S(1)}, bf16[288,128]{1,0:T(8,128)(2,1)S(1)}, u32[]{:S(2)}, u32[]{:S(2)}) %collective-permute-start.2) | collective-permute-done | bytes 73760 | tf_op jit(solution)/shard_map/ppermute | solution.py:312
  94.6 0.0 collective-permute-done.3.three_ref
  94.6 0.2 shard_map.151
  94.8 3.0 %collective-permute-start.4 = (bf16[288,128]{1,0:T(8,128)(2,1)S(1)}, bf16[288,128]{1,0:T(8,128)(2,1)S(1)}, u32[]{:S(2)}, u32[]{:S(2)}) collective-permute-start(bf16[288,128]{1,0:T(8,128)(2,1)S(1)} %get-tuple-element.38.own_ref), channel_id=1, source_target_pairs={{0,32},{32,64},{64,96},{96,128},{128,160},{160,192},{192,224},{1,3... | collective-permute-start | bytes 221192 | tf_op jit(solution)/shard_map/ppermute | solution.py:316
  97.8 3.3 %collective-permute-done.4.one_ref = bf16[288,128]{1,0:T(8,128)(2,1)S(1)} collective-permute-done((bf16[288,128]{1,0:T(8,128)(2,1)S(1)}, bf16[288,128]{1,0:T(8,128)(2,1)S(1)}, u32[]{:S(2)}, u32[]{:S(2)}) %collective-permute-start.4) | collective-permute-done | bytes 73760 | tf_op jit(solution)/shard_map/ppermute | solution.py:316
  101.1 4.2 %collective-permute-start.5 = (bf16[288,128]{1,0:T(8,128)(2,1)S(1)}, bf16[288,128]{1,0:T(8,128)(2,1)S(1)}, u32[]{:S(2)}, u32[]{:S(2)}) collective-permute-start(bf16[288,128]{1,0:T(8,128)(2,1)S(1)} %shard_map.152), channel_id=1, source_target_pairs={{0,64},{32,96},{64,128},{96,160},{128,192},{160,224},{1,65},{33,97... | collective-permute-start | bytes 221192 | tf_op jit(solution)/shard_map/ppermute | solution.py:316
  105.3 2.3 %collective-permute-done.5.two_ref = bf16[288,128]{1,0:T(8,128)(2,1)S(1)} collective-permute-done((bf16[288,128]{1,0:T(8,128)(2,1)S(1)}, bf16[288,128]{1,0:T(8,128)(2,1)S(1)}, u32[]{:S(2)}, u32[]{:S(2)}) %collective-permute-start.5) | collective-permute-done | bytes 73760 | tf_op jit(solution)/shard_map/ppermute | solution.py:316
  107.6 0.1 shard_map.153
  107.7 8.0 %collective-permute-start.6 = (bf16[288,128]{1,0:T(8,128)(2,1)S(1)}, bf16[288,128]{1,0:T(8,128)(2,1)S(1)}, u32[]{:S(2)}, u32[]{:S(2)}) collective-permute-start(bf16[288,128]{1,0:T(8,128)(2,1)S(1)} %get-tuple-element.39), channel_id=1, source_target_pairs={{0,128},{32,160},{64,192},{96,224},{1,129},{33,161},{65,193},{97,2... | collective-permute-start | bytes 221192 | tf_op jit(solution)/shard_map/ppermute | solution.py:316
  115.7 2.0 %collective-permute-done.6.refs_0_ = bf16[288,128]{1,0:T(8,128)(2,1)S(1)} collective-permute-done((bf16[288,128]{1,0:T(8,128)(2,1)S(1)}, bf16[288,128]{1,0:T(8,128)(2,1)S(1)}, u32[]{:S(2)}, u32[]{:S(2)}) %collective-permute-start.6) | collective-permute-done | bytes 73760 | tf_op jit(solution)/shard_map/ppermute | solution.py:316
  117.7 2.3 %shard_map.154 = (bf16[64,2048]{1,0:T(8,128)(2,1)S(1)}, bf16[64,2048]{1,0:T(8,128)(2,1)S(1)}, bf16[64,2048]{1,0:T(8,128)(2,1)S(1)}, bf16[64,2048]{1,0:T(8,128)(2,1)S(1)}) custom-call(bf16[256,256]{1,0:T(8,128)(2,1)} %q_ref.3, f32[2,256]{1,0:T(2,128)} %bitcast.21, f32[2,128]{1,0:T(2,128)} %gain_ref.1, bf16[256,256]{1,0:T(8,128)(2,1)} %gate_ref.1, ...), custom_call_target="tpu_custom_call" | custom-call | tf_op jit(solution)/shard_map/pallas_call | solution.py:50
  120.0 0.5 collective-permute-start.7
  120.5 4.3 %collective-permute-start.8 = (bf16[64,2048]{1,0:T(8,128)(2,1)S(1)}, bf16[64,2048]{1,0:T(8,128)(2,1)S(1)}, u32[]{:S(2)}, u32[]{:S(2)}) collective-permute-start(bf16[64,2048]{1,0:T(8,128)(2,1)S(1)} %get-tuple-element.46), channel_id=1, source_target_pairs={{0,2},{1,3},{2,0},{3,1},{4,6},{5,7},{6,4},{7,5},{8,10},{9,11},{10,... | collective-permute-start | bytes 786440 | tf_op jit(solution)/shard_map/ppermute | solution.py:312
  124.8 0.2 collective-permute-start.9
  125.0 0.0 all-to-all-done.1.back_ref
  125.0 0.1 collective-permute-start.23
  125.1 1.0 shard_map.156.w_ref
  126.1 4.4 %collective-permute-done.7.right = bf16[64,2048]{1,0:T(8,128)(2,1)S(1)} collective-permute-done((bf16[64,2048]{1,0:T(8,128)(2,1)S(1)}, bf16[64,2048]{1,0:T(8,128)(2,1)S(1)}, u32[]{:S(2)}, u32[]{:S(2)}) %collective-permute-start.7) | collective-permute-done | bytes 262176 | tf_op jit(solution)/shard_map/ppermute | solution.py:312
  130.5 3.0 %collective-permute-done.8.far = bf16[64,2048]{1,0:T(8,128)(2,1)S(1)} collective-permute-done((bf16[64,2048]{1,0:T(8,128)(2,1)S(1)}, bf16[64,2048]{1,0:T(8,128)(2,1)S(1)}, u32[]{:S(2)}, u32[]{:S(2)}) %collective-permute-start.8) | collective-permute-done | bytes 262176 | tf_op jit(solution)/shard_map/ppermute | solution.py:312
  133.5 0.0 collective-permute-done.9.left
  133.5 0.8 shard_map.155
  134.3 0.0 collective-permute-done.23.sent_ref
  134.3 1.0 shard_map.165
  (5 shorter events, 0.2 us)
Async XLA Ops:
  2.3 1.6 %collective-permute-start.10 = (bf16[256,512]{1,0:T(8,128)(2,1)S(1)}, bf16[256,512]{1,0:T(8,128)(2,1)S(1)}, u32[]{:S(2)}, u32[]{:S(2)}) collective-permute-start(bf16[256,512]{1,0:T(8,128)(2,1)S(1)} %get-tuple-element.49), channel_id=1, source_target_pairs={{0,4},{4,0},{1,5},{5,1},{2,6},{6,2},{3,7},{7,3},{8,12},{12,8},{9,1... | collective-permute-start | bytes 786440 | tf_op jit(solution)/shard_map/ppermute | solution.py:312
  32.5 10.5 %collective-permute-start.11 = (bf16[256,512]{1,0:T(8,128)(2,1)S(1)}, bf16[256,512]{1,0:T(8,128)(2,1)S(1)}, u32[]{:S(2)}, u32[]{:S(2)}) collective-permute-start(bf16[256,512]{1,0:T(8,128)(2,1)S(1)} %bitcast.15), channel_id=1, source_target_pairs={{0,1},{1,2},{2,3},{3,0},{4,5},{5,6},{6,7},{7,4},{8,9},{9,10},{10,1... | collective-permute-start | bytes 786440 | tf_op jit(solution)/shard_map/ppermute | solution.py:312
  34.1 9.2 %collective-permute-start.13 = (bf16[256,512]{1,0:T(8,128)(2,1)S(1)}, bf16[256,512]{1,0:T(8,128)(2,1)S(1)}, u32[]{:S(2)}, u32[]{:S(2)}) collective-permute-start(bf16[256,512]{1,0:T(8,128)(2,1)S(1)} %bitcast.17), channel_id=1, source_target_pairs={{0,3},{1,0},{2,1},{3,2},{4,7},{5,4},{6,5},{7,6},{8,11},{9,8},{10,9... | collective-permute-start | bytes 786440 | tf_op jit(solution)/shard_map/ppermute | solution.py:312
  35.8 12.8 %collective-permute-start.15 = (bf16[256,512]{1,0:T(8,128)(2,1)S(1)}, bf16[256,512]{1,0:T(8,128)(2,1)S(1)}, u32[]{:S(2)}, u32[]{:S(2)}) collective-permute-start(bf16[256,512]{1,0:T(8,128)(2,1)S(1)} %bitcast.18), channel_id=1, source_target_pairs={{0,1},{1,2},{2,3},{3,0},{4,5},{5,6},{6,7},{7,4},{8,9},{9,10},{10,1... | collective-permute-start | bytes 786440 | tf_op jit(solution)/shard_map/ppermute | solution.py:312
  36.2 12.5 %collective-permute-start.16 = (bf16[256,512]{1,0:T(8,128)(2,1)S(1)}, bf16[256,512]{1,0:T(8,128)(2,1)S(1)}, u32[]{:S(2)}, u32[]{:S(2)}) collective-permute-start(bf16[256,512]{1,0:T(8,128)(2,1)S(1)} %bitcast.16), channel_id=1, source_target_pairs={{0,3},{1,0},{2,1},{3,2},{4,7},{5,4},{6,5},{7,6},{8,11},{9,8},{10,9... | collective-permute-start | bytes 786440 | tf_op jit(solution)/shard_map/ppermute | solution.py:312
  43.0 11.3 %collective-permute-start.12 = (bf16[256,512]{1,0:T(8,128)(2,1)S(1)}, bf16[256,512]{1,0:T(8,128)(2,1)S(1)}, u32[]{:S(2)}, u32[]{:S(2)}) collective-permute-start(bf16[256,512]{1,0:T(8,128)(2,1)S(1)} %collective-permute-done.11.left_a), channel_id=1, source_target_pairs={{0,1},{1,2},{2,3},{3,0},{4,5},{5,6},{6,7},{7,4},{8,9},{9,10},{10,1... | collective-permute-start | bytes 786440 | tf_op jit(solution)/shard_map/ppermute | solution.py:312
  43.3 10.9 %collective-permute-start.14 = (bf16[256,512]{1,0:T(8,128)(2,1)S(1)}, bf16[256,512]{1,0:T(8,128)(2,1)S(1)}, u32[]{:S(2)}, u32[]{:S(2)}) collective-permute-start(bf16[256,512]{1,0:T(8,128)(2,1)S(1)} %collective-permute-done.13.right_b), channel_id=1, source_target_pairs={{0,3},{1,0},{2,1},{3,2},{4,7},{5,4},{6,5},{7,6},{8,11},{9,8},{10,9... | collective-permute-start | bytes 786440 | tf_op jit(solution)/shard_map/ppermute | solution.py:312
  56.1 10.5 %collective-permute-start.17 = (bf16[256,512]{1,0:T(8,128)(2,1)S(1)}, bf16[256,512]{1,0:T(8,128)(2,1)S(1)}, u32[]{:S(2)}, u32[]{:S(2)}) collective-permute-start(bf16[256,512]{1,0:T(8,128)(2,1)S(1)} %get-tuple-element.60), channel_id=1, source_target_pairs={{0,1},{1,2},{2,3},{3,0},{4,5},{5,6},{6,7},{7,4},{8,9},{9,10},{10,1... | collective-permute-start | bytes 786440 | tf_op jit(solution)/shard_map/ppermute | solution.py:312
  57.7 9.0 %collective-permute-start.18 = (bf16[256,512]{1,0:T(8,128)(2,1)S(1)}, bf16[256,512]{1,0:T(8,128)(2,1)S(1)}, u32[]{:S(2)}, u32[]{:S(2)}) collective-permute-start(bf16[256,512]{1,0:T(8,128)(2,1)S(1)} %get-tuple-element.61), channel_id=1, source_target_pairs={{0,3},{1,0},{2,1},{3,2},{4,7},{5,4},{6,5},{7,6},{8,11},{9,8},{10,9... | collective-permute-start | bytes 786440 | tf_op jit(solution)/shard_map/ppermute | solution.py:312
  61.2 9.3 %collective-permute-start.20 = (bf16[256,512]{1,0:T(8,128)(2,1)S(1)}, bf16[256,512]{1,0:T(8,128)(2,1)S(1)}, u32[]{:S(2)}, u32[]{:S(2)}) collective-permute-start(bf16[256,512]{1,0:T(8,128)(2,1)S(1)} %get-tuple-element.63), channel_id=1, source_target_pairs={{0,1},{1,2},{2,3},{3,0},{4,5},{5,6},{6,7},{7,4},{8,9},{9,10},{10,1... | collective-permute-start | bytes 786440 | tf_op jit(solution)/shard_map/ppermute | solution.py:312
  61.6 8.9 %collective-permute-start.21 = (bf16[256,512]{1,0:T(8,128)(2,1)S(1)}, bf16[256,512]{1,0:T(8,128)(2,1)S(1)}, u32[]{:S(2)}, u32[]{:S(2)}) collective-permute-start(bf16[256,512]{1,0:T(8,128)(2,1)S(1)} %get-tuple-element.64), channel_id=1, source_target_pairs={{0,3},{1,0},{2,1},{3,2},{4,7},{5,4},{6,5},{7,6},{8,11},{9,8},{10,9... | collective-permute-start | bytes 786440 | tf_op jit(solution)/shard_map/ppermute | solution.py:312
  66.8 7.7 %collective-permute-start.19 = (bf16[256,512]{1,0:T(8,128)(2,1)S(1)}, bf16[256,512]{1,0:T(8,128)(2,1)S(1)}, u32[]{:S(2)}, u32[]{:S(2)}) collective-permute-start(bf16[256,512]{1,0:T(8,128)(2,1)S(1)} %get-tuple-element.62), channel_id=1, source_target_pairs={{0,1},{1,2},{2,3},{3,0},{4,5},{5,6},{6,7},{7,4},{8,9},{9,10},{10,1... | collective-permute-start | bytes 786440 | tf_op jit(solution)/shard_map/ppermute | solution.py:312
  68.4 6.4 %collective-permute-start.22 = (bf16[256,512]{1,0:T(8,128)(2,1)S(1)}, bf16[256,512]{1,0:T(8,128)(2,1)S(1)}, u32[]{:S(2)}, u32[]{:S(2)}) collective-permute-start(bf16[256,512]{1,0:T(8,128)(2,1)S(1)} %get-tuple-element.65), channel_id=1, source_target_pairs={{0,3},{1,0},{2,1},{3,2},{4,7},{5,4},{6,5},{7,6},{8,11},{9,8},{10,9... | collective-permute-start | bytes 786440 | tf_op jit(solution)/shard_map/ppermute | solution.py:312
  75.7 49.3 %all-to-all-start.1 = ((bf16[32,16,512]{2,1,0:T(8,128)(2,1)}), bf16[32,16,512]{2,1,0:T(8,128)(2,1)S(1)}, u32[]{:S(2)}, u32[]{:S(2)}) async-start(bf16[32,16,512]{2,1,0:T(8,128)(2,1)} %bitcast.10), calls=%async_computation.1 | async-start | bytes 1048576 | tf_op jit(solution)/shard_map/all_to_all | solution.py:321
  82.9 1.3 collective-permute-start
  84.3 6.7 %collective-permute-start.1 = (bf16[288,128]{1,0:T(8,128)(2,1)S(1)}, bf16[288,128]{1,0:T(8,128)(2,1)S(1)}, u32[]{:S(2)}, u32[]{:S(2)}) collective-permute-start(bf16[288,128]{1,0:T(8,128)(2,1)S(1)} %shard_map.150.own_ref), channel_id=1, source_target_pairs={{0,8},{8,16},{16,24},{24,0},{1,9},{9,17},{17,25},{25,1},{2,10},{10... | collective-permute-start | bytes 221192 | tf_op jit(solution)/shard_map/ppermute | solution.py:312
  85.8 8.8 %collective-permute-start.2 = (bf16[288,128]{1,0:T(8,128)(2,1)S(1)}, bf16[288,128]{1,0:T(8,128)(2,1)S(1)}, u32[]{:S(2)}, u32[]{:S(2)}) collective-permute-start(bf16[288,128]{1,0:T(8,128)(2,1)S(1)} %shard_map.150.own_ref), channel_id=1, source_target_pairs={{0,16},{8,24},{16,0},{24,8},{1,17},{9,25},{17,1},{25,9},{2,18},{10... | collective-permute-start | bytes 221192 | tf_op jit(solution)/shard_map/ppermute | solution.py:312
  88.5 6.2 %collective-permute-start.3 = (bf16[288,128]{1,0:T(8,128)(2,1)S(1)}, bf16[288,128]{1,0:T(8,128)(2,1)S(1)}, u32[]{:S(2)}, u32[]{:S(2)}) collective-permute-start(bf16[288,128]{1,0:T(8,128)(2,1)S(1)} %shard_map.150.own_ref), channel_id=1, source_target_pairs={{0,24},{8,0},{16,8},{24,16},{1,25},{9,1},{17,9},{25,17},{2,26},{10... | collective-permute-start | bytes 221192 | tf_op jit(solution)/shard_map/ppermute | solution.py:312
  94.8 6.2 %collective-permute-start.4 = (bf16[288,128]{1,0:T(8,128)(2,1)S(1)}, bf16[288,128]{1,0:T(8,128)(2,1)S(1)}, u32[]{:S(2)}, u32[]{:S(2)}) collective-permute-start(bf16[288,128]{1,0:T(8,128)(2,1)S(1)} %get-tuple-element.38.own_ref), channel_id=1, source_target_pairs={{0,32},{32,64},{64,96},{96,128},{128,160},{160,192},{192,224},{1,3... | collective-permute-start | bytes 221192 | tf_op jit(solution)/shard_map/ppermute | solution.py:316
  101.1 6.5 %collective-permute-start.5 = (bf16[288,128]{1,0:T(8,128)(2,1)S(1)}, bf16[288,128]{1,0:T(8,128)(2,1)S(1)}, u32[]{:S(2)}, u32[]{:S(2)}) collective-permute-start(bf16[288,128]{1,0:T(8,128)(2,1)S(1)} %shard_map.152), channel_id=1, source_target_pairs={{0,64},{32,96},{64,128},{96,160},{128,192},{160,224},{1,65},{33,97... | collective-permute-start | bytes 221192 | tf_op jit(solution)/shard_map/ppermute | solution.py:316
  107.7 10.0 %collective-permute-start.6 = (bf16[288,128]{1,0:T(8,128)(2,1)S(1)}, bf16[288,128]{1,0:T(8,128)(2,1)S(1)}, u32[]{:S(2)}, u32[]{:S(2)}) collective-permute-start(bf16[288,128]{1,0:T(8,128)(2,1)S(1)} %get-tuple-element.39), channel_id=1, source_target_pairs={{0,128},{32,160},{64,192},{96,224},{1,129},{33,161},{65,193},{97,2... | collective-permute-start | bytes 221192 | tf_op jit(solution)/shard_map/ppermute | solution.py:316
  120.0 10.5 %collective-permute-start.7 = (bf16[64,2048]{1,0:T(8,128)(2,1)S(1)}, bf16[64,2048]{1,0:T(8,128)(2,1)S(1)}, u32[]{:S(2)}, u32[]{:S(2)}) collective-permute-start(bf16[64,2048]{1,0:T(8,128)(2,1)S(1)} %get-tuple-element.45), channel_id=1, source_target_pairs={{0,1},{1,2},{2,3},{3,0},{4,5},{5,6},{6,7},{7,4},{8,9},{9,10},{10,1... | collective-permute-start | bytes 786440 | tf_op jit(solution)/shard_map/ppermute | solution.py:312
  120.5 13.0 %collective-permute-start.8 = (bf16[64,2048]{1,0:T(8,128)(2,1)S(1)}, bf16[64,2048]{1,0:T(8,128)(2,1)S(1)}, u32[]{:S(2)}, u32[]{:S(2)}) collective-permute-start(bf16[64,2048]{1,0:T(8,128)(2,1)S(1)} %get-tuple-element.46), channel_id=1, source_target_pairs={{0,2},{1,3},{2,0},{3,1},{4,6},{5,7},{6,4},{7,5},{8,10},{9,11},{10,... | collective-permute-start | bytes 786440 | tf_op jit(solution)/shard_map/ppermute | solution.py:312
  124.8 8.7 %collective-permute-start.9 = (bf16[64,2048]{1,0:T(8,128)(2,1)S(1)}, bf16[64,2048]{1,0:T(8,128)(2,1)S(1)}, u32[]{:S(2)}, u32[]{:S(2)}) collective-permute-start(bf16[64,2048]{1,0:T(8,128)(2,1)S(1)} %get-tuple-element.47), channel_id=1, source_target_pairs={{0,3},{1,0},{2,1},{3,2},{4,7},{5,4},{6,5},{7,6},{8,11},{9,8},{10,9... | collective-permute-start | bytes 786440 | tf_op jit(solution)/shard_map/ppermute | solution.py:312
  125.0 9.3 %collective-permute-start.23 = (bf16[256,512]{1,0:T(8,128)(2,1)S(1)}, bf16[256,512]{1,0:T(8,128)(2,1)S(1)}, u32[]{:S(2)}, u32[]{:S(2)}) collective-permute-start(bf16[256,512]{1,0:T(8,128)(2,1)S(1)} %shard_map.164), channel_id=1, source_target_pairs={{0,4},{4,0},{1,5},{5,1},{2,6},{6,2},{3,7},{7,3},{8,12},{12,8},{9,1... | collective-permute-start | bytes 786440 | tf_op jit(solution)/shard_map/ppermute | solution.py:312

commit v4 on v3

--- a/solution.py
+++ b/solution.py
@@ -36,7 +36,7 @@
     return a, b, (rest - b.astype(F32)).astype(BF16)
 
 
-def call(body, outs, *args, plain=0, held=(), scratch_shapes=(), limit=VMEM_LIMIT):
+def call(body, outs, *args, plain=0, loose=0, held=(), scratch_shapes=()):
     space = pl.BlockSpec(memory_space=pltpu.VMEM)
     kernel = pl.pallas_call(
         body,
@@ -44,10 +44,11 @@
         in_specs=[pl.BlockSpec(memory_space=pl.ANY)] * len(held) + [space] * len(args),
         out_specs=[space] * len(outs) if isinstance(outs, list) else space,
         scratch_shapes=scratch_shapes,
-        compiler_params=pltpu.CompilerParams(vmem_limit_bytes=limit),
+        compiler_params=pltpu.CompilerParams(vmem_limit_bytes=VMEM_LIMIT),
     )
     hbm = [pltpu.with_memory_space_constraint(a, pltpu.HBM) for a in (*held, *args[:plain])]
-    return kernel(*hbm, *(pltpu.with_memory_space_constraint(a, pltpu.VMEM) for a in args[plain:]))
+    rest = (pltpu.with_memory_space_constraint(a, pltpu.VMEM) for a in args[plain + loose :])
+    return kernel(*hbm, *args[plain : plain + loose], *rest)
 
 
 def array(shape, dtype):
@@ -87,12 +88,17 @@
         out_ref[half, 1] = (blend - hi.astype(F32)).astype(BF16)
 
 
-def blend_kernel(w_ref, back_ref, sent_ref, out_ref):
+def blended(w_ref, half, rows):
+    return dot_t(w_ref[half, 0], rows) + dot_t(w_ref[half, 1], rows)
+
+
+def kept_blend_kernel(w_ref, back_ref, out_ref):
     keep = jnp.concatenate([back_ref[j, 0:8] for j in range(back_ref.shape[0])], axis=0)
-    total = 0.0
-    for half, rows in enumerate((keep, sent_ref[...])):
-        total = total + dot_t(w_ref[half, 0], rows) + dot_t(w_ref[half, 1], rows)
-    out_ref[...] = total.astype(BF16)
+    out_ref[...] = blended(w_ref, 0, keep)
+
+
+def blend_kernel(w_ref, kept_ref, sent_ref, out_ref):
+    out_ref[...] = (kept_ref[...] + blended(w_ref, 1, sent_ref[...])).astype(BF16)
 
 
 def parted_kernel(back_ref, out_ref):
@@ -425,7 +431,7 @@
         row_before,
         row_total,
         state_got,
-        plain=5,
+        loose=5,
         scratch_shapes=[pltpu.VMEM(q.shape, F32)],
     )
     mixer_out = call(
@@ -442,7 +448,13 @@
     results = experts(arrived, gate, up, down)
     back = across_chips(results).reshape(chips, 2 * capacity, part)
     sent = call(parted_kernel, array((rows, part), BF16), back)
-    expert_out = call(blend_kernel, jax.ShapeDtypeStruct((tokens, part), BF16), weights, back, shifted(sent, "c", 1))
+    expert_out = call(
+        blend_kernel,
+        jax.ShapeDtypeStruct((tokens, part), BF16),
+        weights,
+        call(kept_blend_kernel, array((tokens, part), F32), weights, back),
+        shifted(sent, "c", 1),
+    )
     return mixer_out, expert_out
 
 

time: 137 us -> 136 us (level)
    pallas_call x17 -> x18, Pallas kernels: 19.1 us -> 17.9 us  [call(): return kernel(*hbm, *args[plain:plain + loose], *rest)]
  transfers between devices with their start and end apart: 25 -> 25, of which waited for: 17 -> 17; matrix products, arithmetic and copies ran while one was open for 0% -> 0% of each run, Pallas kernels for 10% -> 9%
where the time goes in v4:
time: 136 us; the launch traced here: 134 us
  starting transfers between devices  51.5 us (38%)
  waiting for transfers between devices  35.3 us (26%)
  blocking collectives  28.5 us (21%)
  Pallas kernels  17.9 us (13%)
    ppermute x21, starting transfers between devices, shifted(): return lax.ppermute(x, axis, [(i, (i + by) % n) for i in range(n)])  30.9 us
    all_to_all x1, blocking collectives, across_chips(): lax.all_to_all(x.reshape(n, -1, x.shape[-1]), ZX, split_axis=0, concat_ax...  28.5 us
    ppermute x21, waiting for transfers between devices, shifted(): return lax.ppermute(x, axis, [(i, (i + by) % n) for i in range(n)])  27.7 us
    pallas_call x18, Pallas kernels, call(): return kernel(*hbm, *args[plain:plain + loose], *rest)  17.9 us
    ppermute x3, starting transfers between devices, brought(): lax.ppermute(x, axis, [(i, i + by) for i in range(lax.axis_size(axis) - b...  15.2 us
    ppermute x3, waiting for transfers between devices, brought(): lax.ppermute(x, axis, [(i, i + by) for i in range(lax.axis_size(axis) - b...  7.54 us
    all_to_all x1, starting transfers between devices, across_chips(): lax.all_to_all(x.reshape(n, -1, x.shape[-1]), ZX, split_axis=0, concat_ax...  5.39 us
  transfers between devices with their start and end apart: 25, of which 17 were waited for; matrix products, arithmetic and copies ran while one was open for 0% of the time, Pallas kernels for 9%

profile of v4, /device:TPU:32, one launch (start us, length us, event | category | flops | bytes accessed | tf_op | source)
XLA Modules:
  0.0 134.1 jit_solution(6192157667649999622)
XLA Ops:
  0.6 1.7 %shard_map.157 = (bf16[256,512]{1,0:T(8,128)(2,1)S(1)}, bf16[256,512]{1,0:T(8,128)(2,1)S(1)}) custom-call(s32[2,128]{1,0:T(2,128)} %bitcast.22, bf16[128,2048]{1,0:T(8,128)(2,1)} %x_ref.1, f32[1,2048]{1,0:T(1,128)} %bitcast.21), custom_call_target="tpu_custom_call" | custom-call | tf_op jit(solution)/shard_map/pallas_call | solution.py:51
  2.3 0.1 collective-permute-start.10
  2.4 1.5 %collective-permute-done.10.got_ref = bf16[256,512]{1,0:T(8,128)(2,1)S(1)} collective-permute-done((bf16[256,512]{1,0:T(8,128)(2,1)S(1)}, bf16[256,512]{1,0:T(8,128)(2,1)S(1)}, u32[]{:S(2)}, u32[]{:S(2)}) %collective-permute-start.10) | collective-permute-done | bytes 262176 | tf_op jit(solution)/shard_map/ppermute | solution.py:318
  4.0 28.5 %all_to_all.10 = bf16[32,16,512]{2,1,0:T(8,128)(2,1)S(1)} all-to-all(bf16[32,16,512]{2,1,0:T(8,128)(2,1)S(1)} %shard_map.158), channel_id=1, replica_groups=mesh['z'=8,'x'=4,'c'=2,'tp'=4] {'z','x'}, dimensions={0} | all-to-all | bytes 1048576 | tf_op jit(solution)/shard_map/all_to_all | solution.py:327
  32.5 1.7 %collective-permute-start.11 = (bf16[256,512]{1,0:T(8,128)(2,1)S(1)}, bf16[256,512]{1,0:T(8,128)(2,1)S(1)}, u32[]{:S(2)}, u32[]{:S(2)}) collective-permute-start(bf16[256,512]{1,0:T(8,128)(2,1)S(1)} %bitcast.17), channel_id=1, source_target_pairs={{0,1},{1,2},{2,3},{3,0},{4,5},{5,6},{6,7},{7,4},{8,9},{9,10},{10,1... | collective-permute-start | bytes 786440 | tf_op jit(solution)/shard_map/ppermute | solution.py:318
  34.1 1.7 %collective-permute-start.13 = (bf16[256,512]{1,0:T(8,128)(2,1)S(1)}, bf16[256,512]{1,0:T(8,128)(2,1)S(1)}, u32[]{:S(2)}, u32[]{:S(2)}) collective-permute-start(bf16[256,512]{1,0:T(8,128)(2,1)S(1)} %bitcast.19), channel_id=1, source_target_pairs={{0,3},{1,0},{2,1},{3,2},{4,7},{5,4},{6,5},{7,6},{8,11},{9,8},{10,9... | collective-permute-start | bytes 786440 | tf_op jit(solution)/shard_map/ppermute | solution.py:318
  35.8 0.4 collective-permute-start.15
  36.2 2.9 %collective-permute-start.16 = (bf16[256,512]{1,0:T(8,128)(2,1)S(1)}, bf16[256,512]{1,0:T(8,128)(2,1)S(1)}, u32[]{:S(2)}, u32[]{:S(2)}) collective-permute-start(bf16[256,512]{1,0:T(8,128)(2,1)S(1)} %bitcast.18), channel_id=1, source_target_pairs={{0,3},{1,0},{2,1},{3,2},{4,7},{5,4},{6,5},{7,6},{8,11},{9,8},{10,9... | collective-permute-start | bytes 786440 | tf_op jit(solution)/shard_map/ppermute | solution.py:318
  39.0 3.9 %collective-permute-done.11.left_a = bf16[256,512]{1,0:T(8,128)(2,1)S(1)} collective-permute-done((bf16[256,512]{1,0:T(8,128)(2,1)S(1)}, bf16[256,512]{1,0:T(8,128)(2,1)S(1)}, u32[]{:S(2)}, u32[]{:S(2)}) %collective-permute-start.11) | collective-permute-done | bytes 262176 | tf_op jit(solution)/shard_map/ppermute | solution.py:318
  43.0 0.4 collective-permute-start.12
  43.3 0.0 collective-permute-done.13.right_b
  43.3 2.9 %collective-permute-start.14 = (bf16[256,512]{1,0:T(8,128)(2,1)S(1)}, bf16[256,512]{1,0:T(8,128)(2,1)S(1)}, u32[]{:S(2)}, u32[]{:S(2)}) collective-permute-start(bf16[256,512]{1,0:T(8,128)(2,1)S(1)} %collective-permute-done.13.right_b), channel_id=1, source_target_pairs={{0,3},{1,0},{2,1},{3,2},{4,7},{5,4},{6,5},{7,6},{8,11},{9,8},{10,9... | collective-permute-start | bytes 786440 | tf_op jit(solution)/shard_map/ppermute | solution.py:318
  46.2 2.4 %collective-permute-done.15.left_b = bf16[256,512]{1,0:T(8,128)(2,1)S(1)} collective-permute-done((bf16[256,512]{1,0:T(8,128)(2,1)S(1)}, bf16[256,512]{1,0:T(8,128)(2,1)S(1)}, u32[]{:S(2)}, u32[]{:S(2)}) %collective-permute-start.15) | collective-permute-done | bytes 262176 | tf_op jit(solution)/shard_map/ppermute | solution.py:318
  48.6 0.1 collective-permute-done.16.right_a
  48.7 5.5 %shard_map.159 = (f32[512,896]{1,0:T(8,128)S(1)}, f32[512,896]{1,0:T(8,128)S(1)}, bf16[512,896]{1,0:T(8,128)(2,1)S(1)}, bf16[512,896]{1,0:T(8,128)(2,1)S(1)}, bf...) custom-call(bf16[2048,896]{1,0:T(8,128)(2,1)} %bitcast.14, bf16[2048,896]{1,0:T(8,128)(2,1)} %bitcast.15, ...), custom_call_target="tpu_custom_call" | custom-call | tf_op jit(solution)/shard_map/pallas_call | solution.py:51
  54.3 0.0 collective-permute-done.12.far_a
  54.3 1.8 %shard_map.160 = (bf16[512,896]{1,0:T(8,128)(2,1)S(1)}, bf16[256,512]{1,0:T(8,128)(2,1)S(1)}, bf16[256,512]{1,0:T(8,128)(2,1)S(1)}) custom-call(bf16[256,512]{1,0:T(8,128)(2,1)S(1)} %collective-permute-done.12.far_a, bf16[256,512]{1,0:T(8,128)(2,1)S(1)} %collective-permute-done.14.far_b, f32[512,896]{1,0:T(8,128)S(1)} %get-tuple-element.50.g_in, ...), custom_call_target="tpu_custom_call" | custom-call | tf_op jit(solution)/shard_map/pallas_call | solution.py:51
  56.1 1.6 %collective-permute-start.17 = (bf16[256,512]{1,0:T(8,128)(2,1)S(1)}, bf16[256,512]{1,0:T(8,128)(2,1)S(1)}, u32[]{:S(2)}, u32[]{:S(2)}) collective-permute-start(bf16[256,512]{1,0:T(8,128)(2,1)S(1)} %get-tuple-element.60), channel_id=1, source_target_pairs={{0,1},{1,2},{2,3},{3,0},{4,5},{5,6},{6,7},{7,4},{8,9},{9,10},{10,1... | collective-permute-start | bytes 786440 | tf_op jit(solution)/shard_map/ppermute | solution.py:318
  57.7 1.7 %collective-permute-start.18 = (bf16[256,512]{1,0:T(8,128)(2,1)S(1)}, bf16[256,512]{1,0:T(8,128)(2,1)S(1)}, u32[]{:S(2)}, u32[]{:S(2)}) collective-permute-start(bf16[256,512]{1,0:T(8,128)(2,1)S(1)} %get-tuple-element.61), channel_id=1, source_target_pairs={{0,3},{1,0},{2,1},{3,2},{4,7},{5,4},{6,5},{7,6},{8,11},{9,8},{10,9... | collective-permute-start | bytes 786440 | tf_op jit(solution)/shard_map/ppermute | solution.py:318
  59.5 1.8 %shard_map.161 = (bf16[256,512]{1,0:T(8,128)(2,1)S(1)}, bf16[256,512]{1,0:T(8,128)(2,1)S(1)}, bf16[256,512]{1,0:T(8,128)(2,1)S(1)}, bf16[256,512]{1,0:T(8,128)(2,1)S(1)}, bf16[512,512]{1,0:T(8,128)(2,1)S(1)}) custom-call(bf16[512,896]{1,0:T(8,128)(2,1)S(1)} %get-tuple-element.55.hid, bf16[3,896,512]{2,1,0:T(8,128)(2,1)S(1)} %get-tuple-element.56.down), custom_call_target="tpu_custom_call" | custom-call | tf_op jit(solution)/shard_map/pallas_call | solution.py:51
  61.2 0.0 copy-start
  61.3 0.0 copy-start.1
  61.3 0.0 copy-start.2
  61.3 0.0 copy-start.3
  61.3 0.0 copy-start.4
  61.3 0.4 collective-permute-start.20
  61.7 2.9 %collective-permute-start.21 = (bf16[256,512]{1,0:T(8,128)(2,1)S(1)}, bf16[256,512]{1,0:T(8,128)(2,1)S(1)}, u32[]{:S(2)}, u32[]{:S(2)}) collective-permute-start(bf16[256,512]{1,0:T(8,128)(2,1)S(1)} %get-tuple-element.64), channel_id=1, source_target_pairs={{0,3},{1,0},{2,1},{3,2},{4,7},{5,4},{6,5},{7,6},{8,11},{9,8},{10,9... | collective-permute-start | bytes 786440 | tf_op jit(solution)/shard_map/ppermute | solution.py:318
  64.6 1.9 %collective-permute-done.17.got_a = bf16[256,512]{1,0:T(8,128)(2,1)S(1)} collective-permute-done((bf16[256,512]{1,0:T(8,128)(2,1)S(1)}, bf16[256,512]{1,0:T(8,128)(2,1)S(1)}, u32[]{:S(2)}, u32[]{:S(2)}) %collective-permute-start.17) | collective-permute-done | bytes 262176 | tf_op jit(solution)/shard_map/ppermute | solution.py:318
  66.6 0.2 collective-permute-done.18.got_b
  66.8 0.1 shard_map.162
  66.9 1.5 %collective-permute-start.19 = (bf16[256,512]{1,0:T(8,128)(2,1)S(1)}, bf16[256,512]{1,0:T(8,128)(2,1)S(1)}, u32[]{:S(2)}, u32[]{:S(2)}) collective-permute-start(bf16[256,512]{1,0:T(8,128)(2,1)S(1)} %get-tuple-element.62), channel_id=1, source_target_pairs={{0,1},{1,2},{2,3},{3,0},{4,5},{5,6},{6,7},{7,4},{8,9},{9,10},{10,1... | collective-permute-start | bytes 786440 | tf_op jit(solution)/shard_map/ppermute | solution.py:318
  68.4 1.8 %collective-permute-start.22 = (bf16[256,512]{1,0:T(8,128)(2,1)S(1)}, bf16[256,512]{1,0:T(8,128)(2,1)S(1)}, u32[]{:S(2)}, u32[]{:S(2)}) collective-permute-start(bf16[256,512]{1,0:T(8,128)(2,1)S(1)} %get-tuple-element.65), channel_id=1, source_target_pairs={{0,3},{1,0},{2,1},{3,2},{4,7},{5,4},{6,5},{7,6},{8,11},{9,8},{10,9... | collective-permute-start | bytes 786440 | tf_op jit(solution)/shard_map/ppermute | solution.py:318
  70.2 0.4 collective-permute-done.20.low_l
  70.6 3.9 %collective-permute-done.19.top_l = bf16[256,512]{1,0:T(8,128)(2,1)S(1)} collective-permute-done((bf16[256,512]{1,0:T(8,128)(2,1)S(1)}, bf16[256,512]{1,0:T(8,128)(2,1)S(1)}, u32[]{:S(2)}, u32[]{:S(2)}) %collective-permute-start.19) | collective-permute-done | bytes 262176 | tf_op jit(solution)/shard_map/ppermute | solution.py:318
  74.6 0.2 collective-permute-done.22.low_r
  74.7 1.0 shard_map.163
  75.7 5.4 %all-to-all-start.1 = ((bf16[32,16,512]{2,1,0:T(8,128)(2,1)}), bf16[32,16,512]{2,1,0:T(8,128)(2,1)S(1)}, u32[]{:S(2)}, u32[]{:S(2)}) async-start(bf16[32,16,512]{2,1,0:T(8,128)(2,1)} %bitcast.10), calls=%async_computation.1 | async-start | bytes 1048576 | tf_op jit(solution)/shard_map/all_to_all | solution.py:327
  81.1 1.8 %shard_map.149 = (f32[256,256]{1,0:T(8,128)S(1)}, f32[256,128]{1,0:T(8,128)S(1)}, f32[16,128]{1,0:T(8,128)S(1)}, bf16[288,128]{1,0:T(8,128)(2,1)S(1)}) custom-call(bf16[256,256]{1,0:T(8,128)(2,1)} %q_ref.3, bf16[256,256]{1,0:T(8,128)(2,1)} %k_ref.1, bf16[256,256]{1,0:T(8,128)(2,1)} %v_ref.1, f32[2,256]{1,0:T(2,128)} %bitcast.12), custom_call_target="tpu_custom_call" | custom-call | tf_op jit(solution)/shard_map/pallas_call | solution.py:51
  82.9 0.1 collective-permute-start
  83.0 1.3 collective-permute-done.got_ref.refs_5_
  84.3 1.5 %collective-permute-start.1 = (bf16[288,128]{1,0:T(8,128)(2,1)S(1)}, bf16[288,128]{1,0:T(8,128)(2,1)S(1)}, u32[]{:S(2)}, u32[]{:S(2)}) collective-permute-start(bf16[288,128]{1,0:T(8,128)(2,1)S(1)} %shard_map.150.own_ref), channel_id=1, source_target_pairs={{0,8},{8,16},{16,24},{24,0},{1,9},{9,17},{17,25},{25,1},{2,10},{10... | collective-permute-start | bytes 221192 | tf_op jit(solution)/shard_map/ppermute | solution.py:318
  85.8 2.7 %collective-permute-start.2 = (bf16[288,128]{1,0:T(8,128)(2,1)S(1)}, bf16[288,128]{1,0:T(8,128)(2,1)S(1)}, u32[]{:S(2)}, u32[]{:S(2)}) collective-permute-start(bf16[288,128]{1,0:T(8,128)(2,1)S(1)} %shard_map.150.own_ref), channel_id=1, source_target_pairs={{0,16},{8,24},{16,0},{24,8},{1,17},{9,25},{17,1},{25,9},{2,18},{10... | collective-permute-start | bytes 221192 | tf_op jit(solution)/shard_map/ppermute | solution.py:318
  88.5 1.5 %collective-permute-start.3 = (bf16[288,128]{1,0:T(8,128)(2,1)S(1)}, bf16[288,128]{1,0:T(8,128)(2,1)S(1)}, u32[]{:S(2)}, u32[]{:S(2)}) collective-permute-start(bf16[288,128]{1,0:T(8,128)(2,1)S(1)} %shard_map.150.own_ref), channel_id=1, source_target_pairs={{0,24},{8,0},{16,8},{24,16},{1,25},{9,1},{17,9},{25,17},{2,26},{10... | collective-permute-start | bytes 221192 | tf_op jit(solution)/shard_map/ppermute | solution.py:318
  90.0 1.0 collective-permute-done.1.one_ref
  91.0 3.7 %collective-permute-done.2.two_ref = bf16[288,128]{1,0:T(8,128)(2,1)S(1)} collective-permute-done((bf16[288,128]{1,0:T(8,128)(2,1)S(1)}, bf16[288,128]{1,0:T(8,128)(2,1)S(1)}, u32[]{:S(2)}, u32[]{:S(2)}) %collective-permute-start.2) | collective-permute-done | bytes 73760 | tf_op jit(solution)/shard_map/ppermute | solution.py:318
  94.7 0.2 shard_map.151
  94.8 3.0 %collective-permute-start.4 = (bf16[288,128]{1,0:T(8,128)(2,1)S(1)}, bf16[288,128]{1,0:T(8,128)(2,1)S(1)}, u32[]{:S(2)}, u32[]{:S(2)}) collective-permute-start(bf16[288,128]{1,0:T(8,128)(2,1)S(1)} %get-tuple-element.38.own_ref), channel_id=1, source_target_pairs={{0,32},{32,64},{64,96},{96,128},{128,160},{160,192},{192,224},{1,3... | collective-permute-start | bytes 221192 | tf_op jit(solution)/shard_map/ppermute | solution.py:322
  97.8 3.3 %collective-permute-done.4.one_ref = bf16[288,128]{1,0:T(8,128)(2,1)S(1)} collective-permute-done((bf16[288,128]{1,0:T(8,128)(2,1)S(1)}, bf16[288,128]{1,0:T(8,128)(2,1)S(1)}, u32[]{:S(2)}, u32[]{:S(2)}) %collective-permute-start.4) | collective-permute-done | bytes 73760 | tf_op jit(solution)/shard_map/ppermute | solution.py:322
  101.1 4.2 %collective-permute-start.5 = (bf16[288,128]{1,0:T(8,128)(2,1)S(1)}, bf16[288,128]{1,0:T(8,128)(2,1)S(1)}, u32[]{:S(2)}, u32[]{:S(2)}) collective-permute-start(bf16[288,128]{1,0:T(8,128)(2,1)S(1)} %shard_map.152), channel_id=1, source_target_pairs={{0,64},{32,96},{64,128},{96,160},{128,192},{160,224},{1,65},{33,97... | collective-permute-start | bytes 221192 | tf_op jit(solution)/shard_map/ppermute | solution.py:322
  105.3 2.3 %collective-permute-done.5.two_ref = bf16[288,128]{1,0:T(8,128)(2,1)S(1)} collective-permute-done((bf16[288,128]{1,0:T(8,128)(2,1)S(1)}, bf16[288,128]{1,0:T(8,128)(2,1)S(1)}, u32[]{:S(2)}, u32[]{:S(2)}) %collective-permute-start.5) | collective-permute-done | bytes 73760 | tf_op jit(solution)/shard_map/ppermute | solution.py:322
  107.6 0.1 shard_map.153
  107.7 8.0 %collective-permute-start.6 = (bf16[288,128]{1,0:T(8,128)(2,1)S(1)}, bf16[288,128]{1,0:T(8,128)(2,1)S(1)}, u32[]{:S(2)}, u32[]{:S(2)}) collective-permute-start(bf16[288,128]{1,0:T(8,128)(2,1)S(1)} %get-tuple-element.39), channel_id=1, source_target_pairs={{0,128},{32,160},{64,192},{96,224},{1,129},{33,161},{65,193},{97,2... | collective-permute-start | bytes 221192 | tf_op jit(solution)/shard_map/ppermute | solution.py:322
  115.7 2.0 %collective-permute-done.6.refs_0_ = bf16[288,128]{1,0:T(8,128)(2,1)S(1)} collective-permute-done((bf16[288,128]{1,0:T(8,128)(2,1)S(1)}, bf16[288,128]{1,0:T(8,128)(2,1)S(1)}, u32[]{:S(2)}, u32[]{:S(2)}) %collective-permute-start.6) | collective-permute-done | bytes 73760 | tf_op jit(solution)/shard_map/ppermute | solution.py:322
  117.7 0.9 shard_map.154
  118.6 0.4 collective-permute-start.7
  119.1 4.3 %collective-permute-start.8 = (bf16[64,2048]{1,0:T(8,128)(2,1)S(1)}, bf16[64,2048]{1,0:T(8,128)(2,1)S(1)}, u32[]{:S(2)}, u32[]{:S(2)}) collective-permute-start(bf16[64,2048]{1,0:T(8,128)(2,1)S(1)} %get-tuple-element.46), channel_id=1, source_target_pairs={{0,2},{1,3},{2,0},{3,1},{4,6},{5,7},{6,4},{7,5},{8,10},{9,11},{10,... | collective-permute-start | bytes 786440 | tf_op jit(solution)/shard_map/ppermute | solution.py:318
  123.4 0.4 collective-permute-start.9
  123.9 0.1 collective-permute-start.23
  124.0 1.0 shard_map.156.w_ref
  124.9 4.2 %collective-permute-done.7.right = bf16[64,2048]{1,0:T(8,128)(2,1)S(1)} collective-permute-done((bf16[64,2048]{1,0:T(8,128)(2,1)S(1)}, bf16[64,2048]{1,0:T(8,128)(2,1)S(1)}, u32[]{:S(2)}, u32[]{:S(2)}) %collective-permute-start.7) | collective-permute-done | bytes 262176 | tf_op jit(solution)/shard_map/ppermute | solution.py:318
  129.1 3.0 %collective-permute-done.8.far = bf16[64,2048]{1,0:T(8,128)(2,1)S(1)} collective-permute-done((bf16[64,2048]{1,0:T(8,128)(2,1)S(1)}, bf16[64,2048]{1,0:T(8,128)(2,1)S(1)}, u32[]{:S(2)}, u32[]{:S(2)}) %collective-permute-start.8) | collective-permute-done | bytes 262176 | tf_op jit(solution)/shard_map/ppermute | solution.py:318
  132.1 0.8 shard_map.155
  132.9 0.2 shard_map.164.kept_ref
  133.2 0.9 shard_map.166
  (16 shorter events, 0.2 us)
Async XLA Ops:
  2.3 1.6 %collective-permute-start.10 = (bf16[256,512]{1,0:T(8,128)(2,1)S(1)}, bf16[256,512]{1,0:T(8,128)(2,1)S(1)}, u32[]{:S(2)}, u32[]{:S(2)}) collective-permute-start(bf16[256,512]{1,0:T(8,128)(2,1)S(1)} %get-tuple-element.49), channel_id=1, source_target_pairs={{0,4},{4,0},{1,5},{5,1},{2,6},{6,2},{3,7},{7,3},{8,12},{12,8},{9,1... | collective-permute-start | bytes 786440 | tf_op jit(solution)/shard_map/ppermute | solution.py:318
  32.5 10.5 %collective-permute-start.11 = (bf16[256,512]{1,0:T(8,128)(2,1)S(1)}, bf16[256,512]{1,0:T(8,128)(2,1)S(1)}, u32[]{:S(2)}, u32[]{:S(2)}) collective-permute-start(bf16[256,512]{1,0:T(8,128)(2,1)S(1)} %bitcast.17), channel_id=1, source_target_pairs={{0,1},{1,2},{2,3},{3,0},{4,5},{5,6},{6,7},{7,4},{8,9},{9,10},{10,1... | collective-permute-start | bytes 786440 | tf_op jit(solution)/shard_map/ppermute | solution.py:318
  34.1 9.2 %collective-permute-start.13 = (bf16[256,512]{1,0:T(8,128)(2,1)S(1)}, bf16[256,512]{1,0:T(8,128)(2,1)S(1)}, u32[]{:S(2)}, u32[]{:S(2)}) collective-permute-start(bf16[256,512]{1,0:T(8,128)(2,1)S(1)} %bitcast.19), channel_id=1, source_target_pairs={{0,3},{1,0},{2,1},{3,2},{4,7},{5,4},{6,5},{7,6},{8,11},{9,8},{10,9... | collective-permute-start | bytes 786440 | tf_op jit(solution)/shard_map/ppermute | solution.py:318
  35.8 12.8 %collective-permute-start.15 = (bf16[256,512]{1,0:T(8,128)(2,1)S(1)}, bf16[256,512]{1,0:T(8,128)(2,1)S(1)}, u32[]{:S(2)}, u32[]{:S(2)}) collective-permute-start(bf16[256,512]{1,0:T(8,128)(2,1)S(1)} %bitcast.20), channel_id=1, source_target_pairs={{0,1},{1,2},{2,3},{3,0},{4,5},{5,6},{6,7},{7,4},{8,9},{9,10},{10,1... | collective-permute-start | bytes 786440 | tf_op jit(solution)/shard_map/ppermute | solution.py:318
  36.2 12.5 %collective-permute-start.16 = (bf16[256,512]{1,0:T(8,128)(2,1)S(1)}, bf16[256,512]{1,0:T(8,128)(2,1)S(1)}, u32[]{:S(2)}, u32[]{:S(2)}) collective-permute-start(bf16[256,512]{1,0:T(8,128)(2,1)S(1)} %bitcast.18), channel_id=1, source_target_pairs={{0,3},{1,0},{2,1},{3,2},{4,7},{5,4},{6,5},{7,6},{8,11},{9,8},{10,9... | collective-permute-start | bytes 786440 | tf_op jit(solution)/shard_map/ppermute | solution.py:318
  43.0 11.3 %collective-permute-start.12 = (bf16[256,512]{1,0:T(8,128)(2,1)S(1)}, bf16[256,512]{1,0:T(8,128)(2,1)S(1)}, u32[]{:S(2)}, u32[]{:S(2)}) collective-permute-start(bf16[256,512]{1,0:T(8,128)(2,1)S(1)} %collective-permute-done.11.left_a), channel_id=1, source_target_pairs={{0,1},{1,2},{2,3},{3,0},{4,5},{5,6},{6,7},{7,4},{8,9},{9,10},{10,1... | collective-permute-start | bytes 786440 | tf_op jit(solution)/shard_map/ppermute | solution.py:318
  43.3 10.9 %collective-permute-start.14 = (bf16[256,512]{1,0:T(8,128)(2,1)S(1)}, bf16[256,512]{1,0:T(8,128)(2,1)S(1)}, u32[]{:S(2)}, u32[]{:S(2)}) collective-permute-start(bf16[256,512]{1,0:T(8,128)(2,1)S(1)} %collective-permute-done.13.right_b), channel_id=1, source_target_pairs={{0,3},{1,0},{2,1},{3,2},{4,7},{5,4},{6,5},{7,6},{8,11},{9,8},{10,9... | collective-permute-start | bytes 786440 | tf_op jit(solution)/shard_map/ppermute | solution.py:318
  56.1 10.5 %collective-permute-start.17 = (bf16[256,512]{1,0:T(8,128)(2,1)S(1)}, bf16[256,512]{1,0:T(8,128)(2,1)S(1)}, u32[]{:S(2)}, u32[]{:S(2)}) collective-permute-start(bf16[256,512]{1,0:T(8,128)(2,1)S(1)} %get-tuple-element.60), channel_id=1, source_target_pairs={{0,1},{1,2},{2,3},{3,0},{4,5},{5,6},{6,7},{7,4},{8,9},{9,10},{10,1... | collective-permute-start | bytes 786440 | tf_op jit(solution)/shard_map/ppermute | solution.py:318
  57.7 9.0 %collective-permute-start.18 = (bf16[256,512]{1,0:T(8,128)(2,1)S(1)}, bf16[256,512]{1,0:T(8,128)(2,1)S(1)}, u32[]{:S(2)}, u32[]{:S(2)}) collective-permute-start(bf16[256,512]{1,0:T(8,128)(2,1)S(1)} %get-tuple-element.61), channel_id=1, source_target_pairs={{0,3},{1,0},{2,1},{3,2},{4,7},{5,4},{6,5},{7,6},{8,11},{9,8},{10,9... | collective-permute-start | bytes 786440 | tf_op jit(solution)/shard_map/ppermute | solution.py:318
  61.2 56.5 %copy-start = (bf16[256,2048]{1,0:T(8,128)(2,1)S(1)}, bf16[256,2048]{1,0:T(8,128)(2,1)}, u32[]{:S(2)}) copy-start(bf16[256,2048]{1,0:T(8,128)(2,1)} %weight_ref.1) | copy-start | bytes 3145732
  61.3 56.5 %copy-start.1 = (bf16[256,256]{1,0:T(8,128)(2,1)S(1)}, bf16[256,256]{1,0:T(8,128)(2,1)}, u32[]{:S(2)}) copy-start(bf16[256,256]{1,0:T(8,128)(2,1)} %q_ref.3) | copy-start | bytes 393220
  61.3 56.4 %copy-start.2 = (bf16[256,256]{1,0:T(8,128)(2,1)S(1)}, bf16[256,256]{1,0:T(8,128)(2,1)}, u32[]{:S(2)}) copy-start(bf16[256,256]{1,0:T(8,128)(2,1)} %gate_ref.1) | copy-start | bytes 393220
  61.3 56.4 %copy-start.3 = (f32[256,2]{0,1:T(2,128)S(1)}, f32[256,2]{0,1:T(2,128)}, u32[]{:S(2)}) copy-start(f32[256,2]{0,1:T(2,128)} %param.18) | copy-start | bytes 6148
  61.3 56.4 %copy-start.4 = (f32[2,128]{1,0:T(2,128)S(1)}, f32[2,128]{1,0:T(2,128)}, u32[]{:S(2)}) copy-start(f32[2,128]{1,0:T(2,128)} %gain_ref.1) | copy-start | bytes 3076
  61.3 9.3 %collective-permute-start.20 = (bf16[256,512]{1,0:T(8,128)(2,1)S(1)}, bf16[256,512]{1,0:T(8,128)(2,1)S(1)}, u32[]{:S(2)}, u32[]{:S(2)}) collective-permute-start(bf16[256,512]{1,0:T(8,128)(2,1)S(1)} %get-tuple-element.63), channel_id=1, source_target_pairs={{0,1},{1,2},{2,3},{3,0},{4,5},{5,6},{6,7},{7,4},{8,9},{9,10},{10,1... | collective-permute-start | bytes 786440 | tf_op jit(solution)/shard_map/ppermute | solution.py:318
  61.7 8.9 %collective-permute-start.21 = (bf16[256,512]{1,0:T(8,128)(2,1)S(1)}, bf16[256,512]{1,0:T(8,128)(2,1)S(1)}, u32[]{:S(2)}, u32[]{:S(2)}) collective-permute-start(bf16[256,512]{1,0:T(8,128)(2,1)S(1)} %get-tuple-element.64), channel_id=1, source_target_pairs={{0,3},{1,0},{2,1},{3,2},{4,7},{5,4},{6,5},{7,6},{8,11},{9,8},{10,9... | collective-permute-start | bytes 786440 | tf_op jit(solution)/shard_map/ppermute | solution.py:318
  66.9 7.7 %collective-permute-start.19 = (bf16[256,512]{1,0:T(8,128)(2,1)S(1)}, bf16[256,512]{1,0:T(8,128)(2,1)S(1)}, u32[]{:S(2)}, u32[]{:S(2)}) collective-permute-start(bf16[256,512]{1,0:T(8,128)(2,1)S(1)} %get-tuple-element.62), channel_id=1, source_target_pairs={{0,1},{1,2},{2,3},{3,0},{4,5},{5,6},{6,7},{7,4},{8,9},{9,10},{10,1... | collective-permute-start | bytes 786440 | tf_op jit(solution)/shard_map/ppermute | solution.py:318
  68.4 6.4 %collective-permute-start.22 = (bf16[256,512]{1,0:T(8,128)(2,1)S(1)}, bf16[256,512]{1,0:T(8,128)(2,1)S(1)}, u32[]{:S(2)}, u32[]{:S(2)}) collective-permute-start(bf16[256,512]{1,0:T(8,128)(2,1)S(1)} %get-tuple-element.65), channel_id=1, source_target_pairs={{0,3},{1,0},{2,1},{3,2},{4,7},{5,4},{6,5},{7,6},{8,11},{9,8},{10,9... | collective-permute-start | bytes 786440 | tf_op jit(solution)/shard_map/ppermute | solution.py:318
  75.7 48.1 %all-to-all-start.1 = ((bf16[32,16,512]{2,1,0:T(8,128)(2,1)}), bf16[32,16,512]{2,1,0:T(8,128)(2,1)S(1)}, u32[]{:S(2)}, u32[]{:S(2)}) async-start(bf16[32,16,512]{2,1,0:T(8,128)(2,1)} %bitcast.10), calls=%async_computation.1 | async-start | bytes 1048576 | tf_op jit(solution)/shard_map/all_to_all | solution.py:327
  82.9 1.3 %collective-permute-start = (bf16[288,128]{1,0:T(8,128)(2,1)S(1)}, bf16[288,128]{1,0:T(8,128)(2,1)S(1)}, u32[]{:S(2)}, u32[]{:S(2)}) collective-permute-start(bf16[288,128]{1,0:T(8,128)(2,1)S(1)} %get-tuple-element.37), channel_id=1, source_target_pairs={{0,4},{4,0},{1,5},{5,1},{2,6},{6,2},{3,7},{7,3},{8,12},{12,8},{9,1... | collective-permute-start | bytes 221192 | tf_op jit(solution)/shard_map/ppermute | solution.py:318
  84.3 6.7 %collective-permute-start.1 = (bf16[288,128]{1,0:T(8,128)(2,1)S(1)}, bf16[288,128]{1,0:T(8,128)(2,1)S(1)}, u32[]{:S(2)}, u32[]{:S(2)}) collective-permute-start(bf16[288,128]{1,0:T(8,128)(2,1)S(1)} %shard_map.150.own_ref), channel_id=1, source_target_pairs={{0,8},{8,16},{16,24},{24,0},{1,9},{9,17},{17,25},{25,1},{2,10},{10... | collective-permute-start | bytes 221192 | tf_op jit(solution)/shard_map/ppermute | solution.py:318
  85.8 8.8 %collective-permute-start.2 = (bf16[288,128]{1,0:T(8,128)(2,1)S(1)}, bf16[288,128]{1,0:T(8,128)(2,1)S(1)}, u32[]{:S(2)}, u32[]{:S(2)}) collective-permute-start(bf16[288,128]{1,0:T(8,128)(2,1)S(1)} %shard_map.150.own_ref), channel_id=1, source_target_pairs={{0,16},{8,24},{16,0},{24,8},{1,17},{9,25},{17,1},{25,9},{2,18},{10... | collective-permute-start | bytes 221192 | tf_op jit(solution)/shard_map/ppermute | solution.py:318
  88.5 6.2 %collective-permute-start.3 = (bf16[288,128]{1,0:T(8,128)(2,1)S(1)}, bf16[288,128]{1,0:T(8,128)(2,1)S(1)}, u32[]{:S(2)}, u32[]{:S(2)}) collective-permute-start(bf16[288,128]{1,0:T(8,128)(2,1)S(1)} %shard_map.150.own_ref), channel_id=1, source_target_pairs={{0,24},{8,0},{16,8},{24,16},{1,25},{9,1},{17,9},{25,17},{2,26},{10... | collective-permute-start | bytes 221192 | tf_op jit(solution)/shard_map/ppermute | solution.py:318
  94.8 6.2 %collective-permute-start.4 = (bf16[288,128]{1,0:T(8,128)(2,1)S(1)}, bf16[288,128]{1,0:T(8,128)(2,1)S(1)}, u32[]{:S(2)}, u32[]{:S(2)}) collective-permute-start(bf16[288,128]{1,0:T(8,128)(2,1)S(1)} %get-tuple-element.38.own_ref), channel_id=1, source_target_pairs={{0,32},{32,64},{64,96},{96,128},{128,160},{160,192},{192,224},{1,3... | collective-permute-start | bytes 221192 | tf_op jit(solution)/shard_map/ppermute | solution.py:322
  101.1 6.5 %collective-permute-start.5 = (bf16[288,128]{1,0:T(8,128)(2,1)S(1)}, bf16[288,128]{1,0:T(8,128)(2,1)S(1)}, u32[]{:S(2)}, u32[]{:S(2)}) collective-permute-start(bf16[288,128]{1,0:T(8,128)(2,1)S(1)} %shard_map.152), channel_id=1, source_target_pairs={{0,64},{32,96},{64,128},{96,160},{128,192},{160,224},{1,65},{33,97... | collective-permute-start | bytes 221192 | tf_op jit(solution)/shard_map/ppermute | solution.py:322
  107.7 10.0 %collective-permute-start.6 = (bf16[288,128]{1,0:T(8,128)(2,1)S(1)}, bf16[288,128]{1,0:T(8,128)(2,1)S(1)}, u32[]{:S(2)}, u32[]{:S(2)}) collective-permute-start(bf16[288,128]{1,0:T(8,128)(2,1)S(1)} %get-tuple-element.39), channel_id=1, source_target_pairs={{0,128},{32,160},{64,192},{96,224},{1,129},{33,161},{65,193},{97,2... | collective-permute-start | bytes 221192 | tf_op jit(solution)/shard_map/ppermute | solution.py:322
  118.6 10.5 %collective-permute-start.7 = (bf16[64,2048]{1,0:T(8,128)(2,1)S(1)}, bf16[64,2048]{1,0:T(8,128)(2,1)S(1)}, u32[]{:S(2)}, u32[]{:S(2)}) collective-permute-start(bf16[64,2048]{1,0:T(8,128)(2,1)S(1)} %get-tuple-element.45), channel_id=1, source_target_pairs={{0,1},{1,2},{2,3},{3,0},{4,5},{5,6},{6,7},{7,4},{8,9},{9,10},{10,1... | collective-permute-start | bytes 786440 | tf_op jit(solution)/shard_map/ppermute | solution.py:318
  119.1 13.0 %collective-permute-start.8 = (bf16[64,2048]{1,0:T(8,128)(2,1)S(1)}, bf16[64,2048]{1,0:T(8,128)(2,1)S(1)}, u32[]{:S(2)}, u32[]{:S(2)}) collective-permute-start(bf16[64,2048]{1,0:T(8,128)(2,1)S(1)} %get-tuple-element.46), channel_id=1, source_target_pairs={{0,2},{1,3},{2,0},{3,1},{4,6},{5,7},{6,4},{7,5},{8,10},{9,11},{10,... | collective-permute-start | bytes 786440 | tf_op jit(solution)/shard_map/ppermute | solution.py:318
  123.4 8.7 %collective-permute-start.9 = (bf16[64,2048]{1,0:T(8,128)(2,1)S(1)}, bf16[64,2048]{1,0:T(8,128)(2,1)S(1)}, u32[]{:S(2)}, u32[]{:S(2)}) collective-permute-start(bf16[64,2048]{1,0:T(8,128)(2,1)S(1)} %get-tuple-element.47), channel_id=1, source_target_pairs={{0,3},{1,0},{2,1},{3,2},{4,7},{5,4},{6,5},{7,6},{8,11},{9,8},{10,9... | collective-permute-start | bytes 786440 | tf_op jit(solution)/shard_map/ppermute | solution.py:318
  123.9 9.3 %collective-permute-start.23 = (bf16[256,512]{1,0:T(8,128)(2,1)S(1)}, bf16[256,512]{1,0:T(8,128)(2,1)S(1)}, u32[]{:S(2)}, u32[]{:S(2)}) collective-permute-start(bf16[256,512]{1,0:T(8,128)(2,1)S(1)} %shard_map.165), channel_id=1, source_target_pairs={{0,4},{4,0},{1,5},{5,1},{2,6},{6,2},{3,7},{7,3},{8,12},{12,8},{9,1... | collective-permute-start | bytes 786440 | tf_op jit(solution)/shard_map/ppermute | solution.py:318

commit v5 on v4

--- a/solution.py
+++ b/solution.py
@@ -67,16 +67,24 @@
     return first & here, second & here
 
 
-def dispatch_kernel(capacity, ids_ref, x_ref, gain_ref, keep_ref, send_ref):
-    part = keep_ref.shape[1]
+def dispatch_kernel(capacity, ids_ref, x_ref, gain_ref, send_ref, normed_ref):
+    part = send_ref.shape[1]
     x = x_ref[...].astype(F32)
     scale = lax.rsqrt(jnp.mean(x * x, axis=-1, keepdims=True) + epsilon)
     cols = pl.ds(pl.multiple_of(lax.axis_index("tp") * part, part), part)
     normed = (x_ref[:, cols].astype(F32) * scale * gain_ref[:, cols]).astype(BF16)
-    for half, ref in enumerate((keep_ref, send_ref)):
-        first, second = slot_members(ids_ref, half, ref.shape[0], capacity)
-        hot = jnp.where(first | second, 1.0, 0.0).astype(BF16)
-        ref[...] = dot(hot, normed).astype(BF16)
+    normed_ref[...] = normed
+    slotted(capacity, ids_ref, 1, normed, send_ref)
+
+
+def keep_kernel(capacity, ids_ref, normed_ref, keep_ref):
+    slotted(capacity, ids_ref, 0, normed_ref[...], keep_ref)
+
+
+def slotted(capacity, ids_ref, half, normed, out_ref):
+    first, second = slot_members(ids_ref, half, out_ref.shape[0], capacity)
+    hot = jnp.where(first | second, 1.0, 0.0).astype(BF16)
+    out_ref[...] = dot(hot, normed).astype(BF16)
 
 
 def blend_weights_kernel(capacity, ids_ref, w_ref, out_ref):
@@ -399,9 +407,11 @@
     chips = lax.axis_size(ZX)
     capacity = 2 * ids.size // lax.axis_size(EP)
     rows = chips * capacity
-    keep, send = call(
-        functools.partial(dispatch_kernel, capacity), [array((rows, part), BF16)] * 2, ids, x, gain, plain=3
-    )
+    slots = array((rows, part), BF16)
+    send, normed = call(
+        functools.partial(dispatch_kernel, capacity), [slots, array((tokens, part), BF16)], ids, x, gain, plain=3
+    )
+    keep = call(functools.partial(keep_kernel, capacity), slots, ids, normed, plain=1)
     got = shifted(send, "c", 1)
     joined = call(join_kernel, array((chips, 2 * capacity, part), BF16), keep, got)
     arrived = across_chips(joined.reshape(-1, part))

time: 136 us -> 136 us (level)
    pallas_call x18 -> x19, Pallas kernels: 17.9 us -> 18.7 us  [call(): return kernel(*hbm, *args[plain:plain + loose], *rest)]
  transfers between devices with their start and end apart: 25 -> 25, of which waited for: 17 -> 17; matrix products, arithmetic and copies ran while one was open for 0% -> 0% of each run, Pallas kernels for 9% -> 10%
where the time goes in v5:
time: 136 us; the launch traced here: 134 us
  starting transfers between devices  51.5 us (38%)
  waiting for transfers between devices  34.2 us (25%)
  blocking collectives  28.5 us (21%)
  Pallas kernels  18.7 us (14%)
    ppermute x21, starting transfers between devices, shifted(): return lax.ppermute(x, axis, [(i, (i + by) % n) for i in range(n)])  30.9 us
    all_to_all x1, blocking collectives, across_chips(): lax.all_to_all(x.reshape(n, -1, x.shape[-1]), ZX, split_axis=0, concat_ax...  28.5 us
    ppermute x21, waiting for transfers between devices, shifted(): return lax.ppermute(x, axis, [(i, (i + by) % n) for i in range(n)])  26.7 us
    pallas_call x19, Pallas kernels, call(): return kernel(*hbm, *args[plain:plain + loose], *rest)  18.7 us
    ppermute x3, starting transfers between devices, brought(): lax.ppermute(x, axis, [(i, i + by) for i in range(lax.axis_size(axis) - b...  15.2 us
    ppermute x3, waiting for transfers between devices, brought(): lax.ppermute(x, axis, [(i, i + by) for i in range(lax.axis_size(axis) - b...  7.54 us
    all_to_all x1, starting transfers between devices, across_chips(): lax.all_to_all(x.reshape(n, -1, x.shape[-1]), ZX, split_axis=0, concat_ax...  5.38 us
  transfers between devices with their start and end apart: 25, of which 17 were waited for; matrix products, arithmetic and copies ran while one was open for 0% of the time, Pallas kernels for 10%

profile of v5, /device:TPU:32, one launch (start us, length us, event | category | flops | bytes accessed | tf_op | source)
XLA Modules:
  0.0 133.9 jit_solution(6148329901732612406)
XLA Ops:
  0.6 1.5 %shard_map.157 = (bf16[256,512]{1,0:T(8,128)(2,1)S(1)}, bf16[128,512]{1,0:T(8,128)(2,1)S(1)}) custom-call(s32[2,128]{1,0:T(2,128)} %bitcast.21, bf16[128,2048]{1,0:T(8,128)(2,1)} %x_ref.1, f32[1,2048]{1,0:T(1,128)} %bitcast.24), custom_call_target="tpu_custom_call" | custom-call | tf_op jit(solution)/shard_map/pallas_call | solution.py:51
  2.1 0.1 collective-permute-start.10
  2.2 1.0 shard_map.158.keep_ref
  3.2 0.5 collective-permute-done.10.got_ref
  3.8 28.5 %all_to_all.10 = bf16[32,16,512]{2,1,0:T(8,128)(2,1)S(1)} all-to-all(bf16[32,16,512]{2,1,0:T(8,128)(2,1)S(1)} %shard_map.159), channel_id=1, replica_groups=mesh['z'=8,'x'=4,'c'=2,'tp'=4] {'z','x'}, dimensions={0} | all-to-all | bytes 1048576 | tf_op jit(solution)/shard_map/all_to_all | solution.py:335
  32.3 1.7 %collective-permute-start.11 = (bf16[256,512]{1,0:T(8,128)(2,1)S(1)}, bf16[256,512]{1,0:T(8,128)(2,1)S(1)}, u32[]{:S(2)}, u32[]{:S(2)}) collective-permute-start(bf16[256,512]{1,0:T(8,128)(2,1)S(1)} %bitcast.17), channel_id=1, source_target_pairs={{0,1},{1,2},{2,3},{3,0},{4,5},{5,6},{6,7},{7,4},{8,9},{9,10},{10,1... | collective-permute-start | bytes 786440 | tf_op jit(solution)/shard_map/ppermute | solution.py:326
  33.9 1.7 %collective-permute-start.13 = (bf16[256,512]{1,0:T(8,128)(2,1)S(1)}, bf16[256,512]{1,0:T(8,128)(2,1)S(1)}, u32[]{:S(2)}, u32[]{:S(2)}) collective-permute-start(bf16[256,512]{1,0:T(8,128)(2,1)S(1)} %bitcast.19), channel_id=1, source_target_pairs={{0,3},{1,0},{2,1},{3,2},{4,7},{5,4},{6,5},{7,6},{8,11},{9,8},{10,9... | collective-permute-start | bytes 786440 | tf_op jit(solution)/shard_map/ppermute | solution.py:326
  35.6 0.4 collective-permute-start.15
  36.0 2.9 %collective-permute-start.16 = (bf16[256,512]{1,0:T(8,128)(2,1)S(1)}, bf16[256,512]{1,0:T(8,128)(2,1)S(1)}, u32[]{:S(2)}, u32[]{:S(2)}) collective-permute-start(bf16[256,512]{1,0:T(8,128)(2,1)S(1)} %bitcast.18), channel_id=1, source_target_pairs={{0,3},{1,0},{2,1},{3,2},{4,7},{5,4},{6,5},{7,6},{8,11},{9,8},{10,9... | collective-permute-start | bytes 786440 | tf_op jit(solution)/shard_map/ppermute | solution.py:326
  38.8 3.9 %collective-permute-done.11.left_a = bf16[256,512]{1,0:T(8,128)(2,1)S(1)} collective-permute-done((bf16[256,512]{1,0:T(8,128)(2,1)S(1)}, bf16[256,512]{1,0:T(8,128)(2,1)S(1)}, u32[]{:S(2)}, u32[]{:S(2)}) %collective-permute-start.11) | collective-permute-done | bytes 262176 | tf_op jit(solution)/shard_map/ppermute | solution.py:326
  42.7 0.4 collective-permute-start.12
  43.1 0.0 collective-permute-done.13.right_b
  43.1 2.9 %collective-permute-start.14 = (bf16[256,512]{1,0:T(8,128)(2,1)S(1)}, bf16[256,512]{1,0:T(8,128)(2,1)S(1)}, u32[]{:S(2)}, u32[]{:S(2)}) collective-permute-start(bf16[256,512]{1,0:T(8,128)(2,1)S(1)} %collective-permute-done.13.right_b), channel_id=1, source_target_pairs={{0,3},{1,0},{2,1},{3,2},{4,7},{5,4},{6,5},{7,6},{8,11},{9,8},{10,9... | collective-permute-start | bytes 786440 | tf_op jit(solution)/shard_map/ppermute | solution.py:326
  46.0 2.4 %collective-permute-done.15.left_b = bf16[256,512]{1,0:T(8,128)(2,1)S(1)} collective-permute-done((bf16[256,512]{1,0:T(8,128)(2,1)S(1)}, bf16[256,512]{1,0:T(8,128)(2,1)S(1)}, u32[]{:S(2)}, u32[]{:S(2)}) %collective-permute-start.15) | collective-permute-done | bytes 262176 | tf_op jit(solution)/shard_map/ppermute | solution.py:326
  48.4 0.1 collective-permute-done.16.right_a
  48.5 5.5 %shard_map.160 = (f32[512,896]{1,0:T(8,128)S(1)}, f32[512,896]{1,0:T(8,128)S(1)}, bf16[512,896]{1,0:T(8,128)(2,1)S(1)}, bf16[512,896]{1,0:T(8,128)(2,1)S(1)}, bf...) custom-call(bf16[2048,896]{1,0:T(8,128)(2,1)} %bitcast.14, bf16[2048,896]{1,0:T(8,128)(2,1)} %bitcast.15, ...), custom_call_target="tpu_custom_call" | custom-call | tf_op jit(solution)/shard_map/pallas_call | solution.py:51
  54.1 1.8 %shard_map.161 = (bf16[512,896]{1,0:T(8,128)(2,1)S(1)}, bf16[256,512]{1,0:T(8,128)(2,1)S(1)}, bf16[256,512]{1,0:T(8,128)(2,1)S(1)}) custom-call(bf16[256,512]{1,0:T(8,128)(2,1)S(1)} %collective-permute-done.12.far_a, bf16[256,512]{1,0:T(8,128)(2,1)S(1)} %collective-permute-done.14.far_b, f32[512,896]{1,0:T(8,128)S(1)} %get-tuple-element.50.g_in, ...), custom_call_target="tpu_custom_call" | custom-call | tf_op jit(solution)/shard_map/pallas_call | solution.py:51
  55.9 1.7 %collective-permute-start.17 = (bf16[256,512]{1,0:T(8,128)(2,1)S(1)}, bf16[256,512]{1,0:T(8,128)(2,1)S(1)}, u32[]{:S(2)}, u32[]{:S(2)}) collective-permute-start(bf16[256,512]{1,0:T(8,128)(2,1)S(1)} %get-tuple-element.60), channel_id=1, source_target_pairs={{0,1},{1,2},{2,3},{3,0},{4,5},{5,6},{6,7},{7,4},{8,9},{9,10},{10,1... | collective-permute-start | bytes 786440 | tf_op jit(solution)/shard_map/ppermute | solution.py:326
  57.5 1.7 %collective-permute-start.18 = (bf16[256,512]{1,0:T(8,128)(2,1)S(1)}, bf16[256,512]{1,0:T(8,128)(2,1)S(1)}, u32[]{:S(2)}, u32[]{:S(2)}) collective-permute-start(bf16[256,512]{1,0:T(8,128)(2,1)S(1)} %get-tuple-element.61), channel_id=1, source_target_pairs={{0,3},{1,0},{2,1},{3,2},{4,7},{5,4},{6,5},{7,6},{8,11},{9,8},{10,9... | collective-permute-start | bytes 786440 | tf_op jit(solution)/shard_map/ppermute | solution.py:326
  59.2 1.8 %shard_map.162 = (bf16[256,512]{1,0:T(8,128)(2,1)S(1)}, bf16[256,512]{1,0:T(8,128)(2,1)S(1)}, bf16[256,512]{1,0:T(8,128)(2,1)S(1)}, bf16[256,512]{1,0:T(8,128)(2,1)S(1)}, bf16[512,512]{1,0:T(8,128)(2,1)S(1)}) custom-call(bf16[512,896]{1,0:T(8,128)(2,1)S(1)} %get-tuple-element.55.hid, bf16[3,896,512]{2,1,0:T(8,128)(2,1)S(1)} %get-tuple-element.56.down), custom_call_target="tpu_custom_call" | custom-call | tf_op jit(solution)/shard_map/pallas_call | solution.py:51
  61.0 0.0 copy-start
  61.0 0.0 copy-start.1
  61.1 0.0 copy-start.2
  61.1 0.0 copy-start.3
  61.1 0.0 copy-start.4
  61.1 0.4 collective-permute-start.20
  61.5 2.9 %collective-permute-start.21 = (bf16[256,512]{1,0:T(8,128)(2,1)S(1)}, bf16[256,512]{1,0:T(8,128)(2,1)S(1)}, u32[]{:S(2)}, u32[]{:S(2)}) collective-permute-start(bf16[256,512]{1,0:T(8,128)(2,1)S(1)} %get-tuple-element.64), channel_id=1, source_target_pairs={{0,3},{1,0},{2,1},{3,2},{4,7},{5,4},{6,5},{7,6},{8,11},{9,8},{10,9... | collective-permute-start | bytes 786440 | tf_op jit(solution)/shard_map/ppermute | solution.py:326
  64.4 1.9 %collective-permute-done.17.got_a = bf16[256,512]{1,0:T(8,128)(2,1)S(1)} collective-permute-done((bf16[256,512]{1,0:T(8,128)(2,1)S(1)}, bf16[256,512]{1,0:T(8,128)(2,1)S(1)}, u32[]{:S(2)}, u32[]{:S(2)}) %collective-permute-start.17) | collective-permute-done | bytes 262176 | tf_op jit(solution)/shard_map/ppermute | solution.py:326
  66.3 0.2 collective-permute-done.18.got_b
  66.6 0.1 shard_map.163
  66.7 1.5 %collective-permute-start.19 = (bf16[256,512]{1,0:T(8,128)(2,1)S(1)}, bf16[256,512]{1,0:T(8,128)(2,1)S(1)}, u32[]{:S(2)}, u32[]{:S(2)}) collective-permute-start(bf16[256,512]{1,0:T(8,128)(2,1)S(1)} %get-tuple-element.62), channel_id=1, source_target_pairs={{0,1},{1,2},{2,3},{3,0},{4,5},{5,6},{6,7},{7,4},{8,9},{9,10},{10,1... | collective-permute-start | bytes 786440 | tf_op jit(solution)/shard_map/ppermute | solution.py:326
  68.2 1.8 %collective-permute-start.22 = (bf16[256,512]{1,0:T(8,128)(2,1)S(1)}, bf16[256,512]{1,0:T(8,128)(2,1)S(1)}, u32[]{:S(2)}, u32[]{:S(2)}) collective-permute-start(bf16[256,512]{1,0:T(8,128)(2,1)S(1)} %get-tuple-element.65), channel_id=1, source_target_pairs={{0,3},{1,0},{2,1},{3,2},{4,7},{5,4},{6,5},{7,6},{8,11},{9,8},{10,9... | collective-permute-start | bytes 786440 | tf_op jit(solution)/shard_map/ppermute | solution.py:326
  70.0 0.4 collective-permute-done.20.low_l
  70.4 3.9 %collective-permute-done.19.top_l = bf16[256,512]{1,0:T(8,128)(2,1)S(1)} collective-permute-done((bf16[256,512]{1,0:T(8,128)(2,1)S(1)}, bf16[256,512]{1,0:T(8,128)(2,1)S(1)}, u32[]{:S(2)}, u32[]{:S(2)}) %collective-permute-start.19) | collective-permute-done | bytes 262176 | tf_op jit(solution)/shard_map/ppermute | solution.py:326
  74.3 0.2 collective-permute-done.22.low_r
  74.5 1.0 shard_map.164
  75.5 5.4 %all-to-all-start.1 = ((bf16[32,16,512]{2,1,0:T(8,128)(2,1)}), bf16[32,16,512]{2,1,0:T(8,128)(2,1)S(1)}, u32[]{:S(2)}, u32[]{:S(2)}) async-start(bf16[32,16,512]{2,1,0:T(8,128)(2,1)} %bitcast.10), calls=%async_computation.1 | async-start | bytes 1048576 | tf_op jit(solution)/shard_map/all_to_all | solution.py:335
  80.9 1.8 %shard_map.149 = (f32[256,256]{1,0:T(8,128)S(1)}, f32[256,128]{1,0:T(8,128)S(1)}, f32[16,128]{1,0:T(8,128)S(1)}, bf16[288,128]{1,0:T(8,128)(2,1)S(1)}) custom-call(bf16[256,256]{1,0:T(8,128)(2,1)} %q_ref.3, bf16[256,256]{1,0:T(8,128)(2,1)} %k_ref.1, bf16[256,256]{1,0:T(8,128)(2,1)} %v_ref.1, f32[2,256]{1,0:T(2,128)} %bitcast.12), custom_call_target="tpu_custom_call" | custom-call | tf_op jit(solution)/shard_map/pallas_call | solution.py:51
  82.7 0.1 collective-permute-start
  82.8 1.3 collective-permute-done.got_ref.refs_5_
  84.1 1.5 %collective-permute-start.1 = (bf16[288,128]{1,0:T(8,128)(2,1)S(1)}, bf16[288,128]{1,0:T(8,128)(2,1)S(1)}, u32[]{:S(2)}, u32[]{:S(2)}) collective-permute-start(bf16[288,128]{1,0:T(8,128)(2,1)S(1)} %shard_map.150.own_ref), channel_id=1, source_target_pairs={{0,8},{8,16},{16,24},{24,0},{1,9},{9,17},{17,25},{25,1},{2,10},{10... | collective-permute-start | bytes 221192 | tf_op jit(solution)/shard_map/ppermute | solution.py:326
  85.6 2.7 %collective-permute-start.2 = (bf16[288,128]{1,0:T(8,128)(2,1)S(1)}, bf16[288,128]{1,0:T(8,128)(2,1)S(1)}, u32[]{:S(2)}, u32[]{:S(2)}) collective-permute-start(bf16[288,128]{1,0:T(8,128)(2,1)S(1)} %shard_map.150.own_ref), channel_id=1, source_target_pairs={{0,16},{8,24},{16,0},{24,8},{1,17},{9,25},{17,1},{25,9},{2,18},{10... | collective-permute-start | bytes 221192 | tf_op jit(solution)/shard_map/ppermute | solution.py:326
  88.3 1.5 %collective-permute-start.3 = (bf16[288,128]{1,0:T(8,128)(2,1)S(1)}, bf16[288,128]{1,0:T(8,128)(2,1)S(1)}, u32[]{:S(2)}, u32[]{:S(2)}) collective-permute-start(bf16[288,128]{1,0:T(8,128)(2,1)S(1)} %shard_map.150.own_ref), channel_id=1, source_target_pairs={{0,24},{8,0},{16,8},{24,16},{1,25},{9,1},{17,9},{25,17},{2,26},{10... | collective-permute-start | bytes 221192 | tf_op jit(solution)/shard_map/ppermute | solution.py:326
  89.8 1.0 collective-permute-done.1.one_ref
  90.8 3.7 %collective-permute-done.2.two_ref = bf16[288,128]{1,0:T(8,128)(2,1)S(1)} collective-permute-done((bf16[288,128]{1,0:T(8,128)(2,1)S(1)}, bf16[288,128]{1,0:T(8,128)(2,1)S(1)}, u32[]{:S(2)}, u32[]{:S(2)}) %collective-permute-start.2) | collective-permute-done | bytes 73760 | tf_op jit(solution)/shard_map/ppermute | solution.py:326
  94.4 0.2 shard_map.151
  94.6 3.0 %collective-permute-start.4 = (bf16[288,128]{1,0:T(8,128)(2,1)S(1)}, bf16[288,128]{1,0:T(8,128)(2,1)S(1)}, u32[]{:S(2)}, u32[]{:S(2)}) collective-permute-start(bf16[288,128]{1,0:T(8,128)(2,1)S(1)} %get-tuple-element.38.own_ref), channel_id=1, source_target_pairs={{0,32},{32,64},{64,96},{96,128},{128,160},{160,192},{192,224},{1,3... | collective-permute-start | bytes 221192 | tf_op jit(solution)/shard_map/ppermute | solution.py:330
  97.6 3.2 %collective-permute-done.4.one_ref = bf16[288,128]{1,0:T(8,128)(2,1)S(1)} collective-permute-done((bf16[288,128]{1,0:T(8,128)(2,1)S(1)}, bf16[288,128]{1,0:T(8,128)(2,1)S(1)}, u32[]{:S(2)}, u32[]{:S(2)}) %collective-permute-start.4) | collective-permute-done | bytes 73760 | tf_op jit(solution)/shard_map/ppermute | solution.py:330
  100.9 4.2 %collective-permute-start.5 = (bf16[288,128]{1,0:T(8,128)(2,1)S(1)}, bf16[288,128]{1,0:T(8,128)(2,1)S(1)}, u32[]{:S(2)}, u32[]{:S(2)}) collective-permute-start(bf16[288,128]{1,0:T(8,128)(2,1)S(1)} %shard_map.152), channel_id=1, source_target_pairs={{0,64},{32,96},{64,128},{96,160},{128,192},{160,224},{1,65},{33,97... | collective-permute-start | bytes 221192 | tf_op jit(solution)/shard_map/ppermute | solution.py:330
  105.1 2.3 %collective-permute-done.5.two_ref = bf16[288,128]{1,0:T(8,128)(2,1)S(1)} collective-permute-done((bf16[288,128]{1,0:T(8,128)(2,1)S(1)}, bf16[288,128]{1,0:T(8,128)(2,1)S(1)}, u32[]{:S(2)}, u32[]{:S(2)}) %collective-permute-start.5) | collective-permute-done | bytes 73760 | tf_op jit(solution)/shard_map/ppermute | solution.py:330
  107.4 0.1 shard_map.153
  107.5 8.0 %collective-permute-start.6 = (bf16[288,128]{1,0:T(8,128)(2,1)S(1)}, bf16[288,128]{1,0:T(8,128)(2,1)S(1)}, u32[]{:S(2)}, u32[]{:S(2)}) collective-permute-start(bf16[288,128]{1,0:T(8,128)(2,1)S(1)} %get-tuple-element.39), channel_id=1, source_target_pairs={{0,128},{32,160},{64,192},{96,224},{1,129},{33,161},{65,193},{97,2... | collective-permute-start | bytes 221192 | tf_op jit(solution)/shard_map/ppermute | solution.py:330
  115.5 2.0 %collective-permute-done.6.refs_0_ = bf16[288,128]{1,0:T(8,128)(2,1)S(1)} collective-permute-done((bf16[288,128]{1,0:T(8,128)(2,1)S(1)}, bf16[288,128]{1,0:T(8,128)(2,1)S(1)}, u32[]{:S(2)}, u32[]{:S(2)}) %collective-permute-start.6) | collective-permute-done | bytes 73760 | tf_op jit(solution)/shard_map/ppermute | solution.py:330
  117.5 0.9 shard_map.154
  118.4 0.5 collective-permute-start.7
  118.9 4.3 %collective-permute-start.8 = (bf16[64,2048]{1,0:T(8,128)(2,1)S(1)}, bf16[64,2048]{1,0:T(8,128)(2,1)S(1)}, u32[]{:S(2)}, u32[]{:S(2)}) collective-permute-start(bf16[64,2048]{1,0:T(8,128)(2,1)S(1)} %get-tuple-element.46), channel_id=1, source_target_pairs={{0,2},{1,3},{2,0},{3,1},{4,6},{5,7},{6,4},{7,5},{8,10},{9,11},{10,... | collective-permute-start | bytes 786440 | tf_op jit(solution)/shard_map/ppermute | solution.py:326
  123.2 0.4 collective-permute-start.9
  123.6 0.1 collective-permute-start.23
  123.7 1.0 shard_map.156.w_ref
  124.7 4.2 %collective-permute-done.7.right = bf16[64,2048]{1,0:T(8,128)(2,1)S(1)} collective-permute-done((bf16[64,2048]{1,0:T(8,128)(2,1)S(1)}, bf16[64,2048]{1,0:T(8,128)(2,1)S(1)}, u32[]{:S(2)}, u32[]{:S(2)}) %collective-permute-start.7) | collective-permute-done | bytes 262176 | tf_op jit(solution)/shard_map/ppermute | solution.py:326
  128.9 3.0 %collective-permute-done.8.far = bf16[64,2048]{1,0:T(8,128)(2,1)S(1)} collective-permute-done((bf16[64,2048]{1,0:T(8,128)(2,1)S(1)}, bf16[64,2048]{1,0:T(8,128)(2,1)S(1)}, u32[]{:S(2)}, u32[]{:S(2)}) %collective-permute-start.8) | collective-permute-done | bytes 262176 | tf_op jit(solution)/shard_map/ppermute | solution.py:326
  131.9 0.8 shard_map.155
  132.7 0.2 shard_map.165.kept_ref
  133.0 0.9 shard_map.167
  (17 shorter events, 0.2 us)
Async XLA Ops:
  2.1 1.6 %collective-permute-start.10 = (bf16[256,512]{1,0:T(8,128)(2,1)S(1)}, bf16[256,512]{1,0:T(8,128)(2,1)S(1)}, u32[]{:S(2)}, u32[]{:S(2)}) collective-permute-start(bf16[256,512]{1,0:T(8,128)(2,1)S(1)} %get-tuple-element.49), channel_id=1, source_target_pairs={{0,4},{4,0},{1,5},{5,1},{2,6},{6,2},{3,7},{7,3},{8,12},{12,8},{9,1... | collective-permute-start | bytes 786440 | tf_op jit(solution)/shard_map/ppermute | solution.py:326
  32.3 10.5 %collective-permute-start.11 = (bf16[256,512]{1,0:T(8,128)(2,1)S(1)}, bf16[256,512]{1,0:T(8,128)(2,1)S(1)}, u32[]{:S(2)}, u32[]{:S(2)}) collective-permute-start(bf16[256,512]{1,0:T(8,128)(2,1)S(1)} %bitcast.17), channel_id=1, source_target_pairs={{0,1},{1,2},{2,3},{3,0},{4,5},{5,6},{6,7},{7,4},{8,9},{9,10},{10,1... | collective-permute-start | bytes 786440 | tf_op jit(solution)/shard_map/ppermute | solution.py:326
  33.9 9.2 %collective-permute-start.13 = (bf16[256,512]{1,0:T(8,128)(2,1)S(1)}, bf16[256,512]{1,0:T(8,128)(2,1)S(1)}, u32[]{:S(2)}, u32[]{:S(2)}) collective-permute-start(bf16[256,512]{1,0:T(8,128)(2,1)S(1)} %bitcast.19), channel_id=1, source_target_pairs={{0,3},{1,0},{2,1},{3,2},{4,7},{5,4},{6,5},{7,6},{8,11},{9,8},{10,9... | collective-permute-start | bytes 786440 | tf_op jit(solution)/shard_map/ppermute | solution.py:326
  35.6 12.8 %collective-permute-start.15 = (bf16[256,512]{1,0:T(8,128)(2,1)S(1)}, bf16[256,512]{1,0:T(8,128)(2,1)S(1)}, u32[]{:S(2)}, u32[]{:S(2)}) collective-permute-start(bf16[256,512]{1,0:T(8,128)(2,1)S(1)} %bitcast.20), channel_id=1, source_target_pairs={{0,1},{1,2},{2,3},{3,0},{4,5},{5,6},{6,7},{7,4},{8,9},{9,10},{10,1... | collective-permute-start | bytes 786440 | tf_op jit(solution)/shard_map/ppermute | solution.py:326
  36.0 12.5 %collective-permute-start.16 = (bf16[256,512]{1,0:T(8,128)(2,1)S(1)}, bf16[256,512]{1,0:T(8,128)(2,1)S(1)}, u32[]{:S(2)}, u32[]{:S(2)}) collective-permute-start(bf16[256,512]{1,0:T(8,128)(2,1)S(1)} %bitcast.18), channel_id=1, source_target_pairs={{0,3},{1,0},{2,1},{3,2},{4,7},{5,4},{6,5},{7,6},{8,11},{9,8},{10,9... | collective-permute-start | bytes 786440 | tf_op jit(solution)/shard_map/ppermute | solution.py:326
  42.7 11.3 %collective-permute-start.12 = (bf16[256,512]{1,0:T(8,128)(2,1)S(1)}, bf16[256,512]{1,0:T(8,128)(2,1)S(1)}, u32[]{:S(2)}, u32[]{:S(2)}) collective-permute-start(bf16[256,512]{1,0:T(8,128)(2,1)S(1)} %collective-permute-done.11.left_a), channel_id=1, source_target_pairs={{0,1},{1,2},{2,3},{3,0},{4,5},{5,6},{6,7},{7,4},{8,9},{9,10},{10,1... | collective-permute-start | bytes 786440 | tf_op jit(solution)/shard_map/ppermute | solution.py:326
  43.1 10.9 %collective-permute-start.14 = (bf16[256,512]{1,0:T(8,128)(2,1)S(1)}, bf16[256,512]{1,0:T(8,128)(2,1)S(1)}, u32[]{:S(2)}, u32[]{:S(2)}) collective-permute-start(bf16[256,512]{1,0:T(8,128)(2,1)S(1)} %collective-permute-done.13.right_b), channel_id=1, source_target_pairs={{0,3},{1,0},{2,1},{3,2},{4,7},{5,4},{6,5},{7,6},{8,11},{9,8},{10,9... | collective-permute-start | bytes 786440 | tf_op jit(solution)/shard_map/ppermute | solution.py:326
  55.9 10.5 %collective-permute-start.17 = (bf16[256,512]{1,0:T(8,128)(2,1)S(1)}, bf16[256,512]{1,0:T(8,128)(2,1)S(1)}, u32[]{:S(2)}, u32[]{:S(2)}) collective-permute-start(bf16[256,512]{1,0:T(8,128)(2,1)S(1)} %get-tuple-element.60), channel_id=1, source_target_pairs={{0,1},{1,2},{2,3},{3,0},{4,5},{5,6},{6,7},{7,4},{8,9},{9,10},{10,1... | collective-permute-start | bytes 786440 | tf_op jit(solution)/shard_map/ppermute | solution.py:326
  57.5 9.0 %collective-permute-start.18 = (bf16[256,512]{1,0:T(8,128)(2,1)S(1)}, bf16[256,512]{1,0:T(8,128)(2,1)S(1)}, u32[]{:S(2)}, u32[]{:S(2)}) collective-permute-start(bf16[256,512]{1,0:T(8,128)(2,1)S(1)} %get-tuple-element.61), channel_id=1, source_target_pairs={{0,3},{1,0},{2,1},{3,2},{4,7},{5,4},{6,5},{7,6},{8,11},{9,8},{10,9... | collective-permute-start | bytes 786440 | tf_op jit(solution)/shard_map/ppermute | solution.py:326
  61.0 56.5 %copy-start = (bf16[256,2048]{1,0:T(8,128)(2,1)S(1)}, bf16[256,2048]{1,0:T(8,128)(2,1)}, u32[]{:S(2)}) copy-start(bf16[256,2048]{1,0:T(8,128)(2,1)} %weight_ref.1) | copy-start | bytes 3145732
  61.0 56.4 %copy-start.1 = (bf16[256,256]{1,0:T(8,128)(2,1)S(1)}, bf16[256,256]{1,0:T(8,128)(2,1)}, u32[]{:S(2)}) copy-start(bf16[256,256]{1,0:T(8,128)(2,1)} %q_ref.3) | copy-start | bytes 393220
  61.1 56.4 %copy-start.2 = (bf16[256,256]{1,0:T(8,128)(2,1)S(1)}, bf16[256,256]{1,0:T(8,128)(2,1)}, u32[]{:S(2)}) copy-start(bf16[256,256]{1,0:T(8,128)(2,1)} %gate_ref.1) | copy-start | bytes 393220
  61.1 56.4 %copy-start.3 = (f32[256,2]{0,1:T(2,128)S(1)}, f32[256,2]{0,1:T(2,128)}, u32[]{:S(2)}) copy-start(f32[256,2]{0,1:T(2,128)} %param.18) | copy-start | bytes 6148
  61.1 56.4 %copy-start.4 = (f32[2,128]{1,0:T(2,128)S(1)}, f32[2,128]{1,0:T(2,128)}, u32[]{:S(2)}) copy-start(f32[2,128]{1,0:T(2,128)} %gain_ref.1) | copy-start | bytes 3076
  61.1 9.3 %collective-permute-start.20 = (bf16[256,512]{1,0:T(8,128)(2,1)S(1)}, bf16[256,512]{1,0:T(8,128)(2,1)S(1)}, u32[]{:S(2)}, u32[]{:S(2)}) collective-permute-start(bf16[256,512]{1,0:T(8,128)(2,1)S(1)} %get-tuple-element.63), channel_id=1, source_target_pairs={{0,1},{1,2},{2,3},{3,0},{4,5},{5,6},{6,7},{7,4},{8,9},{9,10},{10,1... | collective-permute-start | bytes 786440 | tf_op jit(solution)/shard_map/ppermute | solution.py:326
  61.5 8.9 %collective-permute-start.21 = (bf16[256,512]{1,0:T(8,128)(2,1)S(1)}, bf16[256,512]{1,0:T(8,128)(2,1)S(1)}, u32[]{:S(2)}, u32[]{:S(2)}) collective-permute-start(bf16[256,512]{1,0:T(8,128)(2,1)S(1)} %get-tuple-element.64), channel_id=1, source_target_pairs={{0,3},{1,0},{2,1},{3,2},{4,7},{5,4},{6,5},{7,6},{8,11},{9,8},{10,9... | collective-permute-start | bytes 786440 | tf_op jit(solution)/shard_map/ppermute | solution.py:326
  66.7 7.7 %collective-permute-start.19 = (bf16[256,512]{1,0:T(8,128)(2,1)S(1)}, bf16[256,512]{1,0:T(8,128)(2,1)S(1)}, u32[]{:S(2)}, u32[]{:S(2)}) collective-permute-start(bf16[256,512]{1,0:T(8,128)(2,1)S(1)} %get-tuple-element.62), channel_id=1, source_target_pairs={{0,1},{1,2},{2,3},{3,0},{4,5},{5,6},{6,7},{7,4},{8,9},{9,10},{10,1... | collective-permute-start | bytes 786440 | tf_op jit(solution)/shard_map/ppermute | solution.py:326
  68.2 6.4 %collective-permute-start.22 = (bf16[256,512]{1,0:T(8,128)(2,1)S(1)}, bf16[256,512]{1,0:T(8,128)(2,1)S(1)}, u32[]{:S(2)}, u32[]{:S(2)}) collective-permute-start(bf16[256,512]{1,0:T(8,128)(2,1)S(1)} %get-tuple-element.65), channel_id=1, source_target_pairs={{0,3},{1,0},{2,1},{3,2},{4,7},{5,4},{6,5},{7,6},{8,11},{9,8},{10,9... | collective-permute-start | bytes 786440 | tf_op jit(solution)/shard_map/ppermute | solution.py:326
  75.5 48.1 %all-to-all-start.1 = ((bf16[32,16,512]{2,1,0:T(8,128)(2,1)}), bf16[32,16,512]{2,1,0:T(8,128)(2,1)S(1)}, u32[]{:S(2)}, u32[]{:S(2)}) async-start(bf16[32,16,512]{2,1,0:T(8,128)(2,1)} %bitcast.10), calls=%async_computation.1 | async-start | bytes 1048576 | tf_op jit(solution)/shard_map/all_to_all | solution.py:335
  82.7 1.3 %collective-permute-start = (bf16[288,128]{1,0:T(8,128)(2,1)S(1)}, bf16[288,128]{1,0:T(8,128)(2,1)S(1)}, u32[]{:S(2)}, u32[]{:S(2)}) collective-permute-start(bf16[288,128]{1,0:T(8,128)(2,1)S(1)} %get-tuple-element.37), channel_id=1, source_target_pairs={{0,4},{4,0},{1,5},{5,1},{2,6},{6,2},{3,7},{7,3},{8,12},{12,8},{9,1... | collective-permute-start | bytes 221192 | tf_op jit(solution)/shard_map/ppermute | solution.py:326
  84.1 6.7 %collective-permute-start.1 = (bf16[288,128]{1,0:T(8,128)(2,1)S(1)}, bf16[288,128]{1,0:T(8,128)(2,1)S(1)}, u32[]{:S(2)}, u32[]{:S(2)}) collective-permute-start(bf16[288,128]{1,0:T(8,128)(2,1)S(1)} %shard_map.150.own_ref), channel_id=1, source_target_pairs={{0,8},{8,16},{16,24},{24,0},{1,9},{9,17},{17,25},{25,1},{2,10},{10... | collective-permute-start | bytes 221192 | tf_op jit(solution)/shard_map/ppermute | solution.py:326
  85.6 8.8 %collective-permute-start.2 = (bf16[288,128]{1,0:T(8,128)(2,1)S(1)}, bf16[288,128]{1,0:T(8,128)(2,1)S(1)}, u32[]{:S(2)}, u32[]{:S(2)}) collective-permute-start(bf16[288,128]{1,0:T(8,128)(2,1)S(1)} %shard_map.150.own_ref), channel_id=1, source_target_pairs={{0,16},{8,24},{16,0},{24,8},{1,17},{9,25},{17,1},{25,9},{2,18},{10... | collective-permute-start | bytes 221192 | tf_op jit(solution)/shard_map/ppermute | solution.py:326
  88.3 6.1 %collective-permute-start.3 = (bf16[288,128]{1,0:T(8,128)(2,1)S(1)}, bf16[288,128]{1,0:T(8,128)(2,1)S(1)}, u32[]{:S(2)}, u32[]{:S(2)}) collective-permute-start(bf16[288,128]{1,0:T(8,128)(2,1)S(1)} %shard_map.150.own_ref), channel_id=1, source_target_pairs={{0,24},{8,0},{16,8},{24,16},{1,25},{9,1},{17,9},{25,17},{2,26},{10... | collective-permute-start | bytes 221192 | tf_op jit(solution)/shard_map/ppermute | solution.py:326
  94.6 6.2 %collective-permute-start.4 = (bf16[288,128]{1,0:T(8,128)(2,1)S(1)}, bf16[288,128]{1,0:T(8,128)(2,1)S(1)}, u32[]{:S(2)}, u32[]{:S(2)}) collective-permute-start(bf16[288,128]{1,0:T(8,128)(2,1)S(1)} %get-tuple-element.38.own_ref), channel_id=1, source_target_pairs={{0,32},{32,64},{64,96},{96,128},{128,160},{160,192},{192,224},{1,3... | collective-permute-start | bytes 221192 | tf_op jit(solution)/shard_map/ppermute | solution.py:330
  100.9 6.5 %collective-permute-start.5 = (bf16[288,128]{1,0:T(8,128)(2,1)S(1)}, bf16[288,128]{1,0:T(8,128)(2,1)S(1)}, u32[]{:S(2)}, u32[]{:S(2)}) collective-permute-start(bf16[288,128]{1,0:T(8,128)(2,1)S(1)} %shard_map.152), channel_id=1, source_target_pairs={{0,64},{32,96},{64,128},{96,160},{128,192},{160,224},{1,65},{33,97... | collective-permute-start | bytes 221192 | tf_op jit(solution)/shard_map/ppermute | solution.py:330
  107.5 10.0 %collective-permute-start.6 = (bf16[288,128]{1,0:T(8,128)(2,1)S(1)}, bf16[288,128]{1,0:T(8,128)(2,1)S(1)}, u32[]{:S(2)}, u32[]{:S(2)}) collective-permute-start(bf16[288,128]{1,0:T(8,128)(2,1)S(1)} %get-tuple-element.39), channel_id=1, source_target_pairs={{0,128},{32,160},{64,192},{96,224},{1,129},{33,161},{65,193},{97,2... | collective-permute-start | bytes 221192 | tf_op jit(solution)/shard_map/ppermute | solution.py:330
  118.4 10.5 %collective-permute-start.7 = (bf16[64,2048]{1,0:T(8,128)(2,1)S(1)}, bf16[64,2048]{1,0:T(8,128)(2,1)S(1)}, u32[]{:S(2)}, u32[]{:S(2)}) collective-permute-start(bf16[64,2048]{1,0:T(8,128)(2,1)S(1)} %get-tuple-element.45), channel_id=1, source_target_pairs={{0,1},{1,2},{2,3},{3,0},{4,5},{5,6},{6,7},{7,4},{8,9},{9,10},{10,1... | collective-permute-start | bytes 786440 | tf_op jit(solution)/shard_map/ppermute | solution.py:326
  118.9 13.0 %collective-permute-start.8 = (bf16[64,2048]{1,0:T(8,128)(2,1)S(1)}, bf16[64,2048]{1,0:T(8,128)(2,1)S(1)}, u32[]{:S(2)}, u32[]{:S(2)}) collective-permute-start(bf16[64,2048]{1,0:T(8,128)(2,1)S(1)} %get-tuple-element.46), channel_id=1, source_target_pairs={{0,2},{1,3},{2,0},{3,1},{4,6},{5,7},{6,4},{7,5},{8,10},{9,11},{10,... | collective-permute-start | bytes 786440 | tf_op jit(solution)/shard_map/ppermute | solution.py:326
  123.2 8.7 %collective-permute-start.9 = (bf16[64,2048]{1,0:T(8,128)(2,1)S(1)}, bf16[64,2048]{1,0:T(8,128)(2,1)S(1)}, u32[]{:S(2)}, u32[]{:S(2)}) collective-permute-start(bf16[64,2048]{1,0:T(8,128)(2,1)S(1)} %get-tuple-element.47), channel_id=1, source_target_pairs={{0,3},{1,0},{2,1},{3,2},{4,7},{5,4},{6,5},{7,6},{8,11},{9,8},{10,9... | collective-permute-start | bytes 786440 | tf_op jit(solution)/shard_map/ppermute | solution.py:326
  123.6 9.3 %collective-permute-start.23 = (bf16[256,512]{1,0:T(8,128)(2,1)S(1)}, bf16[256,512]{1,0:T(8,128)(2,1)S(1)}, u32[]{:S(2)}, u32[]{:S(2)}) collective-permute-start(bf16[256,512]{1,0:T(8,128)(2,1)S(1)} %shard_map.166), channel_id=1, source_target_pairs={{0,4},{4,0},{1,5},{5,1},{2,6},{6,2},{3,7},{7,3},{8,12},{12,8},{9,1... | collective-permute-start | bytes 786440 | tf_op jit(solution)/shard_map/ppermute | solution.py:326
